TPU v7x, 128 devices: a whole 4x4x4 slice. The times are simulated.
128 devices in a mesh: sp: 32 (over z, y, core), tp: 4 (over x).
Axes of the slice: x: 4, y: 4, z: 4, core: 2. Of those that a mesh axis runs over, the one named last changes fastest.
Arguments:
- activations: bfloat16 [2, 1024, 1024], P(None, 'sp', 'tp'), may hold values from -6 to 6
- norm_gain: float32 [4, 1024], replicated, may hold values from 0.1 to 1.9
- in_weight: bfloat16 [4, 1024, 512], P(None, 'sp', 'tp'), may hold values from -0.1875 to 0.1875
- out_weight: bfloat16 [4, 512, 1024], P(None, 'tp', 'sp'), may hold values from -0.25 to 0.25
- mixing: bfloat16 [4, 4, 128, 128], P(None, 'tp', 'sp'), may hold values from -0.5 to 0.5
- pool_scale: float32 [4, 512], P(None, 'tp'), may hold values from 0.1 to 1.9
Outputs:
- result: bfloat16 [2, 1024, 1024], P(None, 'sp', 'tp')
All inputs are finite; a program needn't handle non-finite values.
Results may differ from a plain program's by a relative error of at most 0.03.
Values may be sent and summed in bfloat16 or wider, within the bound.
No kernel may reach another device: no remote copies, remote signals or barrier semaphores. Data moves between devices by JAX's collectives and lax.ppermute only.
A program may use at most 64 MiB of HBM per device.

v0:
```python
import functools

import jax
import jax.numpy as jnp
from jax import lax
from jax.experimental import pallas as pl
from jax.experimental.pallas import tpu as pltpu
from jax.sharding import PartitionSpec as P

NZ, NY, NC, NX = 4, 4, 2, 4
AXES = ("sp", "tp")


def flat(z, y, c, x):
    return (((z % NZ) * NY + y % NY) * NC + c) * NX + x % NX


def pairs(source_of):
    return [
        (flat(*source_of(z, y, c, x)), flat(z, y, c, x))
        for z in range(NZ)
        for y in range(NY)
        for c in range(NC)
        for x in range(NX)
    ]


def from_z(k):
    return pairs(lambda z, y, c, x: (z + k, y, c, x))


def from_x(k):
    return pairs(lambda z, y, c, x: (z, y, c, x + k))


def from_u(k):
    return pairs(lambda z, y, c, x: (z, y + k * c, c, x + k * (1 - c)))


def from_v(k):
    return pairs(lambda z, y, c, x: (z, y + k * (1 - c), c, x + k * c))


def from_core():
    return pairs(lambda z, y, c, x: (z, y, 1 - c, x))


def across_chips():
    count = NZ * NY * NC
    swap = []
    for low in range(1, count - 1, 2):
        for x in range(NX):
            swap += [(low * NX + x, (low + 1) * NX + x), ((low + 1) * NX + x, low * NX + x)]
    return swap


def send(value, perm):
    return lax.ppermute(value, AXES, perm)


def blocks(place, source, core, first_row):
    z, y, _, x = place
    column, across, along, corner = source
    first = core == 0
    for k in range(4):
        for j in range(4):
            y_at = lax.rem(y + jnp.where(first, k, j), NY)
            x_at = lax.rem(x + jnp.where(first, j, k), NX)
            for m in range(4):
                index = lax.rem(z + m, NZ) * (NY * NC) + y_at * NC + core
                if k == 0 and j == 0:
                    yield x_at, index, lambda lo, hi: column[m, first_row + lo : first_row + hi, :]
                elif k == 0:
                    yield x_at, index, lambda lo, hi: across[j - 1, m, lo:hi, :]
                elif j == 0:
                    yield (
                        x_at,
                        index,
                        lambda lo, hi: along[k - 1][m, first_row + lo : first_row + hi, :],
                    )
                else:
                    yield x_at, index, lambda lo, hi: corner[k - 1][j - 1, m, lo:hi, :]


def assemble(place, sources, first_row, counts, w_in, w_out, mix_raw=None):
    for source, core in sources:
        for x_at, index, take in blocks(place, source, core, first_row):
            rows = pl.ds(pl.multiple_of(index * 32, 32), 32)
            for l in range(counts):
                w_in[l, x_at, rows, :] = take(64 * l, 64 * l + 32)
                w_out[l, x_at, rows, :] = take(64 * l + 32, 64 * l + 64)
            if mix_raw is not None:
                mix_rows = pl.ds(pl.multiple_of(index * 16, 16), 16)
                mix_raw[x_at, mix_rows, :] = take(64 * counts, 64 * counts + 16)


def windows(start, seqs, span, seq_len):
    rows = seqs * span
    r = lax.broadcasted_iota(jnp.int32, (rows, rows), 0)
    q = lax.broadcasted_iota(jnp.int32, (rows, rows), 1)
    same = (r >= span) == (q >= span)
    pos_r = start + jnp.where(r >= span, r - span, r)
    pos_q = start + jnp.where(q >= span, q - span, q)
    r1 = lax.broadcasted_iota(jnp.int32, (rows, 1), 0)
    pos_1 = start + jnp.where(r1 >= span, r1 - span, r1)
    bands, inverse = [], []
    for g in range(4):
        half = 2**g
        low = jnp.clip(pos_r - half, 0, seq_len)
        high = jnp.clip(pos_r + half, 0, seq_len)
        bands.append(
            jnp.where(same & (pos_q >= low) & (pos_q < high), 1.0, 0.0).astype(jnp.bfloat16)
        )
        count = jnp.clip(pos_1 + half, 0, seq_len) - jnp.clip(pos_1 - half, 0, seq_len)
        inverse.append(1.0 / jnp.maximum(count, 1).astype(jnp.float32))
    return bands, inverse


def mix_layer(state, gain, w_in, scales, mixing, bands, inverse):
    mean = jnp.mean(state * state, axis=-1, keepdims=True)
    normed = (state * lax.rsqrt(mean + 1e-06) * gain).astype(jnp.bfloat16)
    weights = jnp.concatenate([w_in[g] for g in range(4)], axis=1)
    pooled = jnp.dot(normed, weights, preferred_element_type=jnp.float32).astype(jnp.bfloat16)
    mixed = []
    for g in range(4):
        part = pooled[:, 128 * g : 128 * (g + 1)]
        sums = jnp.dot(bands[g], part, preferred_element_type=jnp.float32)
        centred = (sums * inverse[g] - part.astype(jnp.float32)).astype(jnp.bfloat16)
        product = jnp.dot(
            centred, mixing[:, 128 * g : 128 * (g + 1)], preferred_element_type=jnp.float32
        )
        mixed.append((product * scales[g]).astype(jnp.bfloat16))
    return jnp.concatenate(mixed, axis=1)


def project_out(mixed, w_out):
    weights = jnp.concatenate([w_out(g) for g in range(4)], axis=1)
    out = lax.dot_general(
        mixed, weights, (((1,), (1,)), ((), ())), preferred_element_type=jnp.float32
    )
    return out.astype(jnp.bfloat16)


def split(refs):
    return refs[0], refs[1], refs[2:5], refs[5:8]


def first_half(dims, place_ref, *refs):
    layers, seqs, tok, halo, seq_len = dims
    own, other, acts, gain = split(refs[0:8]), split(refs[8:16]), refs[16:20], refs[20]
    state_out, mix_out, scale_out = refs[21:24]
    w_in, w_out, mix_raw, state_parts, scales = refs[24:]
    place = tuple(place_ref[k] for k in range(4))
    z, y, c, x = place
    half = layers // 2
    assemble(place, ((own, c), (other, 1 - c)), 0, half, w_in, w_out, mix_raw)
    span = tok + 2 * halo
    rows = seqs * span
    for k in range(4):
        x_at = lax.rem(x + k, NX)
        state_parts[x_at] = acts[k][:rows, :]
        parts = acts[k][rows : rows + 16, :128].astype(jnp.float32)
        scales[x_at] = parts[0:layers] + parts[layers : 2 * layers] + parts[2 * layers : 3 * layers]
    scale_out[...] = scales[...]
    bands, inverse = windows(((z * NY + y) * NC + c) * tok - halo, seqs, span, seq_len)

    pick_r = lax.broadcasted_iota(jnp.int32, (128, 512), 0)
    pick_q = lax.broadcasted_iota(jnp.int32, (128, 512), 1)
    base = ((pick_r >> 2) << 4) + (pick_r & 3)
    raw = jnp.concatenate([mix_raw[g] for g in range(4)], axis=1)
    mixings = []
    for l in range(layers):
        pick = jnp.where(pick_q == base + 4 * l, 1.0, 0.0).astype(jnp.bfloat16)
        mixings.append(
            jnp.dot(pick, raw, preferred_element_type=jnp.float32).astype(jnp.bfloat16)
        )
    for l in range(half, layers):
        mix_out[l - half] = mixings[l]

    state = jnp.concatenate([state_parts[k] for k in range(4)], axis=1)
    for l in range(half):
        row = [scales[g, l : l + 1, :] for g in range(4)]
        mixed = mix_layer(
            state.astype(jnp.float32),
            gain[l : l + 1, :],
            [w_in[l, g] for g in range(4)],
            row,
            mixings[l],
            bands,
            inverse,
        )
        state = project_out(mixed, lambda g: w_out[l, g])
    state_out[...] = state


def second_half(dims, place_ref, *refs):
    layers, seqs, tok, halo, seq_len = dims
    own, other = split(refs[0:8]), split(refs[8:16])
    state_in, mix_in, scales, gain, out, w_in, w_out = refs[16:]
    place = tuple(place_ref[k] for k in range(4))
    z, y, c, x = place
    half = layers // 2
    assemble(place, ((own, c), (other, 1 - c)), 64 * half + 16, half, w_in, w_out)
    span = tok + 2 * halo
    bands, inverse = windows(((z * NY + y) * NC + c) * tok - halo, seqs, span, seq_len)
    state = state_in[...]
    for l in range(half):
        at = half + l
        row = [scales[g, at : at + 1, :] for g in range(4)]
        mixed = mix_layer(
            state.astype(jnp.float32),
            gain[at : at + 1, :],
            [w_in[l, g] for g in range(4)],
            row,
            mix_in[l],
            bands,
            inverse,
        )
        if l < half - 1:
            state = project_out(mixed, lambda g: w_out[l, g])
        else:
            mixed = jnp.concatenate(
                [mixed[s * span + halo : s * span + halo + tok] for s in range(seqs)], axis=0
            )
            width = out.shape[-1]
            columns = pl.ds(pl.multiple_of(x * width, width), width)
            out[...] = project_out(mixed, lambda g: w_out[l, g, columns, :])


def scale_rows(scale, width):
    high = lax.reduce_precision(scale, 8, 7)
    middle = lax.reduce_precision(scale - high, 8, 7)
    terms = jnp.concatenate([high, middle, scale - high - middle]).astype(jnp.bfloat16)
    return jnp.pad(terms, ((0, 16 - terms.shape[0]), (0, width - terms.shape[1])))


def body(activations, norm_gain, in_weight, out_weight, mixing, pool_scale):
    layers = in_weight.shape[0]
    half = layers // 2
    seqs, tok, width = activations.shape
    i, x = lax.axis_index("sp"), lax.axis_index("tp")
    z, y, c = i // (NY * NC), (i // NC) % NY, i % NC
    seq_len = tok * NZ * NY * NC
    cut = 64 * half + 16

    pair = jnp.stack([in_weight, jnp.swapaxes(out_weight, 1, 2)], axis=1)
    pair = pair.reshape(64 * layers, 128)
    slab = jnp.concatenate(
        [pair[: 64 * half], mixing.reshape(4 * layers, 128), pair[64 * half :]]
    )
    column = jnp.stack([slab] + [send(slab, from_z(k)) for k in (1, 2, 3)])
    chip_mate = send(activations, from_core())
    next_chip = send(activations, across_chips())
    left = jnp.where(c == 0, next_chip, chip_mate)
    right = jnp.where(c == 0, chip_mate, next_chip)
    wide = jnp.concatenate([left, activations, right], axis=1)
    wide = wide.reshape(seqs * 3 * tok, width)
    wide = jnp.concatenate([wide, scale_rows(pool_scale, width)])

    across = jnp.stack([send(column, from_u(k)) for k in (1, 2, 3)])
    along = [send(column, from_v(k)) for k in (1, 2, 3)]
    early, late = across[:, :, :cut, :], across[:, :, cut:, :]
    corner_early = [send(early, from_v(k)) for k in (1, 2, 3)]
    acts = [wide] + [send(wide, from_x(k)) for k in (1, 2, 3)]
    corner_late = [send(late, from_v(k)) for k in (1, 2, 3)]
    column_2 = send(column, from_core())
    early_2 = send(early, from_core())
    along_2 = [send(part, from_core()) for part in along]
    late_2 = send(late, from_core())
    corner_early_2 = [send(part, from_core()) for part in corner_early]
    corner_late_2 = [send(part, from_core()) for part in corner_late]

    place = jnp.stack([z, y, c, x]).astype(jnp.int32)
    vmem = pl.BlockSpec(memory_space=pltpu.VMEM)
    smem = pl.BlockSpec(memory_space=pltpu.SMEM)
    rows = seqs * 3 * tok
    dims = (layers, seqs, tok, tok, seq_len)
    weights = pltpu.VMEM((half, 4, 1024, 128), jnp.bfloat16)
    params = pltpu.CompilerParams(vmem_limit_bytes=20 * 2**20)
    cost = pl.CostEstimate(flops=10**9, bytes_accessed=9 * 10**6, transcendentals=1000)
    state, mix_late, scales = pl.pallas_call(
        functools.partial(first_half, dims),
        out_shape=(
            jax.ShapeDtypeStruct((rows, NX * width), jnp.bfloat16),
            jax.ShapeDtypeStruct((layers - half, 128, 512), jnp.bfloat16),
            jax.ShapeDtypeStruct((4, layers, 128), jnp.float32),
        ),
        in_specs=[smem] + [vmem] * 21,
        out_specs=(vmem, vmem, vmem),
        scratch_shapes=[
            weights,
            weights,
            pltpu.VMEM((4, 512, 128), jnp.bfloat16),
            pltpu.VMEM((4, rows, width), jnp.bfloat16),
            pltpu.VMEM((4, layers, 128), jnp.float32),
        ],
        compiler_params=params,
        cost_estimate=cost,
        name="first_half",
    )(
        place,
        column,
        early,
        *along,
        *corner_early,
        column_2,
        early_2,
        *along_2,
        *corner_early_2,
        *acts,
        norm_gain,
    )
    result = pl.pallas_call(
        functools.partial(second_half, dims),
        out_shape=jax.ShapeDtypeStruct((seqs * tok, width), jnp.bfloat16),
        in_specs=[smem] + [vmem] * 20,
        out_specs=vmem,
        scratch_shapes=[weights, weights],
        compiler_params=params,
        cost_estimate=cost,
        name="second_half",
    )(
        place,
        column,
        late,
        *along,
        *corner_late,
        column_2,
        late_2,
        *along_2,
        *corner_late_2,
        state,
        mix_late,
        scales,
        norm_gain,
    )
    return result.reshape(seqs, tok, width)


def solution(mesh):
    return jax.shard_map(
        body,
        mesh=mesh,
        in_specs=(
            P(None, "sp", "tp"),
            P(),
            P(None, "sp", "tp"),
            P(None, "tp", "sp"),
            P(None, "tp", "sp", None),
            P(None, "tp"),
        ),
        out_specs=P(None, "sp", "tp"),
        check_vma=False,
    )
```

profile of v0, /device:TPU:0, one launch (start us, length us, event | category | flops | bytes accessed | tf_op | source)
XLA Modules:
  0.0 105.8 jit_solution(4552920923797470776)
XLA Ops:
  0.0 0.7 collective-permute-start.27
  0.7 3.1 %collective-permute-start.28 = (bf16[2,32,256]{2,1,0:T(8,128)(2,1)}, bf16[2,32,256]{2,1,0:T(8,128)(2,1)S(1)}, u32[]{:S(2)}, u32[]{:S(2)}) collective-permute-start(bf16[2,32,256]{2,1,0:T(8,128)(2,1)} %param.6), channel_id=1, source_target_pairs={{4,0},{5,1},{6,2},{7,3},{0,4},{1,5},{2,6},{3,7},{12,8},{13,9},{14,... | collective-permute-start | bytes 98312 | tf_op jit(solution)/shard_map/ppermute | solution.py:58
  3.8 0.8 fusion
  4.6 0.7 copy-done.18
  5.3 4.7 %collective-permute-start = (bf16[272,128]{1,0:T(8,128)(2,1)S(1)}, bf16[272,128]{1,0:T(8,128)(2,1)S(1)}, u32[]{:S(2)}, u32[]{:S(2)}) collective-permute-start(bf16[272,128]{1,0:T(8,128)(2,1)S(1)} %get-tuple-element.12), channel_id=1, source_target_pairs={{32,0},{33,1},{34,2},{35,3},{36,4},{37,5},{38,6},{39,7},{40,8},{41... | collective-permute-start | bytes 208904 | tf_op jit(solution)/shard_map/ppermute | solution.py:58
  10.0 1.0 collective-permute-start.2
  11.1 0.7 copy-done.17
  11.8 1.8 %collective-permute-done = bf16[272,128]{1,0:T(8,128)(2,1)S(1)} collective-permute-done((bf16[272,128]{1,0:T(8,128)(2,1)S(1)}, bf16[272,128]{1,0:T(8,128)(2,1)S(1)}, u32[]{:S(2)}, u32[]{:S(2)}) %collective-permute-start) | collective-permute-done | bytes 69664 | tf_op jit(solution)/shard_map/ppermute | solution.py:58
  13.6 2.9 %collective-permute-done.1 = bf16[272,128]{1,0:T(8,128)(2,1)S(1)} collective-permute-done((bf16[272,128]{1,0:T(8,128)(2,1)S(1)}, bf16[272,128]{1,0:T(8,128)(2,1)S(1)}, u32[]{:S(2)}, u32[]{:S(2)}) %collective-permute-start.1) | collective-permute-done | bytes 69664 | tf_op jit(solution)/shard_map/ppermute | solution.py:58
  16.6 0.5 collective-permute-done.2
  17.1 2.8 %collective-permute-start.3 = (bf16[4,272,128]{2,1,0:T(8,128)(2,1)S(1)}, bf16[4,272,128]{2,1,0:T(8,128)(2,1)S(1)}, u32[]{:S(2)}, u32[]{:S(2)}) collective-permute-start(bf16[4,272,128]{2,1,0:T(8,128)(2,1)S(1)} %pad_maximum_fusion.3.refs_0_), channel_id=1, source_target_pairs={{1,0},{2,1},{3,2},{0,3},{12,4},{13,5},{14,6},{15,7},{9,8},{10,9},{... | collective-permute-start | bytes 835592 | tf_op jit(solution)/shard_map/ppermute | solution.py:58
  19.9 0.8 collective-permute-start.4
  20.7 1.2 %collective-permute-start.29 = (bf16[208,256]{1,0:T(8,128)(2,1)S(1)}, bf16[208,256]{1,0:T(8,128)(2,1)S(1)}, u32[]{:S(2)}, u32[]{:S(2)}) collective-permute-start(bf16[208,256]{1,0:T(8,128)(2,1)S(1)} %pad_maximum_fusion.4.refs_16_), channel_id=1, source_target_pairs={{1,0},{2,1},{3,2},{0,3},{5,4},{6,5},{7,6},{4,7},{9,8},{10,9},{11,1... | collective-permute-start | bytes 319496 | tf_op jit(solution)/shard_map/ppermute | solution.py:58
  21.9 1.8 %collective-permute-start.30 = (bf16[208,256]{1,0:T(8,128)(2,1)S(1)}, bf16[208,256]{1,0:T(8,128)(2,1)S(1)}, u32[]{:S(2)}, u32[]{:S(2)}) collective-permute-start(bf16[208,256]{1,0:T(8,128)(2,1)S(1)} %pad_maximum_fusion.4.refs_16_), channel_id=1, source_target_pairs={{2,0},{3,1},{0,2},{1,3},{6,4},{7,5},{4,6},{5,7},{10,8},{11,9},{8,1... | collective-permute-start | bytes 319496 | tf_op jit(solution)/shard_map/ppermute | solution.py:58
  23.7 1.2 %collective-permute-start.6 = (bf16[4,272,128]{2,1,0:T(8,128)(2,1)S(1)}, bf16[4,272,128]{2,1,0:T(8,128)(2,1)S(1)}, u32[]{:S(2)}, u32[]{:S(2)}) collective-permute-start(bf16[4,272,128]{2,1,0:T(8,128)(2,1)S(1)} %pad_maximum_fusion.3.refs_0_), channel_id=1, source_target_pairs={{8,0},{9,1},{10,2},{11,3},{5,4},{6,5},{7,6},{4,7},{16,8},{17,9},{1... | collective-permute-start | bytes 835592 | tf_op jit(solution)/shard_map/ppermute | solution.py:58
  24.9 12.2 %collective-permute-done.29.refs_17_ = bf16[208,256]{1,0:T(8,128)(2,1)S(1)} collective-permute-done((bf16[208,256]{1,0:T(8,128)(2,1)S(1)}, bf16[208,256]{1,0:T(8,128)(2,1)S(1)}, u32[]{:S(2)}, u32[]{:S(2)}) %collective-permute-start.29) | collective-permute-done | bytes 106528 | tf_op jit(solution)/shard_map/ppermute | solution.py:58
  37.1 0.1 collective-permute-start.7
  37.2 0.4 collective-permute-start.8
  37.6 0.5 collective-permute-start.14
  38.1 8.5 %collective-permute-done.5 = bf16[4,272,128]{2,1,0:T(8,128)(2,1)S(1)} collective-permute-done((bf16[4,272,128]{2,1,0:T(8,128)(2,1)S(1)}, bf16[4,272,128]{2,1,0:T(8,128)(2,1)S(1)}, u32[]{:S(2)}, u32[]{:S(2)}) %collective-permute-start.5) | collective-permute-done | bytes 278560 | tf_op jit(solution)/shard_map/ppermute | solution.py:58
  46.7 5.8 %collective-permute-done.31.refs_19_ = bf16[208,256]{1,0:T(8,128)(2,1)S(1)} collective-permute-done((bf16[208,256]{1,0:T(8,128)(2,1)S(1)}, bf16[208,256]{1,0:T(8,128)(2,1)S(1)}, u32[]{:S(2)}, u32[]{:S(2)}) %collective-permute-start.31) | collective-permute-done | bytes 106528 | tf_op jit(solution)/shard_map/ppermute | solution.py:58
  52.5 0.6 copy-done.14
  53.2 1.2 %collective-permute-start.21 = (bf16[3,4,144,128]{3,2,1,0:T(8,128)(2,1)S(1)}, bf16[3,4,144,128]{3,2,1,0:T(8,128)(2,1)S(1)}, u32[]{:S(2)}, u32[]{:S(2)}) collective-permute-start(bf16[3,4,144,128]{3,2,1,0:T(8,128)(2,1)S(1)} %pad_maximum_fusion.refs_1_), channel_id=1, source_target_pairs={{16,0},{17,1},{18,2},{19,3},{6,4},{7,5},{4,6},{5,7},{24,8},{25,9},... | collective-permute-start | bytes 1327112 | tf_op jit(solution)/shard_map/ppermute | solution.py:58
  54.4 3.6 %collective-permute-start.9 = (bf16[3,4,128,128]{3,2,1,0:T(8,128)(2,1)S(1)}, bf16[3,4,128,128]{3,2,1,0:T(8,128)(2,1)}, u32[]{:S(2)}, u32[]{:S(2)}) collective-permute-start(bf16[3,4,128,128]{3,2,1,0:T(8,128)(2,1)S(1)} %pad_maximum_fusion.2.refs_1_), channel_id=1, source_target_pairs={{8,0},{9,1},{10,2},{11,3},{5,4},{6,5},{7,6},{4,7},{16,8},{17,9},{1... | collective-permute-start | bytes 1179656 | tf_op jit(solution)/shard_map/ppermute | solution.py:58
  58.0 1.0 collective-permute-start.22
  59.0 11.6 %collective-permute-done.9.refs_5_ = bf16[3,4,128,128]{3,2,1,0:T(8,128)(2,1)} collective-permute-done((bf16[3,4,128,128]{3,2,1,0:T(8,128)(2,1)S(1)}, bf16[3,4,128,128]{3,2,1,0:T(8,128)(2,1)}, u32[]{:S(2)}, u32[]{:S(2)}) %collective-permute-start.9) | collective-permute-done | bytes 393248 | tf_op jit(solution)/shard_map/ppermute | solution.py:58
  70.6 0.5 collective-permute-start.24
  71.1 0.1 collective-permute-start.25
  71.2 0.8 copy-done
  71.9 2.3 %collective-permute-start.11 = (bf16[3,4,128,128]{3,2,1,0:T(8,128)(2,1)S(1)}, bf16[3,4,128,128]{3,2,1,0:T(8,128)(2,1)}, u32[]{:S(2)}, u32[]{:S(2)}) collective-permute-start(bf16[3,4,128,128]{3,2,1,0:T(8,128)(2,1)S(1)} %pad_maximum_fusion.2.refs_1_), channel_id=1, source_target_pairs={{24,0},{25,1},{26,2},{27,3},{7,4},{4,5},{5,6},{6,7},{0,8},{1,9},{2... | collective-permute-start | bytes 1179656 | tf_op jit(solution)/shard_map/ppermute | solution.py:58
  74.2 9.1 %collective-permute-done.11.refs_7_ = bf16[3,4,128,128]{3,2,1,0:T(8,128)(2,1)} collective-permute-done((bf16[3,4,128,128]{3,2,1,0:T(8,128)(2,1)S(1)}, bf16[3,4,128,128]{3,2,1,0:T(8,128)(2,1)}, u32[]{:S(2)}, u32[]{:S(2)}) %collective-permute-start.11) | collective-permute-done | bytes 393248 | tf_op jit(solution)/shard_map/ppermute | solution.py:58
  83.3 0.8 copy-done.2
  84.1 0.5 collective-permute-start.17
  84.6 0.8 copy-done.4
  85.4 0.8 copy-done.6
  86.1 0.5 collective-permute-start.19
  86.7 0.1 pad_add_fusion.place_ref
  86.7 0.6 copy-done.16
  87.4 1.0 copy-done.1
  88.4 1.0 copy-done.3
  89.4 1.0 copy-done.5
  90.4 1.0 copy-done.7
  91.4 0.9 copy-done.9
  92.3 0.9 copy-done.11
  93.2 0.9 copy-done.13
  94.1 0.9 copy-done.15
  95.0 5.1 %first_half.1 = (bf16[192,1024]{1,0:T(8,128)(2,1)S(1)}, bf16[2,128,512]{2,1,0:T(8,128)(2,1)S(1)}, f32[4,4,128]{2,1,0:T(4,128)S(1)}) custom-call(s32[4]{0:T(128)S(1)} %pad_add_fusion.place_ref, bf16[4,272,128]{2,1,0:T(8,128)(2,1)S(1)} %pad_maximum_fusion.3.refs_0_, bf16[3,4,144,128]{3,2,1,0:T(8,128)(2,1)S(1)} %pad_maximum_fusion.refs_1_, ...), custom_call_target="tpu_custom_call" | custom-call | flops 1000000000 | bytes 9000000 | tf_op jit(solution)/shard_map/first_half/pallas_call | solution.py:281
  100.2 5.6 %second_half.1 = bf16[64,256]{1,0:T(8,128)(2,1)} custom-call(s32[4]{0:T(128)S(1)} %pad_add_fusion.place_ref, bf16[4,272,128]{2,1,0:T(8,128)(2,1)S(1)} %pad_maximum_fusion.3.refs_0_, bf16[3,4,128,128]{3,2,1,0:T(8,128)(2,1)S(1)} %pad_maximum_fusion.2.refs_1_, bf16[4,272,128]{2,1,0:T(8,128)(2,1)S(1)} %collective-permute-done.6.refs_2_, ...), custom_call_target="tpu_custom_call" | custom-call | flops 1000000000 | bytes 9000000 | tf_op jit(solution)/shard_map/second_half/pallas_call | solution.py:313
  (71 shorter events, 0.3 us)
Async XLA Ops:
  0.0 11.0 %collective-permute-start.27 = (bf16[2,32,256]{2,1,0:T(8,128)(2,1)}, bf16[2,32,256]{2,1,0:T(8,128)(2,1)S(1)}, u32[]{:S(2)}, u32[]{:S(2)}) collective-permute-start(bf16[2,32,256]{2,1,0:T(8,128)(2,1)} %param.6), channel_id=1, source_target_pairs={{4,8},{8,4},{5,9},{9,5},{6,10},{10,6},{7,11},{11,7},{12,16},{16,12... | collective-permute-start | bytes 98312 | tf_op jit(solution)/shard_map/ppermute | solution.py:58
  0.7 10.4 %collective-permute-start.28 = (bf16[2,32,256]{2,1,0:T(8,128)(2,1)}, bf16[2,32,256]{2,1,0:T(8,128)(2,1)S(1)}, u32[]{:S(2)}, u32[]{:S(2)}) collective-permute-start(bf16[2,32,256]{2,1,0:T(8,128)(2,1)} %param.6), channel_id=1, source_target_pairs={{4,0},{5,1},{6,2},{7,3},{0,4},{1,5},{2,6},{3,7},{12,8},{13,9},{14,... | collective-permute-start | bytes 98312 | tf_op jit(solution)/shard_map/ppermute | solution.py:58
  5.3 5.7 %copy-start.19 = (f32[4,128]{1,0:T(4,128)S(1)}, f32[4,128]{1,0:T(4,128)}, u32[]{:S(2)}) copy-start(f32[4,128]{1,0:T(4,128)} %param.11) | copy-start | bytes 6148
  5.3 8.3 %collective-permute-start = (bf16[272,128]{1,0:T(8,128)(2,1)S(1)}, bf16[272,128]{1,0:T(8,128)(2,1)S(1)}, u32[]{:S(2)}, u32[]{:S(2)}) collective-permute-start(bf16[272,128]{1,0:T(8,128)(2,1)S(1)} %get-tuple-element.12), channel_id=1, source_target_pairs={{32,0},{33,1},{34,2},{35,3},{36,4},{37,5},{38,6},{39,7},{40,8},{41... | collective-permute-start | bytes 208904 | tf_op jit(solution)/shard_map/ppermute | solution.py:58
  10.0 6.5 %collective-permute-start.1 = (bf16[272,128]{1,0:T(8,128)(2,1)S(1)}, bf16[272,128]{1,0:T(8,128)(2,1)S(1)}, u32[]{:S(2)}, u32[]{:S(2)}) collective-permute-start(bf16[272,128]{1,0:T(8,128)(2,1)S(1)} %get-tuple-element.12), channel_id=1, source_target_pairs={{64,0},{65,1},{66,2},{67,3},{68,4},{69,5},{70,6},{71,7},{72,8},{73... | collective-permute-start | bytes 208904 | tf_op jit(solution)/shard_map/ppermute | solution.py:58
  10.0 7.0 %collective-permute-start.2 = (bf16[272,128]{1,0:T(8,128)(2,1)S(1)}, bf16[272,128]{1,0:T(8,128)(2,1)S(1)}, u32[]{:S(2)}, u32[]{:S(2)}) collective-permute-start(bf16[272,128]{1,0:T(8,128)(2,1)S(1)} %get-tuple-element.12), channel_id=1, source_target_pairs={{96,0},{97,1},{98,2},{99,3},{100,4},{101,5},{102,6},{103,7},{104,8... | collective-permute-start | bytes 208904 | tf_op jit(solution)/shard_map/ppermute | solution.py:58
  11.0 0.8 copy-start.17
  17.1 20.2 %collective-permute-start.3 = (bf16[4,272,128]{2,1,0:T(8,128)(2,1)S(1)}, bf16[4,272,128]{2,1,0:T(8,128)(2,1)S(1)}, u32[]{:S(2)}, u32[]{:S(2)}) collective-permute-start(bf16[4,272,128]{2,1,0:T(8,128)(2,1)S(1)} %pad_maximum_fusion.3.refs_0_), channel_id=1, source_target_pairs={{1,0},{2,1},{3,2},{0,3},{12,4},{13,5},{14,6},{15,7},{9,8},{10,9},{... | collective-permute-start | bytes 835592 | tf_op jit(solution)/shard_map/ppermute | solution.py:58
  19.9 17.7 %collective-permute-start.4 = (bf16[4,272,128]{2,1,0:T(8,128)(2,1)S(1)}, bf16[4,272,128]{2,1,0:T(8,128)(2,1)S(1)}, u32[]{:S(2)}, u32[]{:S(2)}) collective-permute-start(bf16[4,272,128]{2,1,0:T(8,128)(2,1)S(1)} %pad_maximum_fusion.3.refs_0_), channel_id=1, source_target_pairs={{2,0},{3,1},{0,2},{1,3},{20,4},{21,5},{22,6},{23,7},{10,8},{11,9},... | collective-permute-start | bytes 835592 | tf_op jit(solution)/shard_map/ppermute | solution.py:58
  20.7 26.0 %copy-start.8 = (bf16[208,256]{1,0:T(8,128)(2,1)}, bf16[208,256]{1,0:T(8,128)(2,1)S(1)}, u32[]{:S(2)}) copy-start(bf16[208,256]{1,0:T(8,128)(2,1)S(1)} %pad_maximum_fusion.4.refs_16_) | copy-start | bytes 319492
  20.7 16.4 %collective-permute-start.29 = (bf16[208,256]{1,0:T(8,128)(2,1)S(1)}, bf16[208,256]{1,0:T(8,128)(2,1)S(1)}, u32[]{:S(2)}, u32[]{:S(2)}) collective-permute-start(bf16[208,256]{1,0:T(8,128)(2,1)S(1)} %pad_maximum_fusion.4.refs_16_), channel_id=1, source_target_pairs={{1,0},{2,1},{3,2},{0,3},{5,4},{6,5},{7,6},{4,7},{9,8},{10,9},{11,1... | collective-permute-start | bytes 319496 | tf_op jit(solution)/shard_map/ppermute | solution.py:58
  21.9 15.2 %collective-permute-start.30 = (bf16[208,256]{1,0:T(8,128)(2,1)S(1)}, bf16[208,256]{1,0:T(8,128)(2,1)S(1)}, u32[]{:S(2)}, u32[]{:S(2)}) collective-permute-start(bf16[208,256]{1,0:T(8,128)(2,1)S(1)} %pad_maximum_fusion.4.refs_16_), channel_id=1, source_target_pairs={{2,0},{3,1},{0,2},{1,3},{6,4},{7,5},{4,6},{5,7},{10,8},{11,9},{8,1... | collective-permute-start | bytes 319496 | tf_op jit(solution)/shard_map/ppermute | solution.py:58
  23.7 13.9 %collective-permute-start.6 = (bf16[4,272,128]{2,1,0:T(8,128)(2,1)S(1)}, bf16[4,272,128]{2,1,0:T(8,128)(2,1)S(1)}, u32[]{:S(2)}, u32[]{:S(2)}) collective-permute-start(bf16[4,272,128]{2,1,0:T(8,128)(2,1)S(1)} %pad_maximum_fusion.3.refs_0_), channel_id=1, source_target_pairs={{8,0},{9,1},{10,2},{11,3},{5,4},{6,5},{7,6},{4,7},{16,8},{17,9},{1... | collective-permute-start | bytes 835592 | tf_op jit(solution)/shard_map/ppermute | solution.py:58
  37.1 9.6 %copy-start.10 = (bf16[208,256]{1,0:T(8,128)(2,1)}, bf16[208,256]{1,0:T(8,128)(2,1)S(1)}, u32[]{:S(2)}) copy-start(bf16[208,256]{1,0:T(8,128)(2,1)S(1)} %collective-permute-done.29.refs_17_) | copy-start | bytes 319492
  37.1 9.5 %collective-permute-start.5 = (bf16[4,272,128]{2,1,0:T(8,128)(2,1)S(1)}, bf16[4,272,128]{2,1,0:T(8,128)(2,1)S(1)}, u32[]{:S(2)}, u32[]{:S(2)}) collective-permute-start(bf16[4,272,128]{2,1,0:T(8,128)(2,1)S(1)} %pad_maximum_fusion.3.refs_0_), channel_id=1, source_target_pairs={{3,0},{0,1},{1,2},{2,3},{28,4},{29,5},{30,6},{31,7},{11,8},{8,9},{... | collective-permute-start | bytes 835592 | tf_op jit(solution)/shard_map/ppermute | solution.py:58
  37.1 9.6 %copy-start.12 = (bf16[208,256]{1,0:T(8,128)(2,1)}, bf16[208,256]{1,0:T(8,128)(2,1)S(1)}, u32[]{:S(2)}) copy-start(bf16[208,256]{1,0:T(8,128)(2,1)S(1)} %collective-permute-done.30.refs_18_) | copy-start | bytes 319492
  37.1 9.5 %collective-permute-start.7 = (bf16[4,272,128]{2,1,0:T(8,128)(2,1)S(1)}, bf16[4,272,128]{2,1,0:T(8,128)(2,1)S(1)}, u32[]{:S(2)}, u32[]{:S(2)}) collective-permute-start(bf16[4,272,128]{2,1,0:T(8,128)(2,1)S(1)} %pad_maximum_fusion.3.refs_0_), channel_id=1, source_target_pairs={{16,0},{17,1},{18,2},{19,3},{6,4},{7,5},{4,6},{5,7},{24,8},{25,9},... | collective-permute-start | bytes 835592 | tf_op jit(solution)/shard_map/ppermute | solution.py:58
  37.2 15.9 %collective-permute-start.8 = (bf16[4,272,128]{2,1,0:T(8,128)(2,1)S(1)}, bf16[4,272,128]{2,1,0:T(8,128)(2,1)S(1)}, u32[]{:S(2)}, u32[]{:S(2)}) collective-permute-start(bf16[4,272,128]{2,1,0:T(8,128)(2,1)S(1)} %pad_maximum_fusion.3.refs_0_), channel_id=1, source_target_pairs={{24,0},{25,1},{26,2},{27,3},{7,4},{4,5},{5,6},{6,7},{0,8},{1,9},{2... | collective-permute-start | bytes 835592 | tf_op jit(solution)/shard_map/ppermute | solution.py:58
  37.6 16.8 %collective-permute-start.12 = (bf16[4,272,128]{2,1,0:T(8,128)(2,1)S(1)}, bf16[4,272,128]{2,1,0:T(8,128)(2,1)S(1)}, u32[]{:S(2)}, u32[]{:S(2)}) collective-permute-start(bf16[4,272,128]{2,1,0:T(8,128)(2,1)S(1)} %pad_maximum_fusion.3.refs_0_), channel_id=1, source_target_pairs={{4,0},{5,1},{6,2},{7,3},{0,4},{1,5},{2,6},{3,7},{12,8},{13,9},{14,... | collective-permute-start | bytes 835592 | tf_op jit(solution)/shard_map/ppermute | solution.py:58
  37.6 16.8 %collective-permute-start.14 = (bf16[4,272,128]{2,1,0:T(8,128)(2,1)S(1)}, bf16[4,272,128]{2,1,0:T(8,128)(2,1)S(1)}, u32[]{:S(2)}, u32[]{:S(2)}) collective-permute-start(bf16[4,272,128]{2,1,0:T(8,128)(2,1)S(1)} %collective-permute-done.6.refs_2_), channel_id=1, source_target_pairs={{4,0},{5,1},{6,2},{7,3},{0,4},{1,5},{2,6},{3,7},{12,8},{13,9},{14,... | collective-permute-start | bytes 835592 | tf_op jit(solution)/shard_map/ppermute | solution.py:58
  46.6 5.9 %collective-permute-start.31 = (bf16[208,256]{1,0:T(8,128)(2,1)S(1)}, bf16[208,256]{1,0:T(8,128)(2,1)S(1)}, u32[]{:S(2)}, u32[]{:S(2)}) collective-permute-start(bf16[208,256]{1,0:T(8,128)(2,1)S(1)} %pad_maximum_fusion.4.refs_16_), channel_id=1, source_target_pairs={{3,0},{0,1},{1,2},{2,3},{7,4},{4,5},{5,6},{6,7},{11,8},{8,9},{9,10... | collective-permute-start | bytes 319496 | tf_op jit(solution)/shard_map/ppermute | solution.py:58
  46.6 11.4 %collective-permute-start.15 = (bf16[4,272,128]{2,1,0:T(8,128)(2,1)S(1)}, bf16[4,272,128]{2,1,0:T(8,128)(2,1)S(1)}, u32[]{:S(2)}, u32[]{:S(2)}) collective-permute-start(bf16[4,272,128]{2,1,0:T(8,128)(2,1)S(1)} %collective-permute-done.7.refs_3_), channel_id=1, source_target_pairs={{4,0},{5,1},{6,2},{7,3},{0,4},{1,5},{2,6},{3,7},{12,8},{13,9},{14,... | collective-permute-start | bytes 835592 | tf_op jit(solution)/shard_map/ppermute | solution.py:58
  53.2 17.4 %collective-permute-start.20 = (bf16[3,4,144,128]{3,2,1,0:T(8,128)(2,1)S(1)}, bf16[3,4,144,128]{3,2,1,0:T(8,128)(2,1)S(1)}, u32[]{:S(2)}, u32[]{:S(2)}) collective-permute-start(bf16[3,4,144,128]{3,2,1,0:T(8,128)(2,1)S(1)} %pad_maximum_fusion.refs_1_), channel_id=1, source_target_pairs={{8,0},{9,1},{10,2},{11,3},{5,4},{6,5},{7,6},{4,7},{16,8},{17,9},{1... | collective-permute-start | bytes 1327112 | tf_op jit(solution)/shard_map/ppermute | solution.py:58
  53.2 17.9 %collective-permute-start.21 = (bf16[3,4,144,128]{3,2,1,0:T(8,128)(2,1)S(1)}, bf16[3,4,144,128]{3,2,1,0:T(8,128)(2,1)S(1)}, u32[]{:S(2)}, u32[]{:S(2)}) collective-permute-start(bf16[3,4,144,128]{3,2,1,0:T(8,128)(2,1)S(1)} %pad_maximum_fusion.refs_1_), channel_id=1, source_target_pairs={{16,0},{17,1},{18,2},{19,3},{6,4},{7,5},{4,6},{5,7},{24,8},{25,9},... | collective-permute-start | bytes 1327112 | tf_op jit(solution)/shard_map/ppermute | solution.py:58
  54.4 3.6 %collective-permute-start.16 = (bf16[4,272,128]{2,1,0:T(8,128)(2,1)S(1)}, bf16[4,272,128]{2,1,0:T(8,128)(2,1)S(1)}, u32[]{:S(2)}, u32[]{:S(2)}) collective-permute-start(bf16[4,272,128]{2,1,0:T(8,128)(2,1)S(1)} %collective-permute-done.8.refs_4_), channel_id=1, source_target_pairs={{4,0},{5,1},{6,2},{7,3},{0,4},{1,5},{2,6},{3,7},{12,8},{13,9},{14,... | collective-permute-start | bytes 835592 | tf_op jit(solution)/shard_map/ppermute | solution.py:58
  54.4 16.1 %collective-permute-start.9 = (bf16[3,4,128,128]{3,2,1,0:T(8,128)(2,1)S(1)}, bf16[3,4,128,128]{3,2,1,0:T(8,128)(2,1)}, u32[]{:S(2)}, u32[]{:S(2)}) collective-permute-start(bf16[3,4,128,128]{3,2,1,0:T(8,128)(2,1)S(1)} %pad_maximum_fusion.2.refs_1_), channel_id=1, source_target_pairs={{8,0},{9,1},{10,2},{11,3},{5,4},{6,5},{7,6},{4,7},{16,8},{17,9},{1... | collective-permute-start | bytes 1179656 | tf_op jit(solution)/shard_map/ppermute | solution.py:58
  58.0 13.9 %collective-permute-start.10 = (bf16[3,4,128,128]{3,2,1,0:T(8,128)(2,1)S(1)}, bf16[3,4,128,128]{3,2,1,0:T(8,128)(2,1)}, u32[]{:S(2)}, u32[]{:S(2)}) collective-permute-start(bf16[3,4,128,128]{3,2,1,0:T(8,128)(2,1)S(1)} %pad_maximum_fusion.2.refs_1_), channel_id=1, source_target_pairs={{16,0},{17,1},{18,2},{19,3},{6,4},{7,5},{4,6},{5,7},{24,8},{25,9},... | collective-permute-start | bytes 1179656 | tf_op jit(solution)/shard_map/ppermute | solution.py:58
  58.0 16.2 %collective-permute-start.22 = (bf16[3,4,144,128]{3,2,1,0:T(8,128)(2,1)S(1)}, bf16[3,4,144,128]{3,2,1,0:T(8,128)(2,1)}, u32[]{:S(2)}, u32[]{:S(2)}) collective-permute-start(bf16[3,4,144,128]{3,2,1,0:T(8,128)(2,1)S(1)} %pad_maximum_fusion.refs_1_), channel_id=1, source_target_pairs={{24,0},{25,1},{26,2},{27,3},{7,4},{4,5},{5,6},{6,7},{0,8},{1,9},{2... | collective-permute-start | bytes 1327112 | tf_op jit(solution)/shard_map/ppermute | solution.py:58
  70.6 12.8 %collective-permute-start.23 = (bf16[3,4,144,128]{3,2,1,0:T(8,128)(2,1)S(1)}, bf16[3,4,144,128]{3,2,1,0:T(8,128)(2,1)S(1)}, u32[]{:S(2)}, u32[]{:S(2)}) collective-permute-start(bf16[3,4,144,128]{3,2,1,0:T(8,128)(2,1)S(1)} %pad_maximum_fusion.refs_1_), channel_id=1, source_target_pairs={{4,0},{5,1},{6,2},{7,3},{0,4},{1,5},{2,6},{3,7},{12,8},{13,9},{14,... | collective-permute-start | bytes 1327112 | tf_op jit(solution)/shard_map/ppermute | solution.py:58
  70.6 14.0 %collective-permute-start.24 = (bf16[3,4,144,128]{3,2,1,0:T(8,128)(2,1)S(1)}, bf16[3,4,144,128]{3,2,1,0:T(8,128)(2,1)S(1)}, u32[]{:S(2)}, u32[]{:S(2)}) collective-permute-start(bf16[3,4,144,128]{3,2,1,0:T(8,128)(2,1)S(1)} %collective-permute-done.20.refs_5_), channel_id=1, source_target_pairs={{4,0},{5,1},{6,2},{7,3},{0,4},{1,5},{2,6},{3,7},{12,8},{13,9},{14,... | collective-permute-start | bytes 1327112 | tf_op jit(solution)/shard_map/ppermute | solution.py:58
  71.1 14.3 %collective-permute-start.25 = (bf16[3,4,144,128]{3,2,1,0:T(8,128)(2,1)S(1)}, bf16[3,4,144,128]{3,2,1,0:T(8,128)(2,1)S(1)}, u32[]{:S(2)}, u32[]{:S(2)}) collective-permute-start(bf16[3,4,144,128]{3,2,1,0:T(8,128)(2,1)S(1)} %collective-permute-done.21.refs_6_), channel_id=1, source_target_pairs={{4,0},{5,1},{6,2},{7,3},{0,4},{1,5},{2,6},{3,7},{12,8},{13,9},{14,... | collective-permute-start | bytes 1327112 | tf_op jit(solution)/shard_map/ppermute | solution.py:58
  71.2 0.8 copy-start
  71.9 11.4 %collective-permute-start.11 = (bf16[3,4,128,128]{3,2,1,0:T(8,128)(2,1)S(1)}, bf16[3,4,128,128]{3,2,1,0:T(8,128)(2,1)}, u32[]{:S(2)}, u32[]{:S(2)}) collective-permute-start(bf16[3,4,128,128]{3,2,1,0:T(8,128)(2,1)S(1)} %pad_maximum_fusion.2.refs_1_), channel_id=1, source_target_pairs={{24,0},{25,1},{26,2},{27,3},{7,4},{4,5},{5,6},{6,7},{0,8},{1,9},{2... | collective-permute-start | bytes 1179656 | tf_op jit(solution)/shard_map/ppermute | solution.py:58
  74.2 12.5 %collective-permute-start.26 = (bf16[3,4,144,128]{3,2,1,0:T(8,128)(2,1)}, bf16[3,4,144,128]{3,2,1,0:T(8,128)(2,1)}, u32[]{:S(2)}, u32[]{:S(2)}) collective-permute-start(bf16[3,4,144,128]{3,2,1,0:T(8,128)(2,1)} %collective-permute-done.22.refs_7_), channel_id=1, source_target_pairs={{4,0},{5,1},{6,2},{7,3},{0,4},{1,5},{2,6},{3,7},{12,8},{13,9},{14,... | collective-permute-start | bytes 1327112 | tf_op jit(solution)/shard_map/ppermute | solution.py:58
  83.3 16.8 %collective-permute-start.13 = (bf16[3,4,128,128]{3,2,1,0:T(8,128)(2,1)S(1)}, bf16[3,4,128,128]{3,2,1,0:T(8,128)(2,1)}, u32[]{:S(2)}, u32[]{:S(2)}) collective-permute-start(bf16[3,4,128,128]{3,2,1,0:T(8,128)(2,1)S(1)} %pad_maximum_fusion.2.refs_1_), channel_id=1, source_target_pairs={{4,0},{5,1},{6,2},{7,3},{0,4},{1,5},{2,6},{3,7},{12,8},{13,9},{14,... | collective-permute-start | bytes 1179656 | tf_op jit(solution)/shard_map/ppermute | solution.py:58
  83.3 0.8 copy-start.2
  84.1 16.0 %collective-permute-start.17 = (bf16[3,4,128,128]{3,2,1,0:T(8,128)(2,1)}, bf16[3,4,128,128]{3,2,1,0:T(8,128)(2,1)}, u32[]{:S(2)}, u32[]{:S(2)}) collective-permute-start(bf16[3,4,128,128]{3,2,1,0:T(8,128)(2,1)} %collective-permute-done.9.refs_5_), channel_id=1, source_target_pairs={{4,0},{5,1},{6,2},{7,3},{0,4},{1,5},{2,6},{3,7},{12,8},{13,9},{14,... | collective-permute-start | bytes 1179656 | tf_op jit(solution)/shard_map/ppermute | solution.py:58
  84.6 0.8 copy-start.4
  85.4 14.8 %collective-permute-start.18 = (bf16[3,4,128,128]{3,2,1,0:T(8,128)(2,1)}, bf16[3,4,128,128]{3,2,1,0:T(8,128)(2,1)}, u32[]{:S(2)}, u32[]{:S(2)}) collective-permute-start(bf16[3,4,128,128]{3,2,1,0:T(8,128)(2,1)} %collective-permute-done.10.refs_6_), channel_id=1, source_target_pairs={{4,0},{5,1},{6,2},{7,3},{0,4},{1,5},{2,6},{3,7},{12,8},{13,9},{14,... | collective-permute-start | bytes 1179656 | tf_op jit(solution)/shard_map/ppermute | solution.py:58
  86.1 14.0 %collective-permute-start.19 = (bf16[3,4,128,128]{3,2,1,0:T(8,128)(2,1)}, bf16[3,4,128,128]{3,2,1,0:T(8,128)(2,1)}, u32[]{:S(2)}, u32[]{:S(2)}) collective-permute-start(bf16[3,4,128,128]{3,2,1,0:T(8,128)(2,1)} %collective-permute-done.11.refs_7_), channel_id=1, source_target_pairs={{4,0},{5,1},{6,2},{7,3},{0,4},{1,5},{2,6},{3,7},{12,8},{13,9},{14,... | collective-permute-start | bytes 1179656 | tf_op jit(solution)/shard_map/ppermute | solution.py:58
  87.4 1.0 copy-start.1
  88.4 1.0 copy-start.3
  89.4 1.0 copy-start.5
  90.4 1.0 copy-start.7
  91.4 0.9 copy-start.9
  92.3 0.9 copy-start.11
  93.2 0.9 copy-start.13
  94.1 0.9 copy-start.15
  (4 other events, 2.8 us)
where the time goes:
time: 107 us; the launch traced here: 106 us
  waiting for transfers between devices  52.5 us (49%)
  starting transfers between devices  27.9 us (26%)
  local copies, waits for them, and re-layouts  13.4 us (13%)
  Pallas kernels  10.7 us (10%)
    ppermute x32, waiting for transfers between devices, send(): return lax.ppermute(value, AXES, perm)  52.5 us
    ppermute x32, starting transfers between devices, send(): return lax.ppermute(value, AXES, perm)  27.9 us
    unnamed x40, local copies, waits for them, and re-layouts  13.4 us
    pallas_call x1, Pallas kernels, body(): pl.pallas_call(functools.partial(second_half, dims), out_shape=jax.ShapeD...  5.6 us
    pallas_call x1, Pallas kernels, body(): pl.pallas_call(functools.partial(first_half, dims), out_shape=(jax.ShapeD...  5.1 us
  transfers between devices with their start and end apart: 32, of which 8 were waited for; matrix products, arithmetic and copies ran while one was open for 1% of the time, Pallas kernels for 5%

commit v1 on v0

--- a/solution.py
+++ b/solution.py
@@ -29,10 +29,6 @@
     return pairs(lambda z, y, c, x: (z + k, y, c, x))
 
 
-def from_x(k):
-    return pairs(lambda z, y, c, x: (z, y, c, x + k))
-
-
 def from_u(k):
     return pairs(lambda z, y, c, x: (z, y + k * c, c, x + k * (1 - c)))
 
@@ -58,40 +54,32 @@
     return lax.ppermute(value, AXES, perm)
 
 
-def blocks(place, source, core, first_row):
+def copy_blocks(place, sources, steps, copy):
     z, y, _, x = place
-    column, across, along, corner = source
-    first = core == 0
-    for k in range(4):
-        for j in range(4):
-            y_at = lax.rem(y + jnp.where(first, k, j), NY)
-            x_at = lax.rem(x + jnp.where(first, j, k), NX)
+    for parts, core in sources:
+        first = core == 0
+        for k in range(4):
             for m in range(4):
-                index = lax.rem(z + m, NZ) * (NY * NC) + y_at * NC + core
-                if k == 0 and j == 0:
-                    yield x_at, index, lambda lo, hi: column[m, first_row + lo : first_row + hi, :]
-                elif k == 0:
-                    yield x_at, index, lambda lo, hi: across[j - 1, m, lo:hi, :]
-                elif j == 0:
-                    yield (
-                        x_at,
-                        index,
-                        lambda lo, hi: along[k - 1][m, first_row + lo : first_row + hi, :],
-                    )
-                else:
-                    yield x_at, index, lambda lo, hi: corner[k - 1][j - 1, m, lo:hi, :]
-
-
-def assemble(place, sources, first_row, counts, w_in, w_out, mix_raw=None):
-    for source, core in sources:
-        for x_at, index, take in blocks(place, source, core, first_row):
-            rows = pl.ds(pl.multiple_of(index * 32, 32), 32)
-            for l in range(counts):
-                w_in[l, x_at, rows, :] = take(64 * l, 64 * l + 32)
-                w_out[l, x_at, rows, :] = take(64 * l + 32, 64 * l + 64)
-            if mix_raw is not None:
-                mix_rows = pl.ds(pl.multiple_of(index * 16, 16), 16)
-                mix_raw[x_at, mix_rows, :] = take(64 * counts, 64 * counts + 16)
+                for j in range(4):
+                    step = dict(zip(steps, (k, m, j)))
+                    y_at = lax.rem(y + jnp.where(first, step["v"], step["u"]), NY)
+                    x_at = lax.rem(x + jnp.where(first, step["u"], step["v"]), NX)
+                    index = lax.rem(z + step["z"], NZ) * (NY * NC) + y_at * NC + core
+                    copy(x_at, index, parts[k].at[m, j])
+
+
+def put_layers(layers, w_in, w_out, mix_raw=None):
+    def copy(x_at, index, part):
+        rows = pl.ds(pl.multiple_of(index * 32, 32), 32)
+        for at, l in enumerate(layers):
+            w_in[l, x_at, rows, :] = part[64 * at : 64 * at + 32, :]
+            w_out[l, x_at, rows, :] = part[64 * at + 32 : 64 * at + 64, :]
+        if mix_raw is not None:
+            end = 64 * len(layers)
+            mix_rows = pl.ds(pl.multiple_of(index * 16, 16), 16)
+            mix_raw[x_at, mix_rows, :] = part[end : end + 16, :]
+
+    return copy
 
 
 def windows(start, seqs, span, seq_len):
@@ -141,25 +129,30 @@
     return out.astype(jnp.bfloat16)
 
 
-def split(refs):
-    return refs[0], refs[1], refs[2:5], refs[5:8]
-
-
 def first_half(dims, place_ref, *refs):
     layers, seqs, tok, halo, seq_len = dims
-    own, other, acts, gain = split(refs[0:8]), split(refs[8:16]), refs[16:20], refs[20]
-    state_out, mix_out, scale_out = refs[21:24]
-    w_in, w_out, mix_raw, state_parts, scales = refs[24:]
+    own, other, acts, beside, gain = refs[0:4], refs[4:8], refs[8], refs[9], refs[10]
+    state_out, mix_out, scale_out = refs[11:14]
+    w_in, w_out, mix_raw, state_parts, scales = refs[14:]
     place = tuple(place_ref[k] for k in range(4))
     z, y, c, x = place
     half = layers // 2
-    assemble(place, ((own, c), (other, 1 - c)), 0, half, w_in, w_out, mix_raw)
+    put = put_layers(range(half), w_in, w_out, mix_raw)
+    copy_blocks(place, ((own, c), (other, 1 - c)), "vzu", put)
     span = tok + 2 * halo
-    rows = seqs * span
     for k in range(4):
         x_at = lax.rem(x + k, NX)
-        state_parts[x_at] = acts[k][:rows, :]
-        parts = acts[k][rows : rows + 16, :128].astype(jnp.float32)
+        for h in range(2):
+            lanes = slice(128 * h, 128 * (h + 1))
+            for s in range(seqs):
+                for core in range(NC):
+                    low = ((h * NC + core) * seqs + s) * tok
+                    at = pl.ds(pl.multiple_of(s * span + (1 + core - c) * tok, tok), tok)
+                    state_parts[x_at, at, lanes] = acts[k, low : low + tok, :]
+                low = (h * seqs + s) * tok
+                at = pl.ds(pl.multiple_of(s * span + 2 * c * tok, tok), tok)
+                state_parts[x_at, at, lanes] = beside[k, low : low + tok, :]
+        parts = acts[k, 4 * seqs * tok : 4 * seqs * tok + 16, :].astype(jnp.float32)
         scales[x_at] = parts[0:layers] + parts[layers : 2 * layers] + parts[2 * layers : 3 * layers]
     scale_out[...] = scales[...]
     bands, inverse = windows(((z * NY + y) * NC + c) * tok - halo, seqs, span, seq_len)
@@ -195,12 +188,14 @@
 
 def second_half(dims, place_ref, *refs):
     layers, seqs, tok, halo, seq_len = dims
-    own, other = split(refs[0:8]), split(refs[8:16])
     state_in, mix_in, scales, gain, out, w_in, w_out = refs[16:]
     place = tuple(place_ref[k] for k in range(4))
     z, y, c, x = place
     half = layers // 2
-    assemble(place, ((own, c), (other, 1 - c)), 64 * half + 16, half, w_in, w_out)
+    third = ((refs[0:4], c), (refs[4:8], 1 - c))
+    fourth = ((refs[8:12], c), (refs[12:16], 1 - c))
+    copy_blocks(place, third, "vzu", put_layers((0,), w_in, w_out))
+    copy_blocks(place, fourth, "zvu", put_layers((1,), w_in, w_out))
     span = tok + 2 * halo
     bands, inverse = windows(((z * NY + y) * NC + c) * tok - halo, seqs, span, seq_len)
     state = state_in[...]
@@ -227,11 +222,11 @@
             out[...] = project_out(mixed, lambda g: w_out[l, g, columns, :])
 
 
-def scale_rows(scale, width):
+def scale_rows(scale):
     high = lax.reduce_precision(scale, 8, 7)
     middle = lax.reduce_precision(scale - high, 8, 7)
     terms = jnp.concatenate([high, middle, scale - high - middle]).astype(jnp.bfloat16)
-    return jnp.pad(terms, ((0, 16 - terms.shape[0]), (0, width - terms.shape[1])))
+    return jnp.pad(terms, ((0, 16 - terms.shape[0]), (0, 0)))
 
 
 def body(activations, norm_gain, in_weight, out_weight, mixing, pool_scale):
@@ -241,34 +236,46 @@
     i, x = lax.axis_index("sp"), lax.axis_index("tp")
     z, y, c = i // (NY * NC), (i // NC) % NY, i % NC
     seq_len = tok * NZ * NY * NC
-    cut = 64 * half + 16
-
+    cuts = (64 * half + 16, 64 * half + 80, 64 * half + 144)
+
+    chip_mate = send(activations, from_core())
+    both = jnp.where(
+        c == 0, jnp.stack([activations, chip_mate]), jnp.stack([chip_mate, activations])
+    ).reshape(NC * seqs * tok, width)
     pair = jnp.stack([in_weight, jnp.swapaxes(out_weight, 1, 2)], axis=1)
     pair = pair.reshape(64 * layers, 128)
-    slab = jnp.concatenate(
-        [pair[: 64 * half], mixing.reshape(4 * layers, 128), pair[64 * half :]]
-    )
-    column = jnp.stack([slab] + [send(slab, from_z(k)) for k in (1, 2, 3)])
-    chip_mate = send(activations, from_core())
-    next_chip = send(activations, across_chips())
-    left = jnp.where(c == 0, next_chip, chip_mate)
-    right = jnp.where(c == 0, chip_mate, next_chip)
-    wide = jnp.concatenate([left, activations, right], axis=1)
-    wide = wide.reshape(seqs * 3 * tok, width)
-    wide = jnp.concatenate([wide, scale_rows(pool_scale, width)])
-
-    across = jnp.stack([send(column, from_u(k)) for k in (1, 2, 3)])
-    along = [send(column, from_v(k)) for k in (1, 2, 3)]
-    early, late = across[:, :, :cut, :], across[:, :, cut:, :]
-    corner_early = [send(early, from_v(k)) for k in (1, 2, 3)]
-    acts = [wide] + [send(wide, from_x(k)) for k in (1, 2, 3)]
-    corner_late = [send(late, from_v(k)) for k in (1, 2, 3)]
-    column_2 = send(column, from_core())
-    early_2 = send(early, from_core())
-    along_2 = [send(part, from_core()) for part in along]
-    late_2 = send(late, from_core())
-    corner_early_2 = [send(part, from_core()) for part in corner_early]
-    corner_late_2 = [send(part, from_core()) for part in corner_late]
+    message = jnp.concatenate(
+        [
+            pair[: 64 * half],
+            mixing.reshape(4 * layers, 128),
+            pair[64 * half :],
+            both[:, :128],
+            both[:, 128:],
+            scale_rows(pool_scale),
+        ]
+    )
+    got = [message] + [send(message, from_u(k)) for k in (1, 2, 3)]
+    ab = jnp.stack([part[: cuts[1]] for part in got])
+    q = jnp.stack([part[cuts[1] : cuts[2]] for part in got])
+    tokens = jnp.stack([part[cuts[2] :] for part in got])
+    tokens_2 = send(tokens, from_core())
+    tokens = jnp.where(c == 0, tokens, tokens_2)
+
+    ab = [ab] + [send(ab, from_z(k)) for k in (1, 2, 3)]
+    q = jnp.stack([q] + [send(q, from_v(k)) for k in (1, 2, 3)])
+    mine = tokens[:, : 2 * NC * seqs * tok, :].reshape(4, 2, NC, seqs * tok, 128)
+    mine = jnp.where(c == 0, mine[:, :, 0], mine[:, :, 1]).reshape(4, 2 * seqs * tok, 128)
+    beside = send(mine, across_chips())
+    a = jnp.stack([part[:, : cuts[0]] for part in ab])
+    b = jnp.stack([part[:, cuts[0] :] for part in ab])
+    a = [a] + [send(a, from_v(k)) for k in (1, 2, 3)]
+    q = [q] + [send(q, from_z(k)) for k in (1, 2, 3)]
+    b = [b] + [send(b, from_v(k)) for k in (1, 2, 3)]
+    a_2 = [send(part, from_core()) for part in a]
+    b_2 = [send(b[0], from_core())]
+    q_2 = [send(q[0], from_core())]
+    b_2 += [send(part, from_core()) for part in b[1:]]
+    q_2 += [send(part, from_core()) for part in q[1:]]
 
     place = jnp.stack([z, y, c, x]).astype(jnp.int32)
     vmem = pl.BlockSpec(memory_space=pltpu.VMEM)
@@ -276,7 +283,7 @@
     rows = seqs * 3 * tok
     dims = (layers, seqs, tok, tok, seq_len)
     weights = pltpu.VMEM((half, 4, 1024, 128), jnp.bfloat16)
-    params = pltpu.CompilerParams(vmem_limit_bytes=20 * 2**20)
+    params = pltpu.CompilerParams(vmem_limit_bytes=14 * 2**20)
     cost = pl.CostEstimate(flops=10**9, bytes_accessed=9 * 10**6, transcendentals=1000)
     state, mix_late, scales = pl.pallas_call(
         functools.partial(first_half, dims),
@@ -285,7 +292,7 @@
             jax.ShapeDtypeStruct((layers - half, 128, 512), jnp.bfloat16),
             jax.ShapeDtypeStruct((4, layers, 128), jnp.float32),
         ),
-        in_specs=[smem] + [vmem] * 21,
+        in_specs=[smem] + [vmem] * 11,
         out_specs=(vmem, vmem, vmem),
         scratch_shapes=[
             weights,
@@ -299,15 +306,10 @@
         name="first_half",
     )(
         place,
-        column,
-        early,
-        *along,
-        *corner_early,
-        column_2,
-        early_2,
-        *along_2,
-        *corner_early_2,
-        *acts,
+        *a,
+        *a_2,
+        tokens,
+        beside,
         norm_gain,
     )
     result = pl.pallas_call(
@@ -321,14 +323,10 @@
         name="second_half",
     )(
         place,
-        column,
-        late,
-        *along,
-        *corner_late,
-        column_2,
-        late_2,
-        *along_2,
-        *corner_late_2,
+        *b,
+        *b_2,
+        *q,
+        *q_2,
         state,
         mix_late,
         scales,

time: 107 us -> 90.7 us (0.85)
  the two profiles are of different devices: /device:TPU:0 before, /device:TPU:33 now
where the time goes in v1:
time: 90.7 us; the launch traced here: 90.1 us
  starting transfers between devices  43.6 us (48%)
  waiting for transfers between devices  22 us (24%)
  local copies, waits for them, and re-layouts  12.7 us (14%)
  Pallas kernels  10.2 us (11%)
  other arithmetic  1.2 us (1%)
    ppermute x33, starting transfers between devices, send(): return lax.ppermute(value, AXES, perm)  43.6 us
    ppermute x33, waiting for transfers between devices, send(): return lax.ppermute(value, AXES, perm)  22 us
    unnamed x44, local copies, waits for them, and re-layouts  12.5 us
    pallas_call x1, Pallas kernels, body(): pl.pallas_call(functools.partial(second_half, dims), out_shape=jax.ShapeD...  5.76 us
    pallas_call x1, Pallas kernels, body(): pl.pallas_call(functools.partial(first_half, dims), out_shape=(jax.ShapeD...  4.47 us
  transfers between devices with their start and end apart: 33, of which 10 were waited for; matrix products, arithmetic and copies ran while one was open for 1% of the time, Pallas kernels for 5%

profile of v1, /device:TPU:33, one launch (start us, length us, event | category | flops | bytes accessed | tf_op | source)
XLA Modules:
  0.0 90.1 jit_solution(4639482934174993920)
XLA Ops:
  0.0 0.7 collective-permute-start
  0.7 0.8 fusion.1
  1.5 0.7 copy-done.19
  2.2 0.7 copy-done.18
  2.9 0.7 copy-done.17
  3.7 1.4 %collective-permute-start.3 = (bf16[544,128]{1,0:T(8,128)(2,1)S(1)}, bf16[544,128]{1,0:T(8,128)(2,1)S(1)}, u32[]{:S(2)}, u32[]{:S(2)}) collective-permute-start(bf16[544,128]{1,0:T(8,128)(2,1)S(1)} %get-tuple-element.19), channel_id=1, source_target_pairs={{3,0},{0,1},{1,2},{2,3},{28,4},{29,5},{30,6},{31,7},{11,8},{8,9},{... | collective-permute-start | bytes 417800 | tf_op jit(solution)/shard_map/ppermute | solution.py:54
  5.1 2.7 %collective-permute-start.2 = (bf16[544,128]{1,0:T(8,128)(2,1)S(1)}, bf16[544,128]{1,0:T(8,128)(2,1)S(1)}, u32[]{:S(2)}, u32[]{:S(2)}) collective-permute-start(bf16[544,128]{1,0:T(8,128)(2,1)S(1)} %get-tuple-element.19), channel_id=1, source_target_pairs={{2,0},{3,1},{0,2},{1,3},{20,4},{21,5},{22,6},{23,7},{10,8},{11,9},... | collective-permute-start | bytes 417800 | tf_op jit(solution)/shard_map/ppermute | solution.py:54
  7.8 1.1 %collective-permute-start.1 = (bf16[544,128]{1,0:T(8,128)(2,1)S(1)}, bf16[544,128]{1,0:T(8,128)(2,1)S(1)}, u32[]{:S(2)}, u32[]{:S(2)}) collective-permute-start(bf16[544,128]{1,0:T(8,128)(2,1)S(1)} %get-tuple-element.19), channel_id=1, source_target_pairs={{1,0},{2,1},{3,2},{0,3},{12,4},{13,5},{14,6},{15,7},{9,8},{10,9},{... | collective-permute-start | bytes 417800 | tf_op jit(solution)/shard_map/ppermute | solution.py:54
  9.3 2.7 %collective-permute-done.2 = bf16[544,128]{1,0:T(8,128)(2,1)S(1)} collective-permute-done((bf16[544,128]{1,0:T(8,128)(2,1)S(1)}, bf16[544,128]{1,0:T(8,128)(2,1)S(1)}, u32[]{:S(2)}, u32[]{:S(2)}) %collective-permute-start.2) | collective-permute-done | bytes 139296 | tf_op jit(solution)/shard_map/ppermute | solution.py:54
  12.1 1.7 %collective-permute-start.6 = (bf16[4,208,128]{2,1,0:T(8,128)(2,1)S(1)}, bf16[4,208,128]{2,1,0:T(8,128)(2,1)S(1)}, u32[]{:S(2)}, u32[]{:S(2)}) collective-permute-start(bf16[4,208,128]{2,1,0:T(8,128)(2,1)S(1)} %pad_maximum_fusion.4), channel_id=1, source_target_pairs={{96,0},{97,1},{98,2},{99,3},{100,4},{101,5},{102,6},{103,7},{104,8... | collective-permute-start | bytes 638984 | tf_op jit(solution)/shard_map/ppermute | solution.py:54
  13.8 1.2 %collective-permute-start.5 = (bf16[4,208,128]{2,1,0:T(8,128)(2,1)S(1)}, bf16[4,208,128]{2,1,0:T(8,128)(2,1)S(1)}, u32[]{:S(2)}, u32[]{:S(2)}) collective-permute-start(bf16[4,208,128]{2,1,0:T(8,128)(2,1)S(1)} %pad_maximum_fusion.4), channel_id=1, source_target_pairs={{64,0},{65,1},{66,2},{67,3},{68,4},{69,5},{70,6},{71,7},{72,8},{73... | collective-permute-start | bytes 638984 | tf_op jit(solution)/shard_map/ppermute | solution.py:54
  15.0 2.5 %collective-permute-start.14 = (bf16[4,64,128]{2,1,0:T(8,128)(2,1)S(1)}, bf16[4,64,128]{2,1,0:T(8,128)(2,1)S(1)}, u32[]{:S(2)}, u32[]{:S(2)}) collective-permute-start(bf16[4,64,128]{2,1,0:T(8,128)(2,1)S(1)} %get-tuple-element.15), channel_id=1, source_target_pairs={{8,0},{9,1},{10,2},{11,3},{5,4},{6,5},{7,6},{4,7},{16,8},{17,9},{1... | collective-permute-start | bytes 196616 | tf_op jit(solution)/shard_map/ppermute | solution.py:54
  17.5 0.5 collective-permute-start.15
  18.0 0.6 collective-permute-start.16
  18.9 2.0 %collective-permute-start.4 = (bf16[4,208,128]{2,1,0:T(8,128)(2,1)S(1)}, bf16[4,208,128]{2,1,0:T(8,128)(2,1)S(1)}, u32[]{:S(2)}, u32[]{:S(2)}) collective-permute-start(bf16[4,208,128]{2,1,0:T(8,128)(2,1)S(1)} %pad_maximum_fusion.4), channel_id=1, source_target_pairs={{32,0},{33,1},{34,2},{35,3},{36,4},{37,5},{38,6},{39,7},{40,8},{41... | collective-permute-start | bytes 638984 | tf_op jit(solution)/shard_map/ppermute | solution.py:54
  20.8 1.4 %collective-permute-done.15 = bf16[4,64,128]{2,1,0:T(8,128)(2,1)S(1)} collective-permute-done((bf16[4,64,128]{2,1,0:T(8,128)(2,1)S(1)}, bf16[4,64,128]{2,1,0:T(8,128)(2,1)S(1)}, u32[]{:S(2)}, u32[]{:S(2)}) %collective-permute-start.15) | collective-permute-done | bytes 65568 | tf_op jit(solution)/shard_map/ppermute | solution.py:54
  22.2 3.1 %collective-permute-start.31 = (bf16[4,272,128]{2,1,0:T(8,128)(2,1)S(1)}, bf16[4,272,128]{2,1,0:T(8,128)(2,1)S(1)}, u32[]{:S(2)}, u32[]{:S(2)}) collective-permute-start(bf16[4,272,128]{2,1,0:T(8,128)(2,1)S(1)} %pad_maximum_fusion.1), channel_id=1, source_target_pairs={{4,0},{5,1},{6,2},{7,3},{0,4},{1,5},{2,6},{3,7},{12,8},{13,9},{14,... | collective-permute-start | bytes 835592 | tf_op jit(solution)/shard_map/ppermute | solution.py:54
  25.4 2.3 %collective-permute-start.17 = (bf16[4,4,64,128]{3,2,1,0:T(8,128)(2,1)S(1)}, bf16[4,4,64,128]{3,2,1,0:T(8,128)(2,1)S(1)}, u32[]{:S(2)}, u32[]{:S(2)}) collective-permute-start(bf16[4,4,64,128]{3,2,1,0:T(8,128)(2,1)S(1)} %pad_maximum_fusion.3.refs_8_), channel_id=1, source_target_pairs={{32,0},{33,1},{34,2},{35,3},{36,4},{37,5},{38,6},{39,7},{40,8},{41... | collective-permute-start | bytes 786440 | tf_op jit(solution)/shard_map/ppermute | solution.py:54
  27.7 2.0 %collective-permute-start.19 = (bf16[4,4,64,128]{3,2,1,0:T(8,128)(2,1)S(1)}, bf16[4,4,64,128]{3,2,1,0:T(8,128)(2,1)}, u32[]{:S(2)}, u32[]{:S(2)}) collective-permute-start(bf16[4,4,64,128]{3,2,1,0:T(8,128)(2,1)S(1)} %pad_maximum_fusion.3.refs_8_), channel_id=1, source_target_pairs={{96,0},{97,1},{98,2},{99,3},{100,4},{101,5},{102,6},{103,7},{104,8... | collective-permute-start | bytes 786440 | tf_op jit(solution)/shard_map/ppermute | solution.py:54
  29.7 1.6 %collective-permute-start.20 = (bf16[4,4,64,128]{3,2,1,0:T(8,128)(2,1)S(1)}, bf16[4,4,64,128]{3,2,1,0:T(8,128)(2,1)S(1)}, u32[]{:S(2)}, u32[]{:S(2)}) collective-permute-start(bf16[4,4,64,128]{3,2,1,0:T(8,128)(2,1)S(1)} %pad_maximum_fusion.3.refs_8_), channel_id=1, source_target_pairs={{4,0},{5,1},{6,2},{7,3},{0,4},{1,5},{2,6},{3,7},{12,8},{13,9},{14,... | collective-permute-start | bytes 786440 | tf_op jit(solution)/shard_map/ppermute | solution.py:54
  31.5 2.4 %collective-permute-start.24 = (bf16[4,4,144,128]{3,2,1,0:T(8,128)(2,1)S(1)}, bf16[4,4,144,128]{3,2,1,0:T(8,128)(2,1)S(1)}, u32[]{:S(2)}, u32[]{:S(2)}) collective-permute-start(bf16[4,4,144,128]{3,2,1,0:T(8,128)(2,1)S(1)} %pad_maximum_fusion.refs_0_), channel_id=1, source_target_pairs={{8,0},{9,1},{10,2},{11,3},{5,4},{6,5},{7,6},{4,7},{16,8},{17,9},{1... | collective-permute-start | bytes 1769480 | tf_op jit(solution)/shard_map/ppermute | solution.py:54
  34.0 0.8 collective-permute-start.25
  34.8 4.5 %collective-permute-done.18.refs_10_ = bf16[4,4,64,128]{3,2,1,0:T(8,128)(2,1)} collective-permute-done((bf16[4,4,64,128]{3,2,1,0:T(8,128)(2,1)S(1)}, bf16[4,4,64,128]{3,2,1,0:T(8,128)(2,1)}, u32[]{:S(2)}, u32[]{:S(2)}) %collective-permute-start.18) | collective-permute-done | bytes 262176 | tf_op jit(solution)/shard_map/ppermute | solution.py:54
  39.3 1.2 %collective-permute-start.26 = (bf16[4,4,144,128]{3,2,1,0:T(8,128)(2,1)S(1)}, bf16[4,4,144,128]{3,2,1,0:T(8,128)(2,1)S(1)}, u32[]{:S(2)}, u32[]{:S(2)}) collective-permute-start(bf16[4,4,144,128]{3,2,1,0:T(8,128)(2,1)S(1)} %pad_maximum_fusion.refs_0_), channel_id=1, source_target_pairs={{24,0},{25,1},{26,2},{27,3},{7,4},{4,5},{5,6},{6,7},{0,8},{1,9},{2... | collective-permute-start | bytes 1769480 | tf_op jit(solution)/shard_map/ppermute | solution.py:54
  40.4 2.0 %collective-permute-start.7 = (bf16[4,4,64,128]{3,2,1,0:T(8,128)(2,1)S(1)}, bf16[4,4,64,128]{3,2,1,0:T(8,128)(2,1)}, u32[]{:S(2)}, u32[]{:S(2)}) collective-permute-start(bf16[4,4,64,128]{3,2,1,0:T(8,128)(2,1)S(1)} %pad_maximum_fusion.2.refs_0_), channel_id=1, source_target_pairs={{8,0},{9,1},{10,2},{11,3},{5,4},{6,5},{7,6},{4,7},{16,8},{17,9},{1... | collective-permute-start | bytes 786440 | tf_op jit(solution)/shard_map/ppermute | solution.py:54
  42.4 0.7 copy-done.8
  43.2 2.8 %collective-permute-start.32 = (bf16[4,128,128]{2,1,0:T(8,128)(2,1)S(1)}, bf16[4,128,128]{2,1,0:T(8,128)(2,1)S(1)}, u32[]{:S(2)}, u32[]{:S(2)}) collective-permute-start(bf16[4,128,128]{2,1,0:T(8,128)(2,1)S(1)} %bitcast.68), channel_id=1, source_target_pairs={{4,8},{8,4},{5,9},{9,5},{6,10},{10,6},{7,11},{11,7},{12,16},{16,12... | collective-permute-start | bytes 393224 | tf_op jit(solution)/shard_map/ppermute | solution.py:54
  46.0 5.7 %collective-permute-done.32.refs_9_ = bf16[4,128,128]{2,1,0:T(8,128)(2,1)S(1)} collective-permute-done((bf16[4,128,128]{2,1,0:T(8,128)(2,1)S(1)}, bf16[4,128,128]{2,1,0:T(8,128)(2,1)S(1)}, u32[]{:S(2)}, u32[]{:S(2)}) %collective-permute-start.32) | collective-permute-done | bytes 131104 | tf_op jit(solution)/shard_map/ppermute | solution.py:54
  51.6 2.1 %collective-permute-start.8 = (bf16[4,4,64,128]{3,2,1,0:T(8,128)(2,1)S(1)}, bf16[4,4,64,128]{3,2,1,0:T(8,128)(2,1)}, u32[]{:S(2)}, u32[]{:S(2)}) collective-permute-start(bf16[4,4,64,128]{3,2,1,0:T(8,128)(2,1)S(1)} %pad_maximum_fusion.2.refs_0_), channel_id=1, source_target_pairs={{16,0},{17,1},{18,2},{19,3},{6,4},{7,5},{4,6},{5,7},{24,8},{25,9},... | collective-permute-start | bytes 786440 | tf_op jit(solution)/shard_map/ppermute | solution.py:54
  53.8 0.8 collective-permute-start.9
  54.6 4.0 %collective-permute-done.8.refs_2_ = bf16[4,4,64,128]{3,2,1,0:T(8,128)(2,1)} collective-permute-done((bf16[4,4,64,128]{3,2,1,0:T(8,128)(2,1)S(1)}, bf16[4,4,64,128]{3,2,1,0:T(8,128)(2,1)}, u32[]{:S(2)}, u32[]{:S(2)}) %collective-permute-start.8) | collective-permute-done | bytes 262176 | tf_op jit(solution)/shard_map/ppermute | solution.py:54
  58.6 4.0 %collective-permute-start.27 = (bf16[4,4,144,128]{3,2,1,0:T(8,128)(2,1)S(1)}, bf16[4,4,144,128]{3,2,1,0:T(8,128)(2,1)S(1)}, u32[]{:S(2)}, u32[]{:S(2)}) collective-permute-start(bf16[4,4,144,128]{3,2,1,0:T(8,128)(2,1)S(1)} %pad_maximum_fusion.refs_0_), channel_id=1, source_target_pairs={{4,0},{5,1},{6,2},{7,3},{0,4},{1,5},{2,6},{3,7},{12,8},{13,9},{14,... | collective-permute-start | bytes 1769480 | tf_op jit(solution)/shard_map/ppermute | solution.py:54
  63.1 1.8 %collective-permute-start.10 = (bf16[4,4,64,128]{3,2,1,0:T(8,128)(2,1)S(1)}, bf16[4,4,64,128]{3,2,1,0:T(8,128)(2,1)S(1)}, u32[]{:S(2)}, u32[]{:S(2)}) collective-permute-start(bf16[4,4,64,128]{3,2,1,0:T(8,128)(2,1)S(1)} %pad_maximum_fusion.2.refs_0_), channel_id=1, source_target_pairs={{4,0},{5,1},{6,2},{7,3},{0,4},{1,5},{2,6},{3,7},{12,8},{13,9},{14,... | collective-permute-start | bytes 786440 | tf_op jit(solution)/shard_map/ppermute | solution.py:54
  65.0 2.1 %collective-permute-done.10.refs_4_ = bf16[4,4,64,128]{3,2,1,0:T(8,128)(2,1)S(1)} collective-permute-done((bf16[4,4,64,128]{3,2,1,0:T(8,128)(2,1)S(1)}, bf16[4,4,64,128]{3,2,1,0:T(8,128)(2,1)S(1)}, u32[]{:S(2)}, u32[]{:S(2)}) %collective-permute-start.10) | collective-permute-done | bytes 262176 | tf_op jit(solution)/shard_map/ppermute | solution.py:54
  67.1 0.7 copy-done.10
  68.1 1.2 %collective-permute-done.21.refs_13_ = bf16[4,4,64,128]{3,2,1,0:T(8,128)(2,1)S(1)} collective-permute-done((bf16[4,4,64,128]{3,2,1,0:T(8,128)(2,1)S(1)}, bf16[4,4,64,128]{3,2,1,0:T(8,128)(2,1)S(1)}, u32[]{:S(2)}, u32[]{:S(2)}) %collective-permute-start.21) | collective-permute-done | bytes 262176 | tf_op jit(solution)/shard_map/ppermute | solution.py:54
  69.3 0.7 copy-done.12
  70.4 0.8 copy-done
  71.4 0.8 copy-done.2
  72.6 0.8 copy-done.4
  73.5 0.8 copy-done.6
  74.8 1.1 %copy-done.1 = bf16[4,4,144,128]{3,2,1,0:T(8,128)(2,1)S(1)} copy-done((bf16[4,4,144,128]{3,2,1,0:T(8,128)(2,1)S(1)}, bf16[4,4,144,128]{3,2,1,0:T(8,128)(2,1)}, u32[]{:S(2)}) %copy-start.1) | copy-done | bytes 589848
  75.9 1.1 %copy-done.3 = bf16[4,4,144,128]{3,2,1,0:T(8,128)(2,1)S(1)} copy-done((bf16[4,4,144,128]{3,2,1,0:T(8,128)(2,1)S(1)}, bf16[4,4,144,128]{3,2,1,0:T(8,128)(2,1)}, u32[]{:S(2)}) %copy-start.3) | copy-done | bytes 589848
  76.9 1.1 %copy-done.5 = bf16[4,4,144,128]{3,2,1,0:T(8,128)(2,1)S(1)} copy-done((bf16[4,4,144,128]{3,2,1,0:T(8,128)(2,1)S(1)}, bf16[4,4,144,128]{3,2,1,0:T(8,128)(2,1)}, u32[]{:S(2)}) %copy-start.5) | copy-done | bytes 589848
  78.0 1.1 %copy-done.7 = bf16[4,4,144,128]{3,2,1,0:T(8,128)(2,1)S(1)} copy-done((bf16[4,4,144,128]{3,2,1,0:T(8,128)(2,1)S(1)}, bf16[4,4,144,128]{3,2,1,0:T(8,128)(2,1)}, u32[]{:S(2)}) %copy-start.7) | copy-done | bytes 589848
  79.1 0.7 copy-done.14
  79.8 4.5 %first_half.1 = (bf16[192,1024]{1,0:T(8,128)(2,1)S(1)}, bf16[2,128,512]{2,1,0:T(8,128)(2,1)S(1)}, f32[4,4,128]{2,1,0:T(4,128)S(1)}) custom-call(s32[4]{0:T(128)S(1)} %pad_add_fusion.place_ref, bf16[4,4,144,128]{3,2,1,0:T(8,128)(2,1)S(1)} %pad_maximum_fusion.refs_0_, bf16[4,4,144,128]{3,2,1,0:T(8,128)(2,1)S(1)} %collective-permute-done.24.refs_1_, ...), custom_call_target="tpu_custom_call" | custom-call | flops 1000000000 | bytes 9000000 | tf_op jit(solution)/shard_map/first_half/pallas_call | solution.py:288
  84.3 5.8 %second_half.1 = bf16[64,256]{1,0:T(8,128)(2,1)} custom-call(s32[4]{0:T(128)S(1)} %pad_add_fusion.place_ref, bf16[4,4,64,128]{3,2,1,0:T(8,128)(2,1)S(1)} %pad_maximum_fusion.2.refs_0_, bf16[4,4,64,128]{3,2,1,0:T(8,128)(2,1)} %collective-permute-done.7.refs_1_, bf16[4,4,64,128]{3,2,1,0:T(8,128)(2,1)} %collective-permute-done.8.refs_2_, ...), custom_call_target="tpu_custom_call" | custom-call | flops 1000000000 | bytes 9000000 | tf_op jit(solution)/shard_map/second_half/pallas_call | solution.py:315
  (101 shorter events, 3.7 us)
Async XLA Ops:
  0.0 2.9 %collective-permute-start = (bf16[2,32,256]{2,1,0:T(8,128)(2,1)}, bf16[2,32,256]{2,1,0:T(8,128)(2,1)S(1)}, u32[]{:S(2)}, u32[]{:S(2)}) collective-permute-start(bf16[2,32,256]{2,1,0:T(8,128)(2,1)} %param.6), channel_id=1, source_target_pairs={{4,0},{5,1},{6,2},{7,3},{0,4},{1,5},{2,6},{3,7},{12,8},{13,9},{14,... | collective-permute-start | bytes 98312 | tf_op jit(solution)/shard_map/ppermute | solution.py:54
  2.9 0.8 copy-start.17
  3.7 1.4 %copy-start.15 = (bf16[4,32,128]{2,1,0:T(8,128)(2,1)S(1)}, bf16[4,32,128]{2,1,0:T(8,128)(2,1)}, u32[]{:S(2)}) copy-start(bf16[4,32,128]{2,1,0:T(8,128)(2,1)} %param.8) | copy-start | bytes 98308
  3.7 1.4 %copy-start.16 = (bf16[4,128,32]{1,2,0:T(8,128)(2,1)S(1)}, bf16[4,128,32]{1,2,0:T(8,128)(2,1)}, u32[]{:S(2)}) copy-start(bf16[4,128,32]{1,2,0:T(8,128)(2,1)} %param.9) | copy-start | bytes 98308
  3.7 5.5 %collective-permute-start.3 = (bf16[544,128]{1,0:T(8,128)(2,1)S(1)}, bf16[544,128]{1,0:T(8,128)(2,1)S(1)}, u32[]{:S(2)}, u32[]{:S(2)}) collective-permute-start(bf16[544,128]{1,0:T(8,128)(2,1)S(1)} %get-tuple-element.19), channel_id=1, source_target_pairs={{3,0},{0,1},{1,2},{2,3},{28,4},{29,5},{30,6},{31,7},{11,8},{8,9},{... | collective-permute-start | bytes 417800 | tf_op jit(solution)/shard_map/ppermute | solution.py:54
  5.1 6.8 %collective-permute-start.2 = (bf16[544,128]{1,0:T(8,128)(2,1)S(1)}, bf16[544,128]{1,0:T(8,128)(2,1)S(1)}, u32[]{:S(2)}, u32[]{:S(2)}) collective-permute-start(bf16[544,128]{1,0:T(8,128)(2,1)S(1)} %get-tuple-element.19), channel_id=1, source_target_pairs={{2,0},{3,1},{0,2},{1,3},{20,4},{21,5},{22,6},{23,7},{10,8},{11,9},... | collective-permute-start | bytes 417800 | tf_op jit(solution)/shard_map/ppermute | solution.py:54
  7.8 4.2 %collective-permute-start.1 = (bf16[544,128]{1,0:T(8,128)(2,1)S(1)}, bf16[544,128]{1,0:T(8,128)(2,1)S(1)}, u32[]{:S(2)}, u32[]{:S(2)}) collective-permute-start(bf16[544,128]{1,0:T(8,128)(2,1)S(1)} %get-tuple-element.19), channel_id=1, source_target_pairs={{1,0},{2,1},{3,2},{0,3},{12,4},{13,5},{14,6},{15,7},{9,8},{10,9},{... | collective-permute-start | bytes 417800 | tf_op jit(solution)/shard_map/ppermute | solution.py:54
  12.1 15.6 %collective-permute-start.6 = (bf16[4,208,128]{2,1,0:T(8,128)(2,1)S(1)}, bf16[4,208,128]{2,1,0:T(8,128)(2,1)S(1)}, u32[]{:S(2)}, u32[]{:S(2)}) collective-permute-start(bf16[4,208,128]{2,1,0:T(8,128)(2,1)S(1)} %pad_maximum_fusion.4), channel_id=1, source_target_pairs={{96,0},{97,1},{98,2},{99,3},{100,4},{101,5},{102,6},{103,7},{104,8... | collective-permute-start | bytes 638984 | tf_op jit(solution)/shard_map/ppermute | solution.py:54
  13.8 14.0 %collective-permute-start.5 = (bf16[4,208,128]{2,1,0:T(8,128)(2,1)S(1)}, bf16[4,208,128]{2,1,0:T(8,128)(2,1)S(1)}, u32[]{:S(2)}, u32[]{:S(2)}) collective-permute-start(bf16[4,208,128]{2,1,0:T(8,128)(2,1)S(1)} %pad_maximum_fusion.4), channel_id=1, source_target_pairs={{64,0},{65,1},{66,2},{67,3},{68,4},{69,5},{70,6},{71,7},{72,8},{73... | collective-permute-start | bytes 638984 | tf_op jit(solution)/shard_map/ppermute | solution.py:54
  15.0 3.9 %collective-permute-start.14 = (bf16[4,64,128]{2,1,0:T(8,128)(2,1)S(1)}, bf16[4,64,128]{2,1,0:T(8,128)(2,1)S(1)}, u32[]{:S(2)}, u32[]{:S(2)}) collective-permute-start(bf16[4,64,128]{2,1,0:T(8,128)(2,1)S(1)} %get-tuple-element.15), channel_id=1, source_target_pairs={{8,0},{9,1},{10,2},{11,3},{5,4},{6,5},{7,6},{4,7},{16,8},{17,9},{1... | collective-permute-start | bytes 196616 | tf_op jit(solution)/shard_map/ppermute | solution.py:54
  17.5 4.7 %collective-permute-start.15 = (bf16[4,64,128]{2,1,0:T(8,128)(2,1)S(1)}, bf16[4,64,128]{2,1,0:T(8,128)(2,1)S(1)}, u32[]{:S(2)}, u32[]{:S(2)}) collective-permute-start(bf16[4,64,128]{2,1,0:T(8,128)(2,1)S(1)} %get-tuple-element.15), channel_id=1, source_target_pairs={{16,0},{17,1},{18,2},{19,3},{6,4},{7,5},{4,6},{5,7},{24,8},{25,9},... | collective-permute-start | bytes 196616 | tf_op jit(solution)/shard_map/ppermute | solution.py:54
  18.0 7.3 %collective-permute-start.16 = (bf16[4,64,128]{2,1,0:T(8,128)(2,1)S(1)}, bf16[4,64,128]{2,1,0:T(8,128)(2,1)S(1)}, u32[]{:S(2)}, u32[]{:S(2)}) collective-permute-start(bf16[4,64,128]{2,1,0:T(8,128)(2,1)S(1)} %get-tuple-element.15), channel_id=1, source_target_pairs={{24,0},{25,1},{26,2},{27,3},{7,4},{4,5},{5,6},{6,7},{0,8},{1,9},{2... | collective-permute-start | bytes 196616 | tf_op jit(solution)/shard_map/ppermute | solution.py:54
  18.9 10.9 %collective-permute-start.4 = (bf16[4,208,128]{2,1,0:T(8,128)(2,1)S(1)}, bf16[4,208,128]{2,1,0:T(8,128)(2,1)S(1)}, u32[]{:S(2)}, u32[]{:S(2)}) collective-permute-start(bf16[4,208,128]{2,1,0:T(8,128)(2,1)S(1)} %pad_maximum_fusion.4), channel_id=1, source_target_pairs={{32,0},{33,1},{34,2},{35,3},{36,4},{37,5},{38,6},{39,7},{40,8},{41... | collective-permute-start | bytes 638984 | tf_op jit(solution)/shard_map/ppermute | solution.py:54
  22.2 9.3 %collective-permute-start.31 = (bf16[4,272,128]{2,1,0:T(8,128)(2,1)S(1)}, bf16[4,272,128]{2,1,0:T(8,128)(2,1)S(1)}, u32[]{:S(2)}, u32[]{:S(2)}) collective-permute-start(bf16[4,272,128]{2,1,0:T(8,128)(2,1)S(1)} %pad_maximum_fusion.1), channel_id=1, source_target_pairs={{4,0},{5,1},{6,2},{7,3},{0,4},{1,5},{2,6},{3,7},{12,8},{13,9},{14,... | collective-permute-start | bytes 835592 | tf_op jit(solution)/shard_map/ppermute | solution.py:54
  25.4 8.7 %collective-permute-start.17 = (bf16[4,4,64,128]{3,2,1,0:T(8,128)(2,1)S(1)}, bf16[4,4,64,128]{3,2,1,0:T(8,128)(2,1)S(1)}, u32[]{:S(2)}, u32[]{:S(2)}) collective-permute-start(bf16[4,4,64,128]{3,2,1,0:T(8,128)(2,1)S(1)} %pad_maximum_fusion.3.refs_8_), channel_id=1, source_target_pairs={{32,0},{33,1},{34,2},{35,3},{36,4},{37,5},{38,6},{39,7},{40,8},{41... | collective-permute-start | bytes 786440 | tf_op jit(solution)/shard_map/ppermute | solution.py:54
  27.7 11.6 %collective-permute-start.18 = (bf16[4,4,64,128]{3,2,1,0:T(8,128)(2,1)S(1)}, bf16[4,4,64,128]{3,2,1,0:T(8,128)(2,1)}, u32[]{:S(2)}, u32[]{:S(2)}) collective-permute-start(bf16[4,4,64,128]{3,2,1,0:T(8,128)(2,1)S(1)} %pad_maximum_fusion.3.refs_8_), channel_id=1, source_target_pairs={{64,0},{65,1},{66,2},{67,3},{68,4},{69,5},{70,6},{71,7},{72,8},{73... | collective-permute-start | bytes 786440 | tf_op jit(solution)/shard_map/ppermute | solution.py:54
  27.7 12.7 %collective-permute-start.19 = (bf16[4,4,64,128]{3,2,1,0:T(8,128)(2,1)S(1)}, bf16[4,4,64,128]{3,2,1,0:T(8,128)(2,1)}, u32[]{:S(2)}, u32[]{:S(2)}) collective-permute-start(bf16[4,4,64,128]{3,2,1,0:T(8,128)(2,1)S(1)} %pad_maximum_fusion.3.refs_8_), channel_id=1, source_target_pairs={{96,0},{97,1},{98,2},{99,3},{100,4},{101,5},{102,6},{103,7},{104,8... | collective-permute-start | bytes 786440 | tf_op jit(solution)/shard_map/ppermute | solution.py:54
  29.7 12.7 %collective-permute-start.20 = (bf16[4,4,64,128]{3,2,1,0:T(8,128)(2,1)S(1)}, bf16[4,4,64,128]{3,2,1,0:T(8,128)(2,1)S(1)}, u32[]{:S(2)}, u32[]{:S(2)}) collective-permute-start(bf16[4,4,64,128]{3,2,1,0:T(8,128)(2,1)S(1)} %pad_maximum_fusion.3.refs_8_), channel_id=1, source_target_pairs={{4,0},{5,1},{6,2},{7,3},{0,4},{1,5},{2,6},{3,7},{12,8},{13,9},{14,... | collective-permute-start | bytes 786440 | tf_op jit(solution)/shard_map/ppermute | solution.py:54
  31.5 31.0 %collective-permute-start.24 = (bf16[4,4,144,128]{3,2,1,0:T(8,128)(2,1)S(1)}, bf16[4,4,144,128]{3,2,1,0:T(8,128)(2,1)S(1)}, u32[]{:S(2)}, u32[]{:S(2)}) collective-permute-start(bf16[4,4,144,128]{3,2,1,0:T(8,128)(2,1)S(1)} %pad_maximum_fusion.refs_0_), channel_id=1, source_target_pairs={{8,0},{9,1},{10,2},{11,3},{5,4},{6,5},{7,6},{4,7},{16,8},{17,9},{1... | collective-permute-start | bytes 1769480 | tf_op jit(solution)/shard_map/ppermute | solution.py:54
  34.0 28.5 %collective-permute-start.25 = (bf16[4,4,144,128]{3,2,1,0:T(8,128)(2,1)S(1)}, bf16[4,4,144,128]{3,2,1,0:T(8,128)(2,1)S(1)}, u32[]{:S(2)}, u32[]{:S(2)}) collective-permute-start(bf16[4,4,144,128]{3,2,1,0:T(8,128)(2,1)S(1)} %pad_maximum_fusion.refs_0_), channel_id=1, source_target_pairs={{16,0},{17,1},{18,2},{19,3},{6,4},{7,5},{4,6},{5,7},{24,8},{25,9},... | collective-permute-start | bytes 1769480 | tf_op jit(solution)/shard_map/ppermute | solution.py:54
  39.3 23.8 %collective-permute-start.26 = (bf16[4,4,144,128]{3,2,1,0:T(8,128)(2,1)S(1)}, bf16[4,4,144,128]{3,2,1,0:T(8,128)(2,1)S(1)}, u32[]{:S(2)}, u32[]{:S(2)}) collective-permute-start(bf16[4,4,144,128]{3,2,1,0:T(8,128)(2,1)S(1)} %pad_maximum_fusion.refs_0_), channel_id=1, source_target_pairs={{24,0},{25,1},{26,2},{27,3},{7,4},{4,5},{5,6},{6,7},{0,8},{1,9},{2... | collective-permute-start | bytes 1769480 | tf_op jit(solution)/shard_map/ppermute | solution.py:54
  40.4 13.3 %collective-permute-start.7 = (bf16[4,4,64,128]{3,2,1,0:T(8,128)(2,1)S(1)}, bf16[4,4,64,128]{3,2,1,0:T(8,128)(2,1)}, u32[]{:S(2)}, u32[]{:S(2)}) collective-permute-start(bf16[4,4,64,128]{3,2,1,0:T(8,128)(2,1)S(1)} %pad_maximum_fusion.2.refs_0_), channel_id=1, source_target_pairs={{8,0},{9,1},{10,2},{11,3},{5,4},{6,5},{7,6},{4,7},{16,8},{17,9},{1... | collective-permute-start | bytes 786440 | tf_op jit(solution)/shard_map/ppermute | solution.py:54
  43.2 8.5 %collective-permute-start.32 = (bf16[4,128,128]{2,1,0:T(8,128)(2,1)S(1)}, bf16[4,128,128]{2,1,0:T(8,128)(2,1)S(1)}, u32[]{:S(2)}, u32[]{:S(2)}) collective-permute-start(bf16[4,128,128]{2,1,0:T(8,128)(2,1)S(1)} %bitcast.68), channel_id=1, source_target_pairs={{4,8},{8,4},{5,9},{9,5},{6,10},{10,6},{7,11},{11,7},{12,16},{16,12... | collective-permute-start | bytes 393224 | tf_op jit(solution)/shard_map/ppermute | solution.py:54
  51.6 6.9 %collective-permute-start.8 = (bf16[4,4,64,128]{3,2,1,0:T(8,128)(2,1)S(1)}, bf16[4,4,64,128]{3,2,1,0:T(8,128)(2,1)}, u32[]{:S(2)}, u32[]{:S(2)}) collective-permute-start(bf16[4,4,64,128]{3,2,1,0:T(8,128)(2,1)S(1)} %pad_maximum_fusion.2.refs_0_), channel_id=1, source_target_pairs={{16,0},{17,1},{18,2},{19,3},{6,4},{7,5},{4,6},{5,7},{24,8},{25,9},... | collective-permute-start | bytes 786440 | tf_op jit(solution)/shard_map/ppermute | solution.py:54
  53.8 9.4 %collective-permute-start.9 = (bf16[4,4,64,128]{3,2,1,0:T(8,128)(2,1)S(1)}, bf16[4,4,64,128]{3,2,1,0:T(8,128)(2,1)}, u32[]{:S(2)}, u32[]{:S(2)}) collective-permute-start(bf16[4,4,64,128]{3,2,1,0:T(8,128)(2,1)S(1)} %pad_maximum_fusion.2.refs_0_), channel_id=1, source_target_pairs={{24,0},{25,1},{26,2},{27,3},{7,4},{4,5},{5,6},{6,7},{0,8},{1,9},{2... | collective-permute-start | bytes 786440 | tf_op jit(solution)/shard_map/ppermute | solution.py:54
  58.6 11.8 %collective-permute-start.27 = (bf16[4,4,144,128]{3,2,1,0:T(8,128)(2,1)S(1)}, bf16[4,4,144,128]{3,2,1,0:T(8,128)(2,1)S(1)}, u32[]{:S(2)}, u32[]{:S(2)}) collective-permute-start(bf16[4,4,144,128]{3,2,1,0:T(8,128)(2,1)S(1)} %pad_maximum_fusion.refs_0_), channel_id=1, source_target_pairs={{4,0},{5,1},{6,2},{7,3},{0,4},{1,5},{2,6},{3,7},{12,8},{13,9},{14,... | collective-permute-start | bytes 1769480 | tf_op jit(solution)/shard_map/ppermute | solution.py:54
  62.5 8.8 %collective-permute-start.28 = (bf16[4,4,144,128]{3,2,1,0:T(8,128)(2,1)S(1)}, bf16[4,4,144,128]{3,2,1,0:T(8,128)(2,1)S(1)}, u32[]{:S(2)}, u32[]{:S(2)}) collective-permute-start(bf16[4,4,144,128]{3,2,1,0:T(8,128)(2,1)S(1)} %collective-permute-done.24.refs_1_), channel_id=1, source_target_pairs={{4,0},{5,1},{6,2},{7,3},{0,4},{1,5},{2,6},{3,7},{12,8},{13,9},{14,... | collective-permute-start | bytes 1769480 | tf_op jit(solution)/shard_map/ppermute | solution.py:54
  62.6 10.0 %collective-permute-start.29 = (bf16[4,4,144,128]{3,2,1,0:T(8,128)(2,1)S(1)}, bf16[4,4,144,128]{3,2,1,0:T(8,128)(2,1)S(1)}, u32[]{:S(2)}, u32[]{:S(2)}) collective-permute-start(bf16[4,4,144,128]{3,2,1,0:T(8,128)(2,1)S(1)} %collective-permute-done.25.refs_2_), channel_id=1, source_target_pairs={{4,0},{5,1},{6,2},{7,3},{0,4},{1,5},{2,6},{3,7},{12,8},{13,9},{14,... | collective-permute-start | bytes 1769480 | tf_op jit(solution)/shard_map/ppermute | solution.py:54
  63.1 10.5 %collective-permute-start.30 = (bf16[4,4,144,128]{3,2,1,0:T(8,128)(2,1)S(1)}, bf16[4,4,144,128]{3,2,1,0:T(8,128)(2,1)S(1)}, u32[]{:S(2)}, u32[]{:S(2)}) collective-permute-start(bf16[4,4,144,128]{3,2,1,0:T(8,128)(2,1)S(1)} %collective-permute-done.26.refs_3_), channel_id=1, source_target_pairs={{4,0},{5,1},{6,2},{7,3},{0,4},{1,5},{2,6},{3,7},{12,8},{13,9},{14,... | collective-permute-start | bytes 1769480 | tf_op jit(solution)/shard_map/ppermute | solution.py:54
  63.1 3.9 %collective-permute-start.10 = (bf16[4,4,64,128]{3,2,1,0:T(8,128)(2,1)S(1)}, bf16[4,4,64,128]{3,2,1,0:T(8,128)(2,1)S(1)}, u32[]{:S(2)}, u32[]{:S(2)}) collective-permute-start(bf16[4,4,64,128]{3,2,1,0:T(8,128)(2,1)S(1)} %pad_maximum_fusion.2.refs_0_), channel_id=1, source_target_pairs={{4,0},{5,1},{6,2},{7,3},{0,4},{1,5},{2,6},{3,7},{12,8},{13,9},{14,... | collective-permute-start | bytes 786440 | tf_op jit(solution)/shard_map/ppermute | solution.py:54
  67.8 1.5 %collective-permute-start.21 = (bf16[4,4,64,128]{3,2,1,0:T(8,128)(2,1)S(1)}, bf16[4,4,64,128]{3,2,1,0:T(8,128)(2,1)S(1)}, u32[]{:S(2)}, u32[]{:S(2)}) collective-permute-start(bf16[4,4,64,128]{3,2,1,0:T(8,128)(2,1)S(1)} %collective-permute-done.17.refs_9_), channel_id=1, source_target_pairs={{4,0},{5,1},{6,2},{7,3},{0,4},{1,5},{2,6},{3,7},{12,8},{13,9},{14,... | collective-permute-start | bytes 786440 | tf_op jit(solution)/shard_map/ppermute | solution.py:54
  70.0 14.3 %collective-permute-start.22 = (bf16[4,4,64,128]{3,2,1,0:T(8,128)(2,1)}, bf16[4,4,64,128]{3,2,1,0:T(8,128)(2,1)}, u32[]{:S(2)}, u32[]{:S(2)}) collective-permute-start(bf16[4,4,64,128]{3,2,1,0:T(8,128)(2,1)} %collective-permute-done.18.refs_10_), channel_id=1, source_target_pairs={{4,0},{5,1},{6,2},{7,3},{0,4},{1,5},{2,6},{3,7},{12,8},{13,9},{14,... | collective-permute-start | bytes 786440 | tf_op jit(solution)/shard_map/ppermute | solution.py:54
  70.4 0.8 copy-start
  71.2 13.0 %collective-permute-start.23 = (bf16[4,4,64,128]{3,2,1,0:T(8,128)(2,1)}, bf16[4,4,64,128]{3,2,1,0:T(8,128)(2,1)}, u32[]{:S(2)}, u32[]{:S(2)}) collective-permute-start(bf16[4,4,64,128]{3,2,1,0:T(8,128)(2,1)} %collective-permute-done.19.refs_11_), channel_id=1, source_target_pairs={{4,0},{5,1},{6,2},{7,3},{0,4},{1,5},{2,6},{3,7},{12,8},{13,9},{14,... | collective-permute-start | bytes 786440 | tf_op jit(solution)/shard_map/ppermute | solution.py:54
  71.4 0.8 copy-start.2
  72.2 12.1 %collective-permute-start.11 = (bf16[4,4,64,128]{3,2,1,0:T(8,128)(2,1)}, bf16[4,4,64,128]{3,2,1,0:T(8,128)(2,1)}, u32[]{:S(2)}, u32[]{:S(2)}) collective-permute-start(bf16[4,4,64,128]{3,2,1,0:T(8,128)(2,1)} %collective-permute-done.7.refs_1_), channel_id=1, source_target_pairs={{4,0},{5,1},{6,2},{7,3},{0,4},{1,5},{2,6},{3,7},{12,8},{13,9},{14,... | collective-permute-start | bytes 786440 | tf_op jit(solution)/shard_map/ppermute | solution.py:54
  72.6 0.8 copy-start.4
  73.4 10.9 %collective-permute-start.12 = (bf16[4,4,64,128]{3,2,1,0:T(8,128)(2,1)}, bf16[4,4,64,128]{3,2,1,0:T(8,128)(2,1)}, u32[]{:S(2)}, u32[]{:S(2)}) collective-permute-start(bf16[4,4,64,128]{3,2,1,0:T(8,128)(2,1)} %collective-permute-done.8.refs_2_), channel_id=1, source_target_pairs={{4,0},{5,1},{6,2},{7,3},{0,4},{1,5},{2,6},{3,7},{12,8},{13,9},{14,... | collective-permute-start | bytes 786440 | tf_op jit(solution)/shard_map/ppermute | solution.py:54
  73.5 0.8 copy-start.6
  74.4 10.0 %collective-permute-start.13 = (bf16[4,4,64,128]{3,2,1,0:T(8,128)(2,1)}, bf16[4,4,64,128]{3,2,1,0:T(8,128)(2,1)}, u32[]{:S(2)}, u32[]{:S(2)}) collective-permute-start(bf16[4,4,64,128]{3,2,1,0:T(8,128)(2,1)} %collective-permute-done.9.refs_3_), channel_id=1, source_target_pairs={{4,0},{5,1},{6,2},{7,3},{0,4},{1,5},{2,6},{3,7},{12,8},{13,9},{14,... | collective-permute-start | bytes 786440 | tf_op jit(solution)/shard_map/ppermute | solution.py:54
  74.8 1.1 %copy-start.1 = (bf16[4,4,144,128]{3,2,1,0:T(8,128)(2,1)S(1)}, bf16[4,4,144,128]{3,2,1,0:T(8,128)(2,1)}, u32[]{:S(2)}) copy-start(bf16[4,4,144,128]{3,2,1,0:T(8,128)(2,1)} %copy-done) | copy-start | bytes 1769476
  75.9 1.1 %copy-start.3 = (bf16[4,4,144,128]{3,2,1,0:T(8,128)(2,1)S(1)}, bf16[4,4,144,128]{3,2,1,0:T(8,128)(2,1)}, u32[]{:S(2)}) copy-start(bf16[4,4,144,128]{3,2,1,0:T(8,128)(2,1)} %copy-done.2) | copy-start | bytes 1769476
  76.9 1.1 %copy-start.5 = (bf16[4,4,144,128]{3,2,1,0:T(8,128)(2,1)S(1)}, bf16[4,4,144,128]{3,2,1,0:T(8,128)(2,1)}, u32[]{:S(2)}) copy-start(bf16[4,4,144,128]{3,2,1,0:T(8,128)(2,1)} %copy-done.4) | copy-start | bytes 1769476
  78.0 1.1 %copy-start.7 = (bf16[4,4,144,128]{3,2,1,0:T(8,128)(2,1)S(1)}, bf16[4,4,144,128]{3,2,1,0:T(8,128)(2,1)}, u32[]{:S(2)}) copy-start(bf16[4,4,144,128]{3,2,1,0:T(8,128)(2,1)} %copy-done.6) | copy-start | bytes 1769476
  79.1 0.7 copy-start.14
  79.8 4.5 %copy-start.9 = (bf16[4,4,64,128]{3,2,1,0:T(8,128)(2,1)S(1)}, bf16[4,4,64,128]{3,2,1,0:T(8,128)(2,1)}, u32[]{:S(2)}) copy-start(bf16[4,4,64,128]{3,2,1,0:T(8,128)(2,1)} %copy-done.8) | copy-start | bytes 786436
  79.8 4.5 %copy-start.11 = (bf16[4,4,64,128]{3,2,1,0:T(8,128)(2,1)S(1)}, bf16[4,4,64,128]{3,2,1,0:T(8,128)(2,1)}, u32[]{:S(2)}) copy-start(bf16[4,4,64,128]{3,2,1,0:T(8,128)(2,1)} %copy-done.10) | copy-start | bytes 786436
  79.8 4.6 %copy-start.13 = (bf16[4,4,64,128]{3,2,1,0:T(8,128)(2,1)S(1)}, bf16[4,4,64,128]{3,2,1,0:T(8,128)(2,1)}, u32[]{:S(2)}) copy-start(bf16[4,4,64,128]{3,2,1,0:T(8,128)(2,1)} %copy-done.12) | copy-start | bytes 786436
  (5 other events, 3.5 us)

commit v2 on v1

--- a/solution.py
+++ b/solution.py
@@ -146,13 +146,13 @@
             lanes = slice(128 * h, 128 * (h + 1))
             for s in range(seqs):
                 for core in range(NC):
-                    low = ((h * NC + core) * seqs + s) * tok
+                    low = 16 + ((core * 2 + h) * seqs + s) * tok
                     at = pl.ds(pl.multiple_of(s * span + (1 + core - c) * tok, tok), tok)
                     state_parts[x_at, at, lanes] = acts[k, low : low + tok, :]
                 low = (h * seqs + s) * tok
                 at = pl.ds(pl.multiple_of(s * span + 2 * c * tok, tok), tok)
                 state_parts[x_at, at, lanes] = beside[k, low : low + tok, :]
-        parts = acts[k, 4 * seqs * tok : 4 * seqs * tok + 16, :].astype(jnp.float32)
+        parts = acts[k, 0:16, :].astype(jnp.float32)
         scales[x_at] = parts[0:layers] + parts[layers : 2 * layers] + parts[2 * layers : 3 * layers]
     scale_out[...] = scales[...]
     bands, inverse = windows(((z * NY + y) * NC + c) * tok - halo, seqs, span, seq_len)
@@ -222,11 +222,30 @@
             out[...] = project_out(mixed, lambda g: w_out[l, g, columns, :])
 
 
-def scale_rows(scale):
-    high = lax.reduce_precision(scale, 8, 7)
-    middle = lax.reduce_precision(scale - high, 8, 7)
-    terms = jnp.concatenate([high, middle, scale - high - middle]).astype(jnp.bfloat16)
-    return jnp.pad(terms, ((0, 16 - terms.shape[0]), (0, 0)))
+def pack(layers, place_ref, in_ref, out_ref, mix_ref, scale_ref, act_ref, gain_ref, message, gain):
+    half = layers // 2
+    row = 0
+    for l in range(layers):
+        message[row : row + 32, :] = in_ref[l]
+        message[row + 32 : row + 64, :] = out_ref[l]
+        row += 64
+        if l == half - 1:
+            mix = jnp.concatenate([mix_ref[k].astype(jnp.float32) for k in range(layers)])
+            message[row : row + 16, :] = mix.astype(jnp.bfloat16)
+            row += 16
+    scale = scale_ref[...]
+    high = scale.astype(jnp.bfloat16).astype(jnp.float32)
+    middle = (scale - high).astype(jnp.bfloat16).astype(jnp.float32)
+    terms = jnp.concatenate([high, middle, scale - high - middle, jnp.zeros_like(scale)])
+    message[row : row + 16, :] = terms.astype(jnp.bfloat16)
+    row += 16
+    seqs, tok, _ = act_ref.shape
+    own = row + place_ref[2] * (seqs * tok * 2)
+    for h in range(2):
+        for s in range(seqs):
+            at = pl.ds(pl.multiple_of(own + (h * seqs + s) * tok, 16), tok)
+            message[at, :] = act_ref[s, :, 128 * h : 128 * (h + 1)]
+    gain[...] = gain_ref[...]
 
 
 def body(activations, norm_gain, in_weight, out_weight, mixing, pool_scale):
@@ -239,21 +258,34 @@
     cuts = (64 * half + 16, 64 * half + 80, 64 * half + 144)
 
     chip_mate = send(activations, from_core())
-    both = jnp.where(
-        c == 0, jnp.stack([activations, chip_mate]), jnp.stack([chip_mate, activations])
-    ).reshape(NC * seqs * tok, width)
-    pair = jnp.stack([in_weight, jnp.swapaxes(out_weight, 1, 2)], axis=1)
-    pair = pair.reshape(64 * layers, 128)
-    message = jnp.concatenate(
-        [
-            pair[: 64 * half],
-            mixing.reshape(4 * layers, 128),
-            pair[64 * half :],
-            both[:, :128],
-            both[:, 128:],
-            scale_rows(pool_scale),
-        ]
-    )
+    place = jnp.stack([z, y, c, x]).astype(jnp.int32)
+    vmem = pl.BlockSpec(memory_space=pltpu.VMEM)
+    smem = pl.BlockSpec(memory_space=pltpu.SMEM)
+    message, gain = pl.pallas_call(
+        functools.partial(pack, layers),
+        out_shape=(
+            jax.ShapeDtypeStruct((cuts[2] + 16 + 4 * seqs * tok, 128), jnp.bfloat16),
+            jax.ShapeDtypeStruct(norm_gain.shape, jnp.float32),
+        ),
+        in_specs=[smem] + [vmem] * 6,
+        out_specs=(vmem, vmem),
+        compiler_params=pltpu.CompilerParams(vmem_limit_bytes=2**21),
+        cost_estimate=pl.CostEstimate(flops=10**6, bytes_accessed=3 * 10**5, transcendentals=0),
+        name="pack",
+    )(
+        place,
+        in_weight,
+        jnp.swapaxes(out_weight, 1, 2),
+        mixing.reshape(layers, 4, 128),
+        pool_scale,
+        activations,
+        norm_gain,
+    )
+    mate_rows = jnp.concatenate(
+        [chip_mate.reshape(seqs * tok, width)[:, 128 * h : 128 * (h + 1)] for h in range(2)]
+    )
+    mate_at = cuts[2] + 16 + (1 - c) * (2 * seqs * tok)
+    message = lax.dynamic_update_slice(message, mate_rows, (mate_at, 0))
     got = [message] + [send(message, from_u(k)) for k in (1, 2, 3)]
     ab = jnp.stack([part[: cuts[1]] for part in got])
     q = jnp.stack([part[cuts[1] : cuts[2]] for part in got])
@@ -262,13 +294,14 @@
     tokens = jnp.where(c == 0, tokens, tokens_2)
 
     ab = [ab] + [send(ab, from_z(k)) for k in (1, 2, 3)]
-    q = jnp.stack([q] + [send(q, from_v(k)) for k in (1, 2, 3)])
-    mine = tokens[:, : 2 * NC * seqs * tok, :].reshape(4, 2, NC, seqs * tok, 128)
-    mine = jnp.where(c == 0, mine[:, :, 0], mine[:, :, 1]).reshape(4, 2 * seqs * tok, 128)
+    q = [q] + [send(q, from_v(k)) for k in (1, 2, 3)]
+    count = 2 * seqs * tok
+    mine = jnp.where(c == 0, tokens[:, 16 : 16 + count], tokens[:, 16 + count :])
     beside = send(mine, across_chips())
     a = jnp.stack([part[:, : cuts[0]] for part in ab])
     b = jnp.stack([part[:, cuts[0] :] for part in ab])
     a = [a] + [send(a, from_v(k)) for k in (1, 2, 3)]
+    q = jnp.stack(q)
     q = [q] + [send(q, from_z(k)) for k in (1, 2, 3)]
     b = [b] + [send(b, from_v(k)) for k in (1, 2, 3)]
     a_2 = [send(part, from_core()) for part in a]
@@ -277,9 +310,6 @@
     b_2 += [send(part, from_core()) for part in b[1:]]
     q_2 += [send(part, from_core()) for part in q[1:]]
 
-    place = jnp.stack([z, y, c, x]).astype(jnp.int32)
-    vmem = pl.BlockSpec(memory_space=pltpu.VMEM)
-    smem = pl.BlockSpec(memory_space=pltpu.SMEM)
     rows = seqs * 3 * tok
     dims = (layers, seqs, tok, tok, seq_len)
     weights = pltpu.VMEM((half, 4, 1024, 128), jnp.bfloat16)
@@ -310,7 +340,7 @@
         *a_2,
         tokens,
         beside,
-        norm_gain,
+        gain,
     )
     result = pl.pallas_call(
         functools.partial(second_half, dims),
@@ -330,7 +360,7 @@
         state,
         mix_late,
         scales,
-        norm_gain,
+        gain,
     )
     return result.reshape(seqs, tok, width)
 

time: 90.7 us -> 79 us (0.87)
  the two profiles are of different devices: /device:TPU:33 before, /device:TPU:0 now
where the time goes in v2:
time: 79 us; the launch traced here: 77.7 us
  starting transfers between devices  36.4 us (46%)
  waiting for transfers between devices  29.4 us (37%)
  Pallas kernels  9.69 us (12%)
  local copies, waits for them, and re-layouts  1.5 us (2%)
    ppermute x33, starting transfers between devices, send(): return lax.ppermute(value, AXES, perm)  36.4 us
    ppermute x33, waiting for transfers between devices, send(): return lax.ppermute(value, AXES, perm)  29.4 us
    pallas_call x1, Pallas kernels, body(): pl.pallas_call(functools.partial(second_half, dims), out_shape=jax.ShapeD...  4.65 us
    pallas_call x1, Pallas kernels, body(): pl.pallas_call(functools.partial(first_half, dims), out_shape=(jax.ShapeD...  4.49 us
  transfers between devices with their start and end apart: 33, of which 12 were waited for; matrix products, arithmetic and copies ran while one was open for 1% of the time, Pallas kernels for 6%

profile of v2, /device:TPU:0, one launch (start us, length us, event | category | flops | bytes accessed | tf_op | source)
XLA Modules:
  0.0 77.7 jit_solution(9625208511040931085)
XLA Ops:
  0.1 0.1 pad_add_fusion.place_ref
  0.1 0.5 copy-done.5
  0.7 0.1 copy-done.3
  0.7 0.1 copy-done.2
  0.8 0.7 copy-done.4
  1.5 0.6 pack.1
  2.1 1.7 %collective-permute-start.3 = (bf16[544,128]{1,0:T(8,128)(2,1)S(1)}, bf16[544,128]{1,0:T(8,128)(2,1)S(1)}, u32[]{:S(2)}, u32[]{:S(2)}) collective-permute-start(bf16[544,128]{1,0:T(8,128)(2,1)S(1)} %maximum_dynamic-update-slice_fusion), channel_id=1, source_target_pairs={{3,0},{0,1},{1,2},{2,3},{28,4},{29,5},{30,6},{31,7},{11,8},{8,9},{... | collective-permute-start | bytes 417800 | tf_op jit(solution)/shard_map/ppermute | solution.py:54
  3.8 2.7 %collective-permute-start.2 = (bf16[544,128]{1,0:T(8,128)(2,1)S(1)}, bf16[544,128]{1,0:T(8,128)(2,1)S(1)}, u32[]{:S(2)}, u32[]{:S(2)}) collective-permute-start(bf16[544,128]{1,0:T(8,128)(2,1)S(1)} %maximum_dynamic-update-slice_fusion), channel_id=1, source_target_pairs={{2,0},{3,1},{0,2},{1,3},{20,4},{21,5},{22,6},{23,7},{10,8},{11,9},... | collective-permute-start | bytes 417800 | tf_op jit(solution)/shard_map/ppermute | solution.py:54
  6.5 1.4 %collective-permute-start.1 = (bf16[544,128]{1,0:T(8,128)(2,1)S(1)}, bf16[544,128]{1,0:T(8,128)(2,1)S(1)}, u32[]{:S(2)}, u32[]{:S(2)}) collective-permute-start(bf16[544,128]{1,0:T(8,128)(2,1)S(1)} %maximum_dynamic-update-slice_fusion), channel_id=1, source_target_pairs={{1,0},{2,1},{3,2},{0,3},{12,4},{13,5},{14,6},{15,7},{9,8},{10,9},{... | collective-permute-start | bytes 417800 | tf_op jit(solution)/shard_map/ppermute | solution.py:54
  8.0 0.5 collective-permute-done.3
  8.5 2.6 %collective-permute-done.2 = bf16[544,128]{1,0:T(8,128)(2,1)S(1)} collective-permute-done((bf16[544,128]{1,0:T(8,128)(2,1)S(1)}, bf16[544,128]{1,0:T(8,128)(2,1)S(1)}, u32[]{:S(2)}, u32[]{:S(2)}) %collective-permute-start.2) | collective-permute-done | bytes 139296 | tf_op jit(solution)/shard_map/ppermute | solution.py:54
  11.1 0.5 collective-permute-done.1
  11.6 2.0 %collective-permute-start.6 = (bf16[4,208,128]{2,1,0:T(8,128)(2,1)S(1)}, bf16[4,208,128]{2,1,0:T(8,128)(2,1)S(1)}, u32[]{:S(2)}, u32[]{:S(2)}) collective-permute-start(bf16[4,208,128]{2,1,0:T(8,128)(2,1)S(1)} %pad_maximum_fusion.4), channel_id=1, source_target_pairs={{96,0},{97,1},{98,2},{99,3},{100,4},{101,5},{102,6},{103,7},{104,8... | collective-permute-start | bytes 638984 | tf_op jit(solution)/shard_map/ppermute | solution.py:54
  13.6 2.2 %collective-permute-start.4 = (bf16[4,208,128]{2,1,0:T(8,128)(2,1)S(1)}, bf16[4,208,128]{2,1,0:T(8,128)(2,1)S(1)}, u32[]{:S(2)}, u32[]{:S(2)}) collective-permute-start(bf16[4,208,128]{2,1,0:T(8,128)(2,1)S(1)} %pad_maximum_fusion.4), channel_id=1, source_target_pairs={{32,0},{33,1},{34,2},{35,3},{36,4},{37,5},{38,6},{39,7},{40,8},{41... | collective-permute-start | bytes 638984 | tf_op jit(solution)/shard_map/ppermute | solution.py:54
  15.9 3.1 %collective-permute-start.14 = (bf16[4,64,128]{2,1,0:T(8,128)(2,1)S(1)}, bf16[4,64,128]{2,1,0:T(8,128)(2,1)S(1)}, u32[]{:S(2)}, u32[]{:S(2)}) collective-permute-start(bf16[4,64,128]{2,1,0:T(8,128)(2,1)S(1)} %get-tuple-element.16), channel_id=1, source_target_pairs={{8,0},{9,1},{10,2},{11,3},{5,4},{6,5},{7,6},{4,7},{16,8},{17,9},{1... | collective-permute-start | bytes 196616 | tf_op jit(solution)/shard_map/ppermute | solution.py:54
  19.0 0.6 collective-permute-start.15
  19.6 1.0 %collective-permute-start.16 = (bf16[4,64,128]{2,1,0:T(8,128)(2,1)S(1)}, bf16[4,64,128]{2,1,0:T(8,128)(2,1)S(1)}, u32[]{:S(2)}, u32[]{:S(2)}) collective-permute-start(bf16[4,64,128]{2,1,0:T(8,128)(2,1)S(1)} %get-tuple-element.16), channel_id=1, source_target_pairs={{24,0},{25,1},{26,2},{27,3},{7,4},{4,5},{5,6},{6,7},{0,8},{1,9},{2... | collective-permute-start | bytes 196616 | tf_op jit(solution)/shard_map/ppermute | solution.py:54
  20.7 0.2 collective-permute-done.14
  20.9 1.8 %collective-permute-start.5 = (bf16[4,208,128]{2,1,0:T(8,128)(2,1)S(1)}, bf16[4,208,128]{2,1,0:T(8,128)(2,1)S(1)}, u32[]{:S(2)}, u32[]{:S(2)}) collective-permute-start(bf16[4,208,128]{2,1,0:T(8,128)(2,1)S(1)} %pad_maximum_fusion.4), channel_id=1, source_target_pairs={{64,0},{65,1},{66,2},{67,3},{68,4},{69,5},{70,6},{71,7},{72,8},{73... | collective-permute-start | bytes 638984 | tf_op jit(solution)/shard_map/ppermute | solution.py:54
  22.7 2.1 %collective-permute-done.15 = bf16[4,64,128]{2,1,0:T(8,128)(2,1)S(1)} collective-permute-done((bf16[4,64,128]{2,1,0:T(8,128)(2,1)S(1)}, bf16[4,64,128]{2,1,0:T(8,128)(2,1)S(1)}, u32[]{:S(2)}, u32[]{:S(2)}) %collective-permute-start.15) | collective-permute-done | bytes 65568 | tf_op jit(solution)/shard_map/ppermute | solution.py:54
  24.8 0.7 collective-permute-done.16
  25.5 2.0 %collective-permute-start.17 = (bf16[4,4,64,128]{3,2,1,0:T(8,128)(2,1)S(1)}, bf16[4,4,64,128]{3,2,1,0:T(8,128)(2,1)S(1)}, u32[]{:S(2)}, u32[]{:S(2)}) collective-permute-start(bf16[4,4,64,128]{3,2,1,0:T(8,128)(2,1)S(1)} %pad_maximum_fusion.3.refs_8_), channel_id=1, source_target_pairs={{32,0},{33,1},{34,2},{35,3},{36,4},{37,5},{38,6},{39,7},{40,8},{41... | collective-permute-start | bytes 786440 | tf_op jit(solution)/shard_map/ppermute | solution.py:54
  27.5 1.3 %collective-permute-start.19 = (bf16[4,4,64,128]{3,2,1,0:T(8,128)(2,1)S(1)}, bf16[4,4,64,128]{3,2,1,0:T(8,128)(2,1)S(1)}, u32[]{:S(2)}, u32[]{:S(2)}) collective-permute-start(bf16[4,4,64,128]{3,2,1,0:T(8,128)(2,1)S(1)} %pad_maximum_fusion.3.refs_8_), channel_id=1, source_target_pairs={{96,0},{97,1},{98,2},{99,3},{100,4},{101,5},{102,6},{103,7},{104,8... | collective-permute-start | bytes 786440 | tf_op jit(solution)/shard_map/ppermute | solution.py:54
  28.9 0.1 collective-permute-start.20
  29.0 0.1 pad_maximum_fusion.refs_0_
  29.2 2.9 %collective-permute-start.24 = (bf16[4,4,144,128]{3,2,1,0:T(8,128)(2,1)S(1)}, bf16[4,4,144,128]{3,2,1,0:T(8,128)(2,1)S(1)}, u32[]{:S(2)}, u32[]{:S(2)}) collective-permute-start(bf16[4,4,144,128]{3,2,1,0:T(8,128)(2,1)S(1)} %pad_maximum_fusion.refs_0_), channel_id=1, source_target_pairs={{8,0},{9,1},{10,2},{11,3},{5,4},{6,5},{7,6},{4,7},{16,8},{17,9},{1... | collective-permute-start | bytes 1769480 | tf_op jit(solution)/shard_map/ppermute | solution.py:54
  32.0 0.1 broadcast_select_fusion.refs_8_
  32.1 6.6 %collective-permute-done.17.refs_9_ = bf16[4,4,64,128]{3,2,1,0:T(8,128)(2,1)S(1)} collective-permute-done((bf16[4,4,64,128]{3,2,1,0:T(8,128)(2,1)S(1)}, bf16[4,4,64,128]{3,2,1,0:T(8,128)(2,1)S(1)}, u32[]{:S(2)}, u32[]{:S(2)}) %collective-permute-start.17) | collective-permute-done | bytes 262176 | tf_op jit(solution)/shard_map/ppermute | solution.py:54
  38.7 0.4 collective-permute-start.26
  39.2 3.1 %collective-permute-done.19.refs_11_ = bf16[4,4,64,128]{3,2,1,0:T(8,128)(2,1)S(1)} collective-permute-done((bf16[4,4,64,128]{3,2,1,0:T(8,128)(2,1)S(1)}, bf16[4,4,64,128]{3,2,1,0:T(8,128)(2,1)S(1)}, u32[]{:S(2)}, u32[]{:S(2)}) %collective-permute-start.19) | collective-permute-done | bytes 262176 | tf_op jit(solution)/shard_map/ppermute | solution.py:54
  42.2 0.9 %collective-permute-start.7 = (bf16[4,4,64,128]{3,2,1,0:T(8,128)(2,1)S(1)}, bf16[4,4,64,128]{3,2,1,0:T(8,128)(2,1)S(1)}, u32[]{:S(2)}, u32[]{:S(2)}) collective-permute-start(bf16[4,4,64,128]{3,2,1,0:T(8,128)(2,1)S(1)} %pad_maximum_fusion.2.refs_0_), channel_id=1, source_target_pairs={{8,0},{9,1},{10,2},{11,3},{5,4},{6,5},{7,6},{4,7},{16,8},{17,9},{1... | collective-permute-start | bytes 786440 | tf_op jit(solution)/shard_map/ppermute | solution.py:54
  43.1 0.7 collective-permute-start.32
  43.8 9.2 %collective-permute-start.8 = (bf16[4,4,64,128]{3,2,1,0:T(8,128)(2,1)S(1)}, bf16[4,4,64,128]{3,2,1,0:T(8,128)(2,1)S(1)}, u32[]{:S(2)}, u32[]{:S(2)}) collective-permute-start(bf16[4,4,64,128]{3,2,1,0:T(8,128)(2,1)S(1)} %pad_maximum_fusion.2.refs_0_), channel_id=1, source_target_pairs={{16,0},{17,1},{18,2},{19,3},{6,4},{7,5},{4,6},{5,7},{24,8},{25,9},... | collective-permute-start | bytes 786440 | tf_op jit(solution)/shard_map/ppermute | solution.py:54
  53.0 7.8 %collective-permute-done.8.refs_2_ = bf16[4,4,64,128]{3,2,1,0:T(8,128)(2,1)S(1)} collective-permute-done((bf16[4,4,64,128]{3,2,1,0:T(8,128)(2,1)S(1)}, bf16[4,4,64,128]{3,2,1,0:T(8,128)(2,1)S(1)}, u32[]{:S(2)}, u32[]{:S(2)}) %collective-permute-start.8) | collective-permute-done | bytes 262176 | tf_op jit(solution)/shard_map/ppermute | solution.py:54
  60.8 0.5 collective-permute-start.28
  61.3 0.1 collective-permute-start.29
  61.4 0.4 collective-permute-start.30
  61.8 1.6 %collective-permute-done.9.refs_3_ = bf16[4,4,64,128]{3,2,1,0:T(8,128)(2,1)S(1)} collective-permute-done((bf16[4,4,64,128]{3,2,1,0:T(8,128)(2,1)S(1)}, bf16[4,4,64,128]{3,2,1,0:T(8,128)(2,1)S(1)}, u32[]{:S(2)}, u32[]{:S(2)}) %collective-permute-start.9) | collective-permute-done | bytes 262176 | tf_op jit(solution)/shard_map/ppermute | solution.py:54
  63.4 2.3 %collective-permute-done.10.refs_4_ = bf16[4,4,64,128]{3,2,1,0:T(8,128)(2,1)S(1)} collective-permute-done((bf16[4,4,64,128]{3,2,1,0:T(8,128)(2,1)S(1)}, bf16[4,4,64,128]{3,2,1,0:T(8,128)(2,1)S(1)}, u32[]{:S(2)}, u32[]{:S(2)}) %collective-permute-start.10) | collective-permute-done | bytes 262176 | tf_op jit(solution)/shard_map/ppermute | solution.py:54
  65.7 0.1 collective-permute-start.21
  65.8 1.4 %collective-permute-done.21.refs_13_ = bf16[4,4,64,128]{3,2,1,0:T(8,128)(2,1)S(1)} collective-permute-done((bf16[4,4,64,128]{3,2,1,0:T(8,128)(2,1)S(1)}, bf16[4,4,64,128]{3,2,1,0:T(8,128)(2,1)S(1)}, u32[]{:S(2)}, u32[]{:S(2)}) %collective-permute-start.21) | collective-permute-done | bytes 262176 | tf_op jit(solution)/shard_map/ppermute | solution.py:54
  67.2 0.1 collective-permute-start.22
  67.4 0.4 collective-permute-start.23
  67.8 0.1 collective-permute-start.11
  67.9 0.4 collective-permute-start.12
  68.3 0.3 collective-permute-start.13
  68.5 4.5 %first_half.1 = (bf16[192,1024]{1,0:T(8,128)(2,1)S(1)}, bf16[2,128,512]{2,1,0:T(8,128)(2,1)S(1)}, f32[4,4,128]{2,1,0:T(4,128)S(1)}) custom-call(s32[4]{0:T(128)S(1)} %pad_add_fusion.place_ref, bf16[4,4,144,128]{3,2,1,0:T(8,128)(2,1)S(1)} %pad_maximum_fusion.refs_0_, bf16[4,4,144,128]{3,2,1,0:T(8,128)(2,1)S(1)} %collective-permute-done.24.refs_1_, ...), custom_call_target="tpu_custom_call" | custom-call | flops 1000000000 | bytes 9000000 | tf_op jit(solution)/shard_map/first_half/pallas_call | solution.py:318
  73.1 4.6 %second_half.1 = bf16[64,256]{1,0:T(8,128)(2,1)} custom-call(s32[4]{0:T(128)S(1)} %pad_add_fusion.place_ref, bf16[4,4,64,128]{3,2,1,0:T(8,128)(2,1)S(1)} %pad_maximum_fusion.2.refs_0_, bf16[4,4,64,128]{3,2,1,0:T(8,128)(2,1)S(1)} %collective-permute-done.7.refs_1_, bf16[4,4,64,128]{3,2,1,0:T(8,128)(2,1)S(1)} %collective-permute-done.8.refs_2_, ...), custom_call_target="tpu_custom_call" | custom-call | flops 1000000000 | bytes 9000000 | tf_op jit(solution)/shard_map/second_half/pallas_call | solution.py:345
  (64 shorter events, 0.4 us)
Async XLA Ops:
  0.0 2.1 %collective-permute-start = (bf16[2,32,256]{2,1,0:T(8,128)(2,1)}, bf16[2,32,256]{2,1,0:T(8,128)(2,1)S(1)}, u32[]{:S(2)}, u32[]{:S(2)}) collective-permute-start(bf16[2,32,256]{2,1,0:T(8,128)(2,1)} %act_ref.1), channel_id=1, source_target_pairs={{4,0},{5,1},{6,2},{7,3},{0,4},{1,5},{2,6},{3,7},{12,8},{13,9},{14,... | collective-permute-start | bytes 98312 | tf_op jit(solution)/shard_map/ppermute | solution.py:54
  0.0 0.7 copy-start.5
  0.0 0.7 copy-start.3
  0.0 0.8 %copy-start.2 = (bf16[2,32,256]{2,1,0:T(8,128)(2,1)S(1)}, bf16[2,32,256]{2,1,0:T(8,128)(2,1)}, u32[]{:S(2)}) copy-start(bf16[2,32,256]{2,1,0:T(8,128)(2,1)} %act_ref.1) | copy-start | bytes 98308
  0.0 0.8 %copy-start.1 = (bf16[4,128,32]{1,2,0:T(8,128)(2,1)S(1)}, bf16[4,128,32]{1,2,0:T(8,128)(2,1)}, u32[]{:S(2)}) copy-start(bf16[4,128,32]{1,2,0:T(8,128)(2,1)} %param.9) | copy-start | bytes 98308
  0.0 0.8 %copy-start = (bf16[4,32,128]{2,1,0:T(8,128)(2,1)S(1)}, bf16[4,32,128]{2,1,0:T(8,128)(2,1)}, u32[]{:S(2)}) copy-start(bf16[4,32,128]{2,1,0:T(8,128)(2,1)} %in_ref.1) | copy-start | bytes 98308
  0.8 0.7 copy-start.4
  2.1 6.3 %collective-permute-start.3 = (bf16[544,128]{1,0:T(8,128)(2,1)S(1)}, bf16[544,128]{1,0:T(8,128)(2,1)S(1)}, u32[]{:S(2)}, u32[]{:S(2)}) collective-permute-start(bf16[544,128]{1,0:T(8,128)(2,1)S(1)} %maximum_dynamic-update-slice_fusion), channel_id=1, source_target_pairs={{3,0},{0,1},{1,2},{2,3},{28,4},{29,5},{30,6},{31,7},{11,8},{8,9},{... | collective-permute-start | bytes 417800 | tf_op jit(solution)/shard_map/ppermute | solution.py:54
  3.8 7.3 %collective-permute-start.2 = (bf16[544,128]{1,0:T(8,128)(2,1)S(1)}, bf16[544,128]{1,0:T(8,128)(2,1)S(1)}, u32[]{:S(2)}, u32[]{:S(2)}) collective-permute-start(bf16[544,128]{1,0:T(8,128)(2,1)S(1)} %maximum_dynamic-update-slice_fusion), channel_id=1, source_target_pairs={{2,0},{3,1},{0,2},{1,3},{20,4},{21,5},{22,6},{23,7},{10,8},{11,9},... | collective-permute-start | bytes 417800 | tf_op jit(solution)/shard_map/ppermute | solution.py:54
  6.5 5.1 %collective-permute-start.1 = (bf16[544,128]{1,0:T(8,128)(2,1)S(1)}, bf16[544,128]{1,0:T(8,128)(2,1)S(1)}, u32[]{:S(2)}, u32[]{:S(2)}) collective-permute-start(bf16[544,128]{1,0:T(8,128)(2,1)S(1)} %maximum_dynamic-update-slice_fusion), channel_id=1, source_target_pairs={{1,0},{2,1},{3,2},{0,3},{12,4},{13,5},{14,6},{15,7},{9,8},{10,9},{... | collective-permute-start | bytes 417800 | tf_op jit(solution)/shard_map/ppermute | solution.py:54
  11.6 15.9 %collective-permute-start.6 = (bf16[4,208,128]{2,1,0:T(8,128)(2,1)S(1)}, bf16[4,208,128]{2,1,0:T(8,128)(2,1)S(1)}, u32[]{:S(2)}, u32[]{:S(2)}) collective-permute-start(bf16[4,208,128]{2,1,0:T(8,128)(2,1)S(1)} %pad_maximum_fusion.4), channel_id=1, source_target_pairs={{96,0},{97,1},{98,2},{99,3},{100,4},{101,5},{102,6},{103,7},{104,8... | collective-permute-start | bytes 638984 | tf_op jit(solution)/shard_map/ppermute | solution.py:54
  13.6 13.9 %collective-permute-start.4 = (bf16[4,208,128]{2,1,0:T(8,128)(2,1)S(1)}, bf16[4,208,128]{2,1,0:T(8,128)(2,1)S(1)}, u32[]{:S(2)}, u32[]{:S(2)}) collective-permute-start(bf16[4,208,128]{2,1,0:T(8,128)(2,1)S(1)} %pad_maximum_fusion.4), channel_id=1, source_target_pairs={{32,0},{33,1},{34,2},{35,3},{36,4},{37,5},{38,6},{39,7},{40,8},{41... | collective-permute-start | bytes 638984 | tf_op jit(solution)/shard_map/ppermute | solution.py:54
  15.9 5.0 %collective-permute-start.14 = (bf16[4,64,128]{2,1,0:T(8,128)(2,1)S(1)}, bf16[4,64,128]{2,1,0:T(8,128)(2,1)S(1)}, u32[]{:S(2)}, u32[]{:S(2)}) collective-permute-start(bf16[4,64,128]{2,1,0:T(8,128)(2,1)S(1)} %get-tuple-element.16), channel_id=1, source_target_pairs={{8,0},{9,1},{10,2},{11,3},{5,4},{6,5},{7,6},{4,7},{16,8},{17,9},{1... | collective-permute-start | bytes 196616 | tf_op jit(solution)/shard_map/ppermute | solution.py:54
  19.0 5.8 %collective-permute-start.15 = (bf16[4,64,128]{2,1,0:T(8,128)(2,1)S(1)}, bf16[4,64,128]{2,1,0:T(8,128)(2,1)S(1)}, u32[]{:S(2)}, u32[]{:S(2)}) collective-permute-start(bf16[4,64,128]{2,1,0:T(8,128)(2,1)S(1)} %get-tuple-element.16), channel_id=1, source_target_pairs={{16,0},{17,1},{18,2},{19,3},{6,4},{7,5},{4,6},{5,7},{24,8},{25,9},... | collective-permute-start | bytes 196616 | tf_op jit(solution)/shard_map/ppermute | solution.py:54
  19.6 5.8 %collective-permute-start.16 = (bf16[4,64,128]{2,1,0:T(8,128)(2,1)S(1)}, bf16[4,64,128]{2,1,0:T(8,128)(2,1)S(1)}, u32[]{:S(2)}, u32[]{:S(2)}) collective-permute-start(bf16[4,64,128]{2,1,0:T(8,128)(2,1)S(1)} %get-tuple-element.16), channel_id=1, source_target_pairs={{24,0},{25,1},{26,2},{27,3},{7,4},{4,5},{5,6},{6,7},{0,8},{1,9},{2... | collective-permute-start | bytes 196616 | tf_op jit(solution)/shard_map/ppermute | solution.py:54
  20.9 8.0 %collective-permute-start.5 = (bf16[4,208,128]{2,1,0:T(8,128)(2,1)S(1)}, bf16[4,208,128]{2,1,0:T(8,128)(2,1)S(1)}, u32[]{:S(2)}, u32[]{:S(2)}) collective-permute-start(bf16[4,208,128]{2,1,0:T(8,128)(2,1)S(1)} %pad_maximum_fusion.4), channel_id=1, source_target_pairs={{64,0},{65,1},{66,2},{67,3},{68,4},{69,5},{70,6},{71,7},{72,8},{73... | collective-permute-start | bytes 638984 | tf_op jit(solution)/shard_map/ppermute | solution.py:54
  24.8 4.4 %collective-permute-start.31 = (bf16[4,272,128]{2,1,0:T(8,128)(2,1)S(1)}, bf16[4,272,128]{2,1,0:T(8,128)(2,1)S(1)}, u32[]{:S(2)}, u32[]{:S(2)}) collective-permute-start(bf16[4,272,128]{2,1,0:T(8,128)(2,1)S(1)} %pad_maximum_fusion.1), channel_id=1, source_target_pairs={{4,0},{5,1},{6,2},{7,3},{0,4},{1,5},{2,6},{3,7},{12,8},{13,9},{14,... | collective-permute-start | bytes 835592 | tf_op jit(solution)/shard_map/ppermute | solution.py:54
  25.5 13.2 %collective-permute-start.17 = (bf16[4,4,64,128]{3,2,1,0:T(8,128)(2,1)S(1)}, bf16[4,4,64,128]{3,2,1,0:T(8,128)(2,1)S(1)}, u32[]{:S(2)}, u32[]{:S(2)}) collective-permute-start(bf16[4,4,64,128]{3,2,1,0:T(8,128)(2,1)S(1)} %pad_maximum_fusion.3.refs_8_), channel_id=1, source_target_pairs={{32,0},{33,1},{34,2},{35,3},{36,4},{37,5},{38,6},{39,7},{40,8},{41... | collective-permute-start | bytes 786440 | tf_op jit(solution)/shard_map/ppermute | solution.py:54
  27.5 11.2 %collective-permute-start.18 = (bf16[4,4,64,128]{3,2,1,0:T(8,128)(2,1)S(1)}, bf16[4,4,64,128]{3,2,1,0:T(8,128)(2,1)S(1)}, u32[]{:S(2)}, u32[]{:S(2)}) collective-permute-start(bf16[4,4,64,128]{3,2,1,0:T(8,128)(2,1)S(1)} %pad_maximum_fusion.3.refs_8_), channel_id=1, source_target_pairs={{64,0},{65,1},{66,2},{67,3},{68,4},{69,5},{70,6},{71,7},{72,8},{73... | collective-permute-start | bytes 786440 | tf_op jit(solution)/shard_map/ppermute | solution.py:54
  27.5 14.7 %collective-permute-start.19 = (bf16[4,4,64,128]{3,2,1,0:T(8,128)(2,1)S(1)}, bf16[4,4,64,128]{3,2,1,0:T(8,128)(2,1)S(1)}, u32[]{:S(2)}, u32[]{:S(2)}) collective-permute-start(bf16[4,4,64,128]{3,2,1,0:T(8,128)(2,1)S(1)} %pad_maximum_fusion.3.refs_8_), channel_id=1, source_target_pairs={{96,0},{97,1},{98,2},{99,3},{100,4},{101,5},{102,6},{103,7},{104,8... | collective-permute-start | bytes 786440 | tf_op jit(solution)/shard_map/ppermute | solution.py:54
  28.9 14.2 %collective-permute-start.20 = (bf16[4,4,64,128]{3,2,1,0:T(8,128)(2,1)S(1)}, bf16[4,4,64,128]{3,2,1,0:T(8,128)(2,1)S(1)}, u32[]{:S(2)}, u32[]{:S(2)}) collective-permute-start(bf16[4,4,64,128]{3,2,1,0:T(8,128)(2,1)S(1)} %pad_maximum_fusion.3.refs_8_), channel_id=1, source_target_pairs={{4,0},{5,1},{6,2},{7,3},{0,4},{1,5},{2,6},{3,7},{12,8},{13,9},{14,... | collective-permute-start | bytes 786440 | tf_op jit(solution)/shard_map/ppermute | solution.py:54
  29.2 31.6 %collective-permute-start.24 = (bf16[4,4,144,128]{3,2,1,0:T(8,128)(2,1)S(1)}, bf16[4,4,144,128]{3,2,1,0:T(8,128)(2,1)S(1)}, u32[]{:S(2)}, u32[]{:S(2)}) collective-permute-start(bf16[4,4,144,128]{3,2,1,0:T(8,128)(2,1)S(1)} %pad_maximum_fusion.refs_0_), channel_id=1, source_target_pairs={{8,0},{9,1},{10,2},{11,3},{5,4},{6,5},{7,6},{4,7},{16,8},{17,9},{1... | collective-permute-start | bytes 1769480 | tf_op jit(solution)/shard_map/ppermute | solution.py:54
  38.7 22.6 %collective-permute-start.25 = (bf16[4,4,144,128]{3,2,1,0:T(8,128)(2,1)S(1)}, bf16[4,4,144,128]{3,2,1,0:T(8,128)(2,1)S(1)}, u32[]{:S(2)}, u32[]{:S(2)}) collective-permute-start(bf16[4,4,144,128]{3,2,1,0:T(8,128)(2,1)S(1)} %pad_maximum_fusion.refs_0_), channel_id=1, source_target_pairs={{16,0},{17,1},{18,2},{19,3},{6,4},{7,5},{4,6},{5,7},{24,8},{25,9},... | collective-permute-start | bytes 1769480 | tf_op jit(solution)/shard_map/ppermute | solution.py:54
  38.7 22.7 %collective-permute-start.26 = (bf16[4,4,144,128]{3,2,1,0:T(8,128)(2,1)S(1)}, bf16[4,4,144,128]{3,2,1,0:T(8,128)(2,1)S(1)}, u32[]{:S(2)}, u32[]{:S(2)}) collective-permute-start(bf16[4,4,144,128]{3,2,1,0:T(8,128)(2,1)S(1)} %pad_maximum_fusion.refs_0_), channel_id=1, source_target_pairs={{24,0},{25,1},{26,2},{27,3},{7,4},{4,5},{5,6},{6,7},{0,8},{1,9},{2... | collective-permute-start | bytes 1769480 | tf_op jit(solution)/shard_map/ppermute | solution.py:54
  42.2 10.8 %collective-permute-start.7 = (bf16[4,4,64,128]{3,2,1,0:T(8,128)(2,1)S(1)}, bf16[4,4,64,128]{3,2,1,0:T(8,128)(2,1)S(1)}, u32[]{:S(2)}, u32[]{:S(2)}) collective-permute-start(bf16[4,4,64,128]{3,2,1,0:T(8,128)(2,1)S(1)} %pad_maximum_fusion.2.refs_0_), channel_id=1, source_target_pairs={{8,0},{9,1},{10,2},{11,3},{5,4},{6,5},{7,6},{4,7},{16,8},{17,9},{1... | collective-permute-start | bytes 786440 | tf_op jit(solution)/shard_map/ppermute | solution.py:54
  43.1 0.7 collective-permute-start.32
  43.8 17.0 %collective-permute-start.8 = (bf16[4,4,64,128]{3,2,1,0:T(8,128)(2,1)S(1)}, bf16[4,4,64,128]{3,2,1,0:T(8,128)(2,1)S(1)}, u32[]{:S(2)}, u32[]{:S(2)}) collective-permute-start(bf16[4,4,64,128]{3,2,1,0:T(8,128)(2,1)S(1)} %pad_maximum_fusion.2.refs_0_), channel_id=1, source_target_pairs={{16,0},{17,1},{18,2},{19,3},{6,4},{7,5},{4,6},{5,7},{24,8},{25,9},... | collective-permute-start | bytes 786440 | tf_op jit(solution)/shard_map/ppermute | solution.py:54
  53.0 10.4 %collective-permute-start.9 = (bf16[4,4,64,128]{3,2,1,0:T(8,128)(2,1)S(1)}, bf16[4,4,64,128]{3,2,1,0:T(8,128)(2,1)S(1)}, u32[]{:S(2)}, u32[]{:S(2)}) collective-permute-start(bf16[4,4,64,128]{3,2,1,0:T(8,128)(2,1)S(1)} %pad_maximum_fusion.2.refs_0_), channel_id=1, source_target_pairs={{24,0},{25,1},{26,2},{27,3},{7,4},{4,5},{5,6},{6,7},{0,8},{1,9},{2... | collective-permute-start | bytes 786440 | tf_op jit(solution)/shard_map/ppermute | solution.py:54
  60.8 6.6 %collective-permute-start.27 = (bf16[4,4,144,128]{3,2,1,0:T(8,128)(2,1)S(1)}, bf16[4,4,144,128]{3,2,1,0:T(8,128)(2,1)S(1)}, u32[]{:S(2)}, u32[]{:S(2)}) collective-permute-start(bf16[4,4,144,128]{3,2,1,0:T(8,128)(2,1)S(1)} %pad_maximum_fusion.refs_0_), channel_id=1, source_target_pairs={{4,0},{5,1},{6,2},{7,3},{0,4},{1,5},{2,6},{3,7},{12,8},{13,9},{14,... | collective-permute-start | bytes 1769480 | tf_op jit(solution)/shard_map/ppermute | solution.py:54
  60.8 7.0 %collective-permute-start.28 = (bf16[4,4,144,128]{3,2,1,0:T(8,128)(2,1)S(1)}, bf16[4,4,144,128]{3,2,1,0:T(8,128)(2,1)S(1)}, u32[]{:S(2)}, u32[]{:S(2)}) collective-permute-start(bf16[4,4,144,128]{3,2,1,0:T(8,128)(2,1)S(1)} %collective-permute-done.24.refs_1_), channel_id=1, source_target_pairs={{4,0},{5,1},{6,2},{7,3},{0,4},{1,5},{2,6},{3,7},{12,8},{13,9},{14,... | collective-permute-start | bytes 1769480 | tf_op jit(solution)/shard_map/ppermute | solution.py:54
  61.3 6.6 %collective-permute-start.29 = (bf16[4,4,144,128]{3,2,1,0:T(8,128)(2,1)S(1)}, bf16[4,4,144,128]{3,2,1,0:T(8,128)(2,1)S(1)}, u32[]{:S(2)}, u32[]{:S(2)}) collective-permute-start(bf16[4,4,144,128]{3,2,1,0:T(8,128)(2,1)S(1)} %collective-permute-done.25.refs_2_), channel_id=1, source_target_pairs={{4,0},{5,1},{6,2},{7,3},{0,4},{1,5},{2,6},{3,7},{12,8},{13,9},{14,... | collective-permute-start | bytes 1769480 | tf_op jit(solution)/shard_map/ppermute | solution.py:54
  61.4 6.9 %collective-permute-start.30 = (bf16[4,4,144,128]{3,2,1,0:T(8,128)(2,1)S(1)}, bf16[4,4,144,128]{3,2,1,0:T(8,128)(2,1)S(1)}, u32[]{:S(2)}, u32[]{:S(2)}) collective-permute-start(bf16[4,4,144,128]{3,2,1,0:T(8,128)(2,1)S(1)} %collective-permute-done.26.refs_3_), channel_id=1, source_target_pairs={{4,0},{5,1},{6,2},{7,3},{0,4},{1,5},{2,6},{3,7},{12,8},{13,9},{14,... | collective-permute-start | bytes 1769480 | tf_op jit(solution)/shard_map/ppermute | solution.py:54
  63.4 2.3 %collective-permute-start.10 = (bf16[4,4,64,128]{3,2,1,0:T(8,128)(2,1)S(1)}, bf16[4,4,64,128]{3,2,1,0:T(8,128)(2,1)S(1)}, u32[]{:S(2)}, u32[]{:S(2)}) collective-permute-start(bf16[4,4,64,128]{3,2,1,0:T(8,128)(2,1)S(1)} %pad_maximum_fusion.2.refs_0_), channel_id=1, source_target_pairs={{4,0},{5,1},{6,2},{7,3},{0,4},{1,5},{2,6},{3,7},{12,8},{13,9},{14,... | collective-permute-start | bytes 786440 | tf_op jit(solution)/shard_map/ppermute | solution.py:54
  65.7 1.5 %collective-permute-start.21 = (bf16[4,4,64,128]{3,2,1,0:T(8,128)(2,1)S(1)}, bf16[4,4,64,128]{3,2,1,0:T(8,128)(2,1)S(1)}, u32[]{:S(2)}, u32[]{:S(2)}) collective-permute-start(bf16[4,4,64,128]{3,2,1,0:T(8,128)(2,1)S(1)} %collective-permute-done.17.refs_9_), channel_id=1, source_target_pairs={{4,0},{5,1},{6,2},{7,3},{0,4},{1,5},{2,6},{3,7},{12,8},{13,9},{14,... | collective-permute-start | bytes 786440 | tf_op jit(solution)/shard_map/ppermute | solution.py:54
  67.2 5.8 %collective-permute-start.22 = (bf16[4,4,64,128]{3,2,1,0:T(8,128)(2,1)S(1)}, bf16[4,4,64,128]{3,2,1,0:T(8,128)(2,1)S(1)}, u32[]{:S(2)}, u32[]{:S(2)}) collective-permute-start(bf16[4,4,64,128]{3,2,1,0:T(8,128)(2,1)S(1)} %collective-permute-done.18.refs_10_), channel_id=1, source_target_pairs={{4,0},{5,1},{6,2},{7,3},{0,4},{1,5},{2,6},{3,7},{12,8},{13,9},{14,... | collective-permute-start | bytes 786440 | tf_op jit(solution)/shard_map/ppermute | solution.py:54
  67.4 5.7 %collective-permute-start.23 = (bf16[4,4,64,128]{3,2,1,0:T(8,128)(2,1)S(1)}, bf16[4,4,64,128]{3,2,1,0:T(8,128)(2,1)S(1)}, u32[]{:S(2)}, u32[]{:S(2)}) collective-permute-start(bf16[4,4,64,128]{3,2,1,0:T(8,128)(2,1)S(1)} %collective-permute-done.19.refs_11_), channel_id=1, source_target_pairs={{4,0},{5,1},{6,2},{7,3},{0,4},{1,5},{2,6},{3,7},{12,8},{13,9},{14,... | collective-permute-start | bytes 786440 | tf_op jit(solution)/shard_map/ppermute | solution.py:54
  67.8 5.3 %collective-permute-start.11 = (bf16[4,4,64,128]{3,2,1,0:T(8,128)(2,1)S(1)}, bf16[4,4,64,128]{3,2,1,0:T(8,128)(2,1)S(1)}, u32[]{:S(2)}, u32[]{:S(2)}) collective-permute-start(bf16[4,4,64,128]{3,2,1,0:T(8,128)(2,1)S(1)} %collective-permute-done.7.refs_1_), channel_id=1, source_target_pairs={{4,0},{5,1},{6,2},{7,3},{0,4},{1,5},{2,6},{3,7},{12,8},{13,9},{14,... | collective-permute-start | bytes 786440 | tf_op jit(solution)/shard_map/ppermute | solution.py:54
  67.9 5.2 %collective-permute-start.12 = (bf16[4,4,64,128]{3,2,1,0:T(8,128)(2,1)S(1)}, bf16[4,4,64,128]{3,2,1,0:T(8,128)(2,1)S(1)}, u32[]{:S(2)}, u32[]{:S(2)}) collective-permute-start(bf16[4,4,64,128]{3,2,1,0:T(8,128)(2,1)S(1)} %collective-permute-done.8.refs_2_), channel_id=1, source_target_pairs={{4,0},{5,1},{6,2},{7,3},{0,4},{1,5},{2,6},{3,7},{12,8},{13,9},{14,... | collective-permute-start | bytes 786440 | tf_op jit(solution)/shard_map/ppermute | solution.py:54
  68.3 4.8 %collective-permute-start.13 = (bf16[4,4,64,128]{3,2,1,0:T(8,128)(2,1)S(1)}, bf16[4,4,64,128]{3,2,1,0:T(8,128)(2,1)S(1)}, u32[]{:S(2)}, u32[]{:S(2)}) collective-permute-start(bf16[4,4,64,128]{3,2,1,0:T(8,128)(2,1)S(1)} %collective-permute-done.9.refs_3_), channel_id=1, source_target_pairs={{4,0},{5,1},{6,2},{7,3},{0,4},{1,5},{2,6},{3,7},{12,8},{13,9},{14,... | collective-permute-start | bytes 786440 | tf_op jit(solution)/shard_map/ppermute | solution.py:54

commit v3 on v2

--- a/solution.py
+++ b/solution.py
@@ -25,16 +25,21 @@
     ]
 
 
-def from_z(k):
-    return pairs(lambda z, y, c, x: (z + k, y, c, x))
-
-
-def from_u(k):
-    return pairs(lambda z, y, c, x: (z, y + k * c, c, x + k * (1 - c)))
-
-
-def from_v(k):
-    return pairs(lambda z, y, c, x: (z, y + k * (1 - c), c, x + k * c))
+FIRST = ("xzy", "zyx")
+LAST = ("xyz", "yxz")
+
+
+def along(order, step, k):
+    def source(z, y, c, x):
+        at = dict(z=z, y=y, x=x)
+        at[order[c][step]] += k
+        return at["z"], at["y"], c, at["x"]
+
+    return pairs(source)
+
+
+def gather(value, order, step):
+    return [send(value, along(order, step, k)) for k in (1, 2, 3)]
 
 
 def from_core():
@@ -54,18 +59,18 @@
     return lax.ppermute(value, AXES, perm)
 
 
-def copy_blocks(place, sources, steps, copy):
+def copy_blocks(place, sources, order, copy):
     z, y, _, x = place
     for parts, core in sources:
         first = core == 0
         for k in range(4):
             for m in range(4):
                 for j in range(4):
-                    step = dict(zip(steps, (k, m, j)))
-                    y_at = lax.rem(y + jnp.where(first, step["v"], step["u"]), NY)
-                    x_at = lax.rem(x + jnp.where(first, step["u"], step["v"]), NX)
-                    index = lax.rem(z + step["z"], NZ) * (NY * NC) + y_at * NC + core
-                    copy(x_at, index, parts[k].at[m, j])
+                    north, south = (dict(zip(axes, (j, m, k))) for axes in order)
+                    y_at = lax.rem(y + jnp.where(first, north["y"], south["y"]), NY)
+                    x_at = lax.rem(x + jnp.where(first, north["x"], south["x"]), NX)
+                    z_at = lax.rem(z + jnp.where(first, north["z"], south["z"]), NZ)
+                    copy(x_at, z_at * (NY * NC) + y_at * NC + core, parts[k].at[m, j])
 
 
 def put_layers(layers, w_in, w_out, mix_raw=None):
@@ -82,26 +87,31 @@
     return copy
 
 
-def windows(start, seqs, span, seq_len):
+def tables(layers, seqs, tok, halo, seq_len, place_ref, bands, inverse, picks):
+    z, y, c = (place_ref[k] for k in range(3))
+    start = ((z * NY + y) * NC + c) * tok - halo
+    span = tok + 2 * halo
     rows = seqs * span
     r = lax.broadcasted_iota(jnp.int32, (rows, rows), 0)
     q = lax.broadcasted_iota(jnp.int32, (rows, rows), 1)
     same = (r >= span) == (q >= span)
     pos_r = start + jnp.where(r >= span, r - span, r)
     pos_q = start + jnp.where(q >= span, q - span, q)
-    r1 = lax.broadcasted_iota(jnp.int32, (rows, 1), 0)
+    r1 = lax.broadcasted_iota(jnp.int32, (rows, 128), 0)
     pos_1 = start + jnp.where(r1 >= span, r1 - span, r1)
-    bands, inverse = [], []
     for g in range(4):
         half = 2**g
         low = jnp.clip(pos_r - half, 0, seq_len)
         high = jnp.clip(pos_r + half, 0, seq_len)
-        bands.append(
-            jnp.where(same & (pos_q >= low) & (pos_q < high), 1.0, 0.0).astype(jnp.bfloat16)
-        )
+        inside = same & (pos_q >= low) & (pos_q < high)
+        bands[g] = jnp.where(inside, 1.0, 0.0).astype(jnp.bfloat16)
         count = jnp.clip(pos_1 + half, 0, seq_len) - jnp.clip(pos_1 - half, 0, seq_len)
-        inverse.append(1.0 / jnp.maximum(count, 1).astype(jnp.float32))
-    return bands, inverse
+        inverse[g] = 1.0 / jnp.maximum(count, 1).astype(jnp.float32)
+    pick_r = lax.broadcasted_iota(jnp.int32, (128, 512), 0)
+    pick_q = lax.broadcasted_iota(jnp.int32, (128, 512), 1)
+    base = ((pick_r >> 2) << 4) + (pick_r & 3)
+    for l in range(layers):
+        picks[l] = jnp.where(pick_q == base + 4 * l, 1.0, 0.0).astype(jnp.bfloat16)
 
 
 def mix_layer(state, gain, w_in, scales, mixing, bands, inverse):
@@ -130,15 +140,16 @@
 
 
 def first_half(dims, place_ref, *refs):
-    layers, seqs, tok, halo, seq_len = dims
+    layers, seqs, tok, halo, _ = dims
     own, other, acts, beside, gain = refs[0:4], refs[4:8], refs[8], refs[9], refs[10]
-    state_out, mix_out, scale_out = refs[11:14]
-    w_in, w_out, mix_raw, state_parts, scales = refs[14:]
+    bands, inverse, picks = refs[11:14]
+    state_out, mix_out, scale_out = refs[14:17]
+    w_in, w_out, mix_raw, state_parts, scales = refs[17:]
     place = tuple(place_ref[k] for k in range(4))
-    z, y, c, x = place
+    _, _, c, x = place
     half = layers // 2
     put = put_layers(range(half), w_in, w_out, mix_raw)
-    copy_blocks(place, ((own, c), (other, 1 - c)), "vzu", put)
+    copy_blocks(place, ((own, c), (other, 1 - c)), FIRST, put)
     span = tok + 2 * halo
     for k in range(4):
         x_at = lax.rem(x + k, NX)
@@ -155,18 +166,11 @@
         parts = acts[k, 0:16, :].astype(jnp.float32)
         scales[x_at] = parts[0:layers] + parts[layers : 2 * layers] + parts[2 * layers : 3 * layers]
     scale_out[...] = scales[...]
-    bands, inverse = windows(((z * NY + y) * NC + c) * tok - halo, seqs, span, seq_len)
-
-    pick_r = lax.broadcasted_iota(jnp.int32, (128, 512), 0)
-    pick_q = lax.broadcasted_iota(jnp.int32, (128, 512), 1)
-    base = ((pick_r >> 2) << 4) + (pick_r & 3)
     raw = jnp.concatenate([mix_raw[g] for g in range(4)], axis=1)
     mixings = []
     for l in range(layers):
-        pick = jnp.where(pick_q == base + 4 * l, 1.0, 0.0).astype(jnp.bfloat16)
-        mixings.append(
-            jnp.dot(pick, raw, preferred_element_type=jnp.float32).astype(jnp.bfloat16)
-        )
+        product = jnp.dot(picks[l], raw, preferred_element_type=jnp.float32)
+        mixings.append(product.astype(jnp.bfloat16))
     for l in range(half, layers):
         mix_out[l - half] = mixings[l]
 
@@ -187,17 +191,16 @@
 
 
 def second_half(dims, place_ref, *refs):
-    layers, seqs, tok, halo, seq_len = dims
-    state_in, mix_in, scales, gain, out, w_in, w_out = refs[16:]
+    layers, seqs, tok, halo, _ = dims
+    state_in, mix_in, scales, gain, bands, inverse, out, w_in, w_out = refs[16:]
     place = tuple(place_ref[k] for k in range(4))
-    z, y, c, x = place
+    _, _, c, x = place
     half = layers // 2
     third = ((refs[0:4], c), (refs[4:8], 1 - c))
     fourth = ((refs[8:12], c), (refs[12:16], 1 - c))
-    copy_blocks(place, third, "vzu", put_layers((0,), w_in, w_out))
-    copy_blocks(place, fourth, "zvu", put_layers((1,), w_in, w_out))
+    copy_blocks(place, third, FIRST, put_layers((0,), w_in, w_out))
+    copy_blocks(place, fourth, LAST, put_layers((1,), w_in, w_out))
     span = tok + 2 * halo
-    bands, inverse = windows(((z * NY + y) * NC + c) * tok - halo, seqs, span, seq_len)
     state = state_in[...]
     for l in range(half):
         at = half + l
@@ -222,29 +225,32 @@
             out[...] = project_out(mixed, lambda g: w_out[l, g, columns, :])
 
 
-def pack(layers, place_ref, in_ref, out_ref, mix_ref, scale_ref, act_ref, gain_ref, message, gain):
+def pack(
+    layers, place_ref, in_ref, out_ref, mix_ref, scale_ref, act_ref, gain_ref, first, last, gain
+):
     half = layers // 2
     row = 0
-    for l in range(layers):
-        message[row : row + 32, :] = in_ref[l]
-        message[row + 32 : row + 64, :] = out_ref[l]
+    for l in range(layers - 1):
+        first[row : row + 32, :] = in_ref[l]
+        first[row + 32 : row + 64, :] = out_ref[l]
         row += 64
         if l == half - 1:
             mix = jnp.concatenate([mix_ref[k].astype(jnp.float32) for k in range(layers)])
-            message[row : row + 16, :] = mix.astype(jnp.bfloat16)
+            first[row : row + 16, :] = mix.astype(jnp.bfloat16)
             row += 16
+    last[0:32, :] = in_ref[layers - 1]
+    last[32:64, :] = out_ref[layers - 1]
     scale = scale_ref[...]
     high = scale.astype(jnp.bfloat16).astype(jnp.float32)
     middle = (scale - high).astype(jnp.bfloat16).astype(jnp.float32)
     terms = jnp.concatenate([high, middle, scale - high - middle, jnp.zeros_like(scale)])
-    message[row : row + 16, :] = terms.astype(jnp.bfloat16)
-    row += 16
+    last[64:80, :] = terms.astype(jnp.bfloat16)
     seqs, tok, _ = act_ref.shape
-    own = row + place_ref[2] * (seqs * tok * 2)
+    own = 80 + place_ref[2] * (seqs * tok * 2)
     for h in range(2):
         for s in range(seqs):
             at = pl.ds(pl.multiple_of(own + (h * seqs + s) * tok, 16), tok)
-            message[at, :] = act_ref[s, :, 128 * h : 128 * (h + 1)]
+            last[at, :] = act_ref[s, :, 128 * h : 128 * (h + 1)]
     gain[...] = gain_ref[...]
 
 
@@ -255,20 +261,20 @@
     i, x = lax.axis_index("sp"), lax.axis_index("tp")
     z, y, c = i // (NY * NC), (i // NC) % NY, i % NC
     seq_len = tok * NZ * NY * NC
-    cuts = (64 * half + 16, 64 * half + 80, 64 * half + 144)
-
+    cut = 64 * half + 16
     chip_mate = send(activations, from_core())
     place = jnp.stack([z, y, c, x]).astype(jnp.int32)
     vmem = pl.BlockSpec(memory_space=pltpu.VMEM)
     smem = pl.BlockSpec(memory_space=pltpu.SMEM)
-    message, gain = pl.pallas_call(
+    first, last, gain = pl.pallas_call(
         functools.partial(pack, layers),
         out_shape=(
-            jax.ShapeDtypeStruct((cuts[2] + 16 + 4 * seqs * tok, 128), jnp.bfloat16),
+            jax.ShapeDtypeStruct((cut + 64, 128), jnp.bfloat16),
+            jax.ShapeDtypeStruct((80 + 4 * seqs * tok, 128), jnp.bfloat16),
             jax.ShapeDtypeStruct(norm_gain.shape, jnp.float32),
         ),
         in_specs=[smem] + [vmem] * 6,
-        out_specs=(vmem, vmem),
+        out_specs=(vmem, vmem, vmem),
         compiler_params=pltpu.CompilerParams(vmem_limit_bytes=2**21),
         cost_estimate=pl.CostEstimate(flops=10**6, bytes_accessed=3 * 10**5, transcendentals=0),
         name="pack",
@@ -284,34 +290,50 @@
     mate_rows = jnp.concatenate(
         [chip_mate.reshape(seqs * tok, width)[:, 128 * h : 128 * (h + 1)] for h in range(2)]
     )
-    mate_at = cuts[2] + 16 + (1 - c) * (2 * seqs * tok)
-    message = lax.dynamic_update_slice(message, mate_rows, (mate_at, 0))
-    got = [message] + [send(message, from_u(k)) for k in (1, 2, 3)]
-    ab = jnp.stack([part[: cuts[1]] for part in got])
-    q = jnp.stack([part[cuts[1] : cuts[2]] for part in got])
-    tokens = jnp.stack([part[cuts[2] :] for part in got])
+    count = 2 * seqs * tok
+    last = lax.dynamic_update_slice(last, mate_rows, (80 + (1 - c) * count, 0))
+
+    got = [first] + gather(first, FIRST, 0)
+    got_last = [last] + gather(last, LAST, 0)
+    ab = jnp.stack(got)
+    ab = [ab] + gather(ab, FIRST, 1)
+    q = jnp.stack([part[:64] for part in got_last])
+    tokens = jnp.stack([part[64:] for part in got_last])
     tokens_2 = send(tokens, from_core())
+    q = [q] + gather(q, LAST, 1)
+
+    a = jnp.stack([part[:, :cut] for part in ab])
+    a = [a] + gather(a, FIRST, 2)
+    b = jnp.stack([part[:, cut:] for part in ab])
     tokens = jnp.where(c == 0, tokens, tokens_2)
-
-    ab = [ab] + [send(ab, from_z(k)) for k in (1, 2, 3)]
-    q = [q] + [send(q, from_v(k)) for k in (1, 2, 3)]
-    count = 2 * seqs * tok
     mine = jnp.where(c == 0, tokens[:, 16 : 16 + count], tokens[:, 16 + count :])
     beside = send(mine, across_chips())
-    a = jnp.stack([part[:, : cuts[0]] for part in ab])
-    b = jnp.stack([part[:, cuts[0] :] for part in ab])
-    a = [a] + [send(a, from_v(k)) for k in (1, 2, 3)]
     q = jnp.stack(q)
-    q = [q] + [send(q, from_z(k)) for k in (1, 2, 3)]
-    b = [b] + [send(b, from_v(k)) for k in (1, 2, 3)]
-    a_2 = [send(part, from_core()) for part in a]
+    q = [q] + gather(q, LAST, 2)
+    b = [b] + gather(b, FIRST, 2)
+    a_2 = [send(a[0], from_core())]
     b_2 = [send(b[0], from_core())]
     q_2 = [send(q[0], from_core())]
+    a_2 += [send(a[1], from_core())]
+    a_2 += [send(part, from_core()) for part in a[2:]]
     b_2 += [send(part, from_core()) for part in b[1:]]
     q_2 += [send(part, from_core()) for part in q[1:]]
 
     rows = seqs * 3 * tok
     dims = (layers, seqs, tok, tok, seq_len)
+    bands, inverse, picks = pl.pallas_call(
+        functools.partial(tables, *dims),
+        out_shape=(
+            jax.ShapeDtypeStruct((4, rows, rows), jnp.bfloat16),
+            jax.ShapeDtypeStruct((4, rows, 128), jnp.float32),
+            jax.ShapeDtypeStruct((layers, 128, 512), jnp.bfloat16),
+        ),
+        in_specs=[smem],
+        out_specs=(vmem, vmem, vmem),
+        compiler_params=pltpu.CompilerParams(vmem_limit_bytes=2**22),
+        cost_estimate=pl.CostEstimate(flops=10**7, bytes_accessed=10**6, transcendentals=0),
+        name="tables",
+    )(place)
     weights = pltpu.VMEM((half, 4, 1024, 128), jnp.bfloat16)
     params = pltpu.CompilerParams(vmem_limit_bytes=14 * 2**20)
     cost = pl.CostEstimate(flops=10**9, bytes_accessed=9 * 10**6, transcendentals=1000)
@@ -322,7 +344,7 @@
             jax.ShapeDtypeStruct((layers - half, 128, 512), jnp.bfloat16),
             jax.ShapeDtypeStruct((4, layers, 128), jnp.float32),
         ),
-        in_specs=[smem] + [vmem] * 11,
+        in_specs=[smem] + [vmem] * 14,
         out_specs=(vmem, vmem, vmem),
         scratch_shapes=[
             weights,
@@ -341,11 +363,14 @@
         tokens,
         beside,
         gain,
+        bands,
+        inverse,
+        picks,
     )
     result = pl.pallas_call(
         functools.partial(second_half, dims),
         out_shape=jax.ShapeDtypeStruct((seqs * tok, width), jnp.bfloat16),
-        in_specs=[smem] + [vmem] * 20,
+        in_specs=[smem] + [vmem] * 22,
         out_specs=vmem,
         scratch_shapes=[weights, weights],
         compiler_params=params,
@@ -361,6 +386,8 @@
         mix_late,
         scales,
         gain,
+        bands,
+        inverse,
     )
     return result.reshape(seqs, tok, width)
 

time: 79 us -> 82.5 us (1.044)
  starting transfers between devices: 36.4 us -> 46.9 us
  waiting for transfers between devices: 29.4 us -> 21.1 us
  Pallas kernels: 9.69 us -> 10.9 us
    ppermute x33 -> x36, starting transfers between devices: 36.4 us -> 46.9 us  [send(): return lax.ppermute(value, AXES, perm)]
    ppermute x33 -> x36, waiting for transfers between devices: 29.4 us -> 21.1 us  [send(): return lax.ppermute(value, AXES, perm)]
    pallas_call x0 -> x1, Pallas kernels: none -> 0.95 us  [body(): pl.pallas_call(functools.partial(tables, *dims), out_shape=(jax.ShapeDtyp...]
  transfers between devices with their start and end apart: 33 -> 36, of which waited for: 12 -> 9; matrix products, arithmetic and copies ran while one was open for 1% -> 1% of each run, Pallas kernels for 6% -> 8%
where the time goes in v3:
time: 82.5 us; the launch traced here: 81.1 us
  starting transfers between devices  46.9 us (57%)
  waiting for transfers between devices  21.1 us (26%)
  Pallas kernels  10.9 us (13%)
  local copies, waits for them, and re-layouts  1.51 us (2%)
    ppermute x36, starting transfers between devices, send(): return lax.ppermute(value, AXES, perm)  46.9 us
    ppermute x36, waiting for transfers between devices, send(): return lax.ppermute(value, AXES, perm)  21.1 us
    pallas_call x1, Pallas kernels, body(): pl.pallas_call(functools.partial(second_half, dims), out_shape=jax.ShapeD...  4.8 us
    pallas_call x1, Pallas kernels, body(): pl.pallas_call(functools.partial(first_half, dims), out_shape=(jax.ShapeD...  4.61 us
  transfers between devices with their start and end apart: 36, of which 9 were waited for; matrix products, arithmetic and copies ran while one was open for 1% of the time, Pallas kernels for 8%

profile of v3, /device:TPU:0, one launch (start us, length us, event | category | flops | bytes accessed | tf_op | source)
XLA Modules:
  0.0 81.1 jit_solution(6280878287715467422)
XLA Ops:
  0.1 0.5 copy-done.5
  0.7 0.1 copy-done.2
  0.8 0.7 copy-done.3
  1.5 0.6 pack.1
  2.1 2.9 %collective-permute-start = (bf16[208,128]{1,0:T(8,128)(2,1)S(1)}, bf16[208,128]{1,0:T(8,128)(2,1)S(1)}, u32[]{:S(2)}, u32[]{:S(2)}) collective-permute-start(bf16[208,128]{1,0:T(8,128)(2,1)S(1)} %get-tuple-element.14), channel_id=1, source_target_pairs={{1,0},{2,1},{3,2},{0,3},{36,4},{37,5},{38,6},{39,7},{9,8},{10,9},{... | collective-permute-start | bytes 159752 | tf_op jit(solution)/shard_map/ppermute | solution.py:59
  5.0 0.8 collective-permute-start.1
  5.8 0.9 %collective-permute-start.2 = (bf16[208,128]{1,0:T(8,128)(2,1)S(1)}, bf16[208,128]{1,0:T(8,128)(2,1)S(1)}, u32[]{:S(2)}, u32[]{:S(2)}) collective-permute-start(bf16[208,128]{1,0:T(8,128)(2,1)S(1)} %get-tuple-element.14), channel_id=1, source_target_pairs={{3,0},{0,1},{1,2},{2,3},{100,4},{101,5},{102,6},{103,7},{11,8},{8,... | collective-permute-start | bytes 159752 | tf_op jit(solution)/shard_map/ppermute | solution.py:59
  6.8 1.9 %collective-permute-start.16 = (bf16[336,128]{1,0:T(8,128)(2,1)S(1)}, bf16[336,128]{1,0:T(8,128)(2,1)S(1)}, u32[]{:S(2)}, u32[]{:S(2)}) collective-permute-start(bf16[336,128]{1,0:T(8,128)(2,1)S(1)} %maximum_dynamic-update-slice_fusion), channel_id=1, source_target_pairs={{3,0},{0,1},{1,2},{2,3},{28,4},{29,5},{30,6},{31,7},{11,8},{8,9},{... | collective-permute-start | bytes 258056 | tf_op jit(solution)/shard_map/ppermute | solution.py:59
  8.6 2.0 %collective-permute-start.15 = (bf16[336,128]{1,0:T(8,128)(2,1)S(1)}, bf16[336,128]{1,0:T(8,128)(2,1)S(1)}, u32[]{:S(2)}, u32[]{:S(2)}) collective-permute-start(bf16[336,128]{1,0:T(8,128)(2,1)S(1)} %maximum_dynamic-update-slice_fusion), channel_id=1, source_target_pairs={{2,0},{3,1},{0,2},{1,3},{20,4},{21,5},{22,6},{23,7},{10,8},{11,9},... | collective-permute-start | bytes 258056 | tf_op jit(solution)/shard_map/ppermute | solution.py:59
  10.7 0.8 %collective-permute-start.14 = (bf16[336,128]{1,0:T(8,128)(2,1)S(1)}, bf16[336,128]{1,0:T(8,128)(2,1)S(1)}, u32[]{:S(2)}, u32[]{:S(2)}) collective-permute-start(bf16[336,128]{1,0:T(8,128)(2,1)S(1)} %maximum_dynamic-update-slice_fusion), channel_id=1, source_target_pairs={{1,0},{2,1},{3,2},{0,3},{12,4},{13,5},{14,6},{15,7},{9,8},{10,9},{... | collective-permute-start | bytes 258056 | tf_op jit(solution)/shard_map/ppermute | solution.py:59
  11.5 2.0 %collective-permute-start.5 = (bf16[4,208,128]{2,1,0:T(8,128)(2,1)S(1)}, bf16[4,208,128]{2,1,0:T(8,128)(2,1)S(1)}, u32[]{:S(2)}, u32[]{:S(2)}) collective-permute-start(bf16[4,208,128]{2,1,0:T(8,128)(2,1)S(1)} %pad_maximum_fusion.4), channel_id=1, source_target_pairs={{96,0},{97,1},{98,2},{99,3},{28,4},{29,5},{30,6},{31,7},{104,8},{1... | collective-permute-start | bytes 638984 | tf_op jit(solution)/shard_map/ppermute | solution.py:59
  13.5 2.2 %collective-permute-start.3 = (bf16[4,208,128]{2,1,0:T(8,128)(2,1)S(1)}, bf16[4,208,128]{2,1,0:T(8,128)(2,1)S(1)}, u32[]{:S(2)}, u32[]{:S(2)}) collective-permute-start(bf16[4,208,128]{2,1,0:T(8,128)(2,1)S(1)} %pad_maximum_fusion.4), channel_id=1, source_target_pairs={{32,0},{33,1},{34,2},{35,3},{12,4},{13,5},{14,6},{15,7},{40,8},{41... | collective-permute-start | bytes 638984 | tf_op jit(solution)/shard_map/ppermute | solution.py:59
  15.8 3.1 %collective-permute-start.17 = (bf16[4,64,128]{2,1,0:T(8,128)(2,1)S(1)}, bf16[4,64,128]{2,1,0:T(8,128)(2,1)S(1)}, u32[]{:S(2)}, u32[]{:S(2)}) collective-permute-start(bf16[4,64,128]{2,1,0:T(8,128)(2,1)S(1)} %get-tuple-element.24), channel_id=1, source_target_pairs={{8,0},{9,1},{10,2},{11,3},{5,4},{6,5},{7,6},{4,7},{16,8},{17,9},{1... | collective-permute-start | bytes 196616 | tf_op jit(solution)/shard_map/ppermute | solution.py:59
  18.9 0.6 collective-permute-start.18
  19.5 1.0 %collective-permute-start.19 = (bf16[4,64,128]{2,1,0:T(8,128)(2,1)S(1)}, bf16[4,64,128]{2,1,0:T(8,128)(2,1)S(1)}, u32[]{:S(2)}, u32[]{:S(2)}) collective-permute-start(bf16[4,64,128]{2,1,0:T(8,128)(2,1)S(1)} %get-tuple-element.24), channel_id=1, source_target_pairs={{24,0},{25,1},{26,2},{27,3},{7,4},{4,5},{5,6},{6,7},{0,8},{1,9},{2... | collective-permute-start | bytes 196616 | tf_op jit(solution)/shard_map/ppermute | solution.py:59
  20.6 0.2 collective-permute-done.17
  20.8 3.3 %collective-permute-start.4 = (bf16[4,208,128]{2,1,0:T(8,128)(2,1)S(1)}, bf16[4,208,128]{2,1,0:T(8,128)(2,1)S(1)}, u32[]{:S(2)}, u32[]{:S(2)}) collective-permute-start(bf16[4,208,128]{2,1,0:T(8,128)(2,1)S(1)} %pad_maximum_fusion.4), channel_id=1, source_target_pairs={{64,0},{65,1},{66,2},{67,3},{20,4},{21,5},{22,6},{23,7},{72,8},{73... | collective-permute-start | bytes 638984 | tf_op jit(solution)/shard_map/ppermute | solution.py:59
  24.1 1.4 %collective-permute-done.18 = bf16[4,64,128]{2,1,0:T(8,128)(2,1)S(1)} collective-permute-done((bf16[4,64,128]{2,1,0:T(8,128)(2,1)S(1)}, bf16[4,64,128]{2,1,0:T(8,128)(2,1)S(1)}, u32[]{:S(2)}, u32[]{:S(2)}) %collective-permute-start.18) | collective-permute-done | bytes 65568 | tf_op jit(solution)/shard_map/ppermute | solution.py:59
  25.5 1.3 %collective-permute-done.19 = bf16[4,64,128]{2,1,0:T(8,128)(2,1)S(1)} collective-permute-done((bf16[4,64,128]{2,1,0:T(8,128)(2,1)S(1)}, bf16[4,64,128]{2,1,0:T(8,128)(2,1)S(1)}, u32[]{:S(2)}, u32[]{:S(2)}) %collective-permute-start.19) | collective-permute-done | bytes 65568 | tf_op jit(solution)/shard_map/ppermute | solution.py:59
  26.8 2.5 %collective-permute-start.20 = (bf16[4,4,64,128]{3,2,1,0:T(8,128)(2,1)S(1)}, bf16[4,4,64,128]{3,2,1,0:T(8,128)(2,1)S(1)}, u32[]{:S(2)}, u32[]{:S(2)}) collective-permute-start(bf16[4,4,64,128]{3,2,1,0:T(8,128)(2,1)S(1)} %pad_maximum_fusion.3.refs_8_), channel_id=1, source_target_pairs={{32,0},{33,1},{34,2},{35,3},{36,4},{37,5},{38,6},{39,7},{40,8},{41... | collective-permute-start | bytes 786440 | tf_op jit(solution)/shard_map/ppermute | solution.py:59
  29.4 0.7 collective-permute-start.21
  30.1 1.1 %collective-permute-start.22 = (bf16[4,4,64,128]{3,2,1,0:T(8,128)(2,1)S(1)}, bf16[4,4,64,128]{3,2,1,0:T(8,128)(2,1)S(1)}, u32[]{:S(2)}, u32[]{:S(2)}) collective-permute-start(bf16[4,4,64,128]{3,2,1,0:T(8,128)(2,1)S(1)} %pad_maximum_fusion.3.refs_8_), channel_id=1, source_target_pairs={{96,0},{97,1},{98,2},{99,3},{100,4},{101,5},{102,6},{103,7},{104,8... | collective-permute-start | bytes 786440 | tf_op jit(solution)/shard_map/ppermute | solution.py:59
  31.2 0.1 collective-permute-start.23
  31.5 0.6 collective-permute-start.27
  32.2 8.4 %collective-permute-done.20.refs_9_ = bf16[4,4,64,128]{3,2,1,0:T(8,128)(2,1)S(1)} collective-permute-done((bf16[4,4,64,128]{3,2,1,0:T(8,128)(2,1)S(1)}, bf16[4,4,64,128]{3,2,1,0:T(8,128)(2,1)S(1)}, u32[]{:S(2)}, u32[]{:S(2)}) %collective-permute-start.20) | collective-permute-done | bytes 262176 | tf_op jit(solution)/shard_map/ppermute | solution.py:59
  40.6 2.9 %collective-permute-start.28 = (bf16[4,4,144,128]{3,2,1,0:T(8,128)(2,1)S(1)}, bf16[4,4,144,128]{3,2,1,0:T(8,128)(2,1)S(1)}, u32[]{:S(2)}, u32[]{:S(2)}) collective-permute-start(bf16[4,4,144,128]{3,2,1,0:T(8,128)(2,1)S(1)} %pad_maximum_fusion.refs_0_), channel_id=1, source_target_pairs={{16,0},{17,1},{18,2},{19,3},{6,4},{7,5},{4,6},{5,7},{24,8},{25,9},... | collective-permute-start | bytes 1769480 | tf_op jit(solution)/shard_map/ppermute | solution.py:59
  43.5 0.6 collective-permute-start.29
  44.2 0.1 collective-permute-done.22.refs_11_
  44.3 2.5 %collective-permute-start.6 = (bf16[4,4,64,128]{3,2,1,0:T(8,128)(2,1)S(1)}, bf16[4,4,64,128]{3,2,1,0:T(8,128)(2,1)S(1)}, u32[]{:S(2)}, u32[]{:S(2)}) collective-permute-start(bf16[4,4,64,128]{3,2,1,0:T(8,128)(2,1)S(1)} %pad_maximum_fusion.2.refs_0_), channel_id=1, source_target_pairs={{8,0},{9,1},{10,2},{11,3},{5,4},{6,5},{7,6},{4,7},{16,8},{17,9},{1... | collective-permute-start | bytes 786440 | tf_op jit(solution)/shard_map/ppermute | solution.py:59
  46.8 0.7 collective-permute-start.35
  47.5 10.3 %collective-permute-start.7 = (bf16[4,4,64,128]{3,2,1,0:T(8,128)(2,1)S(1)}, bf16[4,4,64,128]{3,2,1,0:T(8,128)(2,1)S(1)}, u32[]{:S(2)}, u32[]{:S(2)}) collective-permute-start(bf16[4,4,64,128]{3,2,1,0:T(8,128)(2,1)S(1)} %pad_maximum_fusion.2.refs_0_), channel_id=1, source_target_pairs={{16,0},{17,1},{18,2},{19,3},{6,4},{7,5},{4,6},{5,7},{24,8},{25,9},... | collective-permute-start | bytes 786440 | tf_op jit(solution)/shard_map/ppermute | solution.py:59
  57.8 4.7 %collective-permute-done.7.refs_2_ = bf16[4,4,64,128]{3,2,1,0:T(8,128)(2,1)S(1)} collective-permute-done((bf16[4,4,64,128]{3,2,1,0:T(8,128)(2,1)S(1)}, bf16[4,4,64,128]{3,2,1,0:T(8,128)(2,1)S(1)}, u32[]{:S(2)}, u32[]{:S(2)}) %collective-permute-start.7) | collective-permute-done | bytes 262176 | tf_op jit(solution)/shard_map/ppermute | solution.py:59
  62.6 0.7 collective-permute-start.30
  63.2 0.5 collective-permute-start.32
  63.7 0.1 collective-permute-start.33
  63.8 1.6 %collective-permute-done.8.refs_3_ = bf16[4,4,64,128]{3,2,1,0:T(8,128)(2,1)S(1)} collective-permute-done((bf16[4,4,64,128]{3,2,1,0:T(8,128)(2,1)S(1)}, bf16[4,4,64,128]{3,2,1,0:T(8,128)(2,1)S(1)}, u32[]{:S(2)}, u32[]{:S(2)}) %collective-permute-start.8) | collective-permute-done | bytes 262176 | tf_op jit(solution)/shard_map/ppermute | solution.py:59
  65.4 0.2 collective-permute-start.9
  65.6 2.1 %collective-permute-done.9.refs_4_ = bf16[4,4,64,128]{3,2,1,0:T(8,128)(2,1)S(1)} collective-permute-done((bf16[4,4,64,128]{3,2,1,0:T(8,128)(2,1)S(1)}, bf16[4,4,64,128]{3,2,1,0:T(8,128)(2,1)S(1)}, u32[]{:S(2)}, u32[]{:S(2)}) %collective-permute-start.9) | collective-permute-done | bytes 262176 | tf_op jit(solution)/shard_map/ppermute | solution.py:59
  67.8 0.4 collective-permute-start.24
  68.1 1.2 %collective-permute-done.24.refs_13_ = bf16[4,4,64,128]{3,2,1,0:T(8,128)(2,1)S(1)} collective-permute-done((bf16[4,4,64,128]{3,2,1,0:T(8,128)(2,1)S(1)}, bf16[4,4,64,128]{3,2,1,0:T(8,128)(2,1)S(1)}, u32[]{:S(2)}, u32[]{:S(2)}) %collective-permute-start.24) | collective-permute-done | bytes 262176 | tf_op jit(solution)/shard_map/ppermute | solution.py:59
  69.3 0.4 collective-permute-start.25
  69.7 0.1 collective-permute-start.26
  69.8 0.4 collective-permute-start.10
  70.2 0.1 collective-permute-start.11
  70.3 0.4 collective-permute-start.12
  70.7 0.9 %tables.1 = (bf16[4,192,192]{2,1,0:T(8,128)(2,1)S(1)}, f32[4,192,128]{2,1,0:T(8,128)S(1)}, bf16[4,128,512]{2,1,0:T(8,128)(2,1)S(1)}) custom-call(s32[4]{0:T(128)S(1)} %pad_add_fusion.place_ref), custom_call_target="tpu_custom_call" | custom-call | flops 10000000 | bytes 1000000 | tf_op jit(solution)/shard_map/tables/pallas_call | solution.py:324
  71.7 4.6 %first_half.1 = (bf16[192,1024]{1,0:T(8,128)(2,1)S(1)}, bf16[2,128,512]{2,1,0:T(8,128)(2,1)S(1)}, f32[4,4,128]{2,1,0:T(4,128)S(1)}) custom-call(s32[4]{0:T(128)S(1)} %pad_add_fusion.place_ref, bf16[4,4,144,128]{3,2,1,0:T(8,128)(2,1)S(1)} %pad_maximum_fusion.refs_0_, bf16[4,4,144,128]{3,2,1,0:T(8,128)(2,1)S(1)} %collective-permute-done.27.refs_1_, ...), custom_call_target="tpu_custom_call" | custom-call | flops 1000000000 | bytes 9000000 | tf_op jit(solution)/shard_map/first_half/pallas_call | solution.py:340
  76.3 4.8 %second_half.1 = bf16[64,256]{1,0:T(8,128)(2,1)} custom-call(s32[4]{0:T(128)S(1)} %pad_add_fusion.place_ref, bf16[4,4,64,128]{3,2,1,0:T(8,128)(2,1)S(1)} %pad_maximum_fusion.2.refs_0_, bf16[4,4,64,128]{3,2,1,0:T(8,128)(2,1)S(1)} %collective-permute-done.6.refs_1_, bf16[4,4,64,128]{3,2,1,0:T(8,128)(2,1)S(1)} %collective-permute-done.7.refs_2_, ...), custom_call_target="tpu_custom_call" | custom-call | flops 1000000000 | bytes 9000000 | tf_op jit(solution)/shard_map/second_half/pallas_call | solution.py:370
  (67 shorter events, 0.6 us)
Async XLA Ops:
  0.0 6.7 %collective-permute-start.13 = (bf16[2,32,256]{2,1,0:T(8,128)(2,1)}, bf16[2,32,256]{2,1,0:T(8,128)(2,1)S(1)}, u32[]{:S(2)}, u32[]{:S(2)}) collective-permute-start(bf16[2,32,256]{2,1,0:T(8,128)(2,1)} %act_ref.1), channel_id=1, source_target_pairs={{4,0},{5,1},{6,2},{7,3},{0,4},{1,5},{2,6},{3,7},{12,8},{13,9},{14,... | collective-permute-start | bytes 98312 | tf_op jit(solution)/shard_map/ppermute | solution.py:59
  0.0 0.7 copy-start.5
  0.0 0.7 copy-start.4
  0.0 0.8 copy-start.2
  0.0 0.8 copy-start.1
  0.0 0.8 copy-start
  0.8 0.7 copy-start.3
  2.1 8.5 %collective-permute-start = (bf16[208,128]{1,0:T(8,128)(2,1)S(1)}, bf16[208,128]{1,0:T(8,128)(2,1)S(1)}, u32[]{:S(2)}, u32[]{:S(2)}) collective-permute-start(bf16[208,128]{1,0:T(8,128)(2,1)S(1)} %get-tuple-element.14), channel_id=1, source_target_pairs={{1,0},{2,1},{3,2},{0,3},{36,4},{37,5},{38,6},{39,7},{9,8},{10,9},{... | collective-permute-start | bytes 159752 | tf_op jit(solution)/shard_map/ppermute | solution.py:59
  5.0 6.4 %collective-permute-start.1 = (bf16[208,128]{1,0:T(8,128)(2,1)S(1)}, bf16[208,128]{1,0:T(8,128)(2,1)S(1)}, u32[]{:S(2)}, u32[]{:S(2)}) collective-permute-start(bf16[208,128]{1,0:T(8,128)(2,1)S(1)} %get-tuple-element.14), channel_id=1, source_target_pairs={{2,0},{3,1},{0,2},{1,3},{68,4},{69,5},{70,6},{71,7},{10,8},{11,9},... | collective-permute-start | bytes 159752 | tf_op jit(solution)/shard_map/ppermute | solution.py:59
  5.8 5.6 %collective-permute-start.2 = (bf16[208,128]{1,0:T(8,128)(2,1)S(1)}, bf16[208,128]{1,0:T(8,128)(2,1)S(1)}, u32[]{:S(2)}, u32[]{:S(2)}) collective-permute-start(bf16[208,128]{1,0:T(8,128)(2,1)S(1)} %get-tuple-element.14), channel_id=1, source_target_pairs={{3,0},{0,1},{1,2},{2,3},{100,4},{101,5},{102,6},{103,7},{11,8},{8,... | collective-permute-start | bytes 159752 | tf_op jit(solution)/shard_map/ppermute | solution.py:59
  6.8 9.0 %collective-permute-start.16 = (bf16[336,128]{1,0:T(8,128)(2,1)S(1)}, bf16[336,128]{1,0:T(8,128)(2,1)S(1)}, u32[]{:S(2)}, u32[]{:S(2)}) collective-permute-start(bf16[336,128]{1,0:T(8,128)(2,1)S(1)} %maximum_dynamic-update-slice_fusion), channel_id=1, source_target_pairs={{3,0},{0,1},{1,2},{2,3},{28,4},{29,5},{30,6},{31,7},{11,8},{8,9},{... | collective-permute-start | bytes 258056 | tf_op jit(solution)/shard_map/ppermute | solution.py:59
  8.6 7.1 %collective-permute-start.15 = (bf16[336,128]{1,0:T(8,128)(2,1)S(1)}, bf16[336,128]{1,0:T(8,128)(2,1)S(1)}, u32[]{:S(2)}, u32[]{:S(2)}) collective-permute-start(bf16[336,128]{1,0:T(8,128)(2,1)S(1)} %maximum_dynamic-update-slice_fusion), channel_id=1, source_target_pairs={{2,0},{3,1},{0,2},{1,3},{20,4},{21,5},{22,6},{23,7},{10,8},{11,9},... | collective-permute-start | bytes 258056 | tf_op jit(solution)/shard_map/ppermute | solution.py:59
  10.7 5.1 %collective-permute-start.14 = (bf16[336,128]{1,0:T(8,128)(2,1)S(1)}, bf16[336,128]{1,0:T(8,128)(2,1)S(1)}, u32[]{:S(2)}, u32[]{:S(2)}) collective-permute-start(bf16[336,128]{1,0:T(8,128)(2,1)S(1)} %maximum_dynamic-update-slice_fusion), channel_id=1, source_target_pairs={{1,0},{2,1},{3,2},{0,3},{12,4},{13,5},{14,6},{15,7},{9,8},{10,9},{... | collective-permute-start | bytes 258056 | tf_op jit(solution)/shard_map/ppermute | solution.py:59
  11.5 18.6 %collective-permute-start.5 = (bf16[4,208,128]{2,1,0:T(8,128)(2,1)S(1)}, bf16[4,208,128]{2,1,0:T(8,128)(2,1)S(1)}, u32[]{:S(2)}, u32[]{:S(2)}) collective-permute-start(bf16[4,208,128]{2,1,0:T(8,128)(2,1)S(1)} %pad_maximum_fusion.4), channel_id=1, source_target_pairs={{96,0},{97,1},{98,2},{99,3},{28,4},{29,5},{30,6},{31,7},{104,8},{1... | collective-permute-start | bytes 638984 | tf_op jit(solution)/shard_map/ppermute | solution.py:59
  13.5 15.8 %collective-permute-start.3 = (bf16[4,208,128]{2,1,0:T(8,128)(2,1)S(1)}, bf16[4,208,128]{2,1,0:T(8,128)(2,1)S(1)}, u32[]{:S(2)}, u32[]{:S(2)}) collective-permute-start(bf16[4,208,128]{2,1,0:T(8,128)(2,1)S(1)} %pad_maximum_fusion.4), channel_id=1, source_target_pairs={{32,0},{33,1},{34,2},{35,3},{12,4},{13,5},{14,6},{15,7},{40,8},{41... | collective-permute-start | bytes 638984 | tf_op jit(solution)/shard_map/ppermute | solution.py:59
  15.8 5.0 %collective-permute-start.17 = (bf16[4,64,128]{2,1,0:T(8,128)(2,1)S(1)}, bf16[4,64,128]{2,1,0:T(8,128)(2,1)S(1)}, u32[]{:S(2)}, u32[]{:S(2)}) collective-permute-start(bf16[4,64,128]{2,1,0:T(8,128)(2,1)S(1)} %get-tuple-element.24), channel_id=1, source_target_pairs={{8,0},{9,1},{10,2},{11,3},{5,4},{6,5},{7,6},{4,7},{16,8},{17,9},{1... | collective-permute-start | bytes 196616 | tf_op jit(solution)/shard_map/ppermute | solution.py:59
  18.9 6.6 %collective-permute-start.18 = (bf16[4,64,128]{2,1,0:T(8,128)(2,1)S(1)}, bf16[4,64,128]{2,1,0:T(8,128)(2,1)S(1)}, u32[]{:S(2)}, u32[]{:S(2)}) collective-permute-start(bf16[4,64,128]{2,1,0:T(8,128)(2,1)S(1)} %get-tuple-element.24), channel_id=1, source_target_pairs={{16,0},{17,1},{18,2},{19,3},{6,4},{7,5},{4,6},{5,7},{24,8},{25,9},... | collective-permute-start | bytes 196616 | tf_op jit(solution)/shard_map/ppermute | solution.py:59
  19.5 7.2 %collective-permute-start.19 = (bf16[4,64,128]{2,1,0:T(8,128)(2,1)S(1)}, bf16[4,64,128]{2,1,0:T(8,128)(2,1)S(1)}, u32[]{:S(2)}, u32[]{:S(2)}) collective-permute-start(bf16[4,64,128]{2,1,0:T(8,128)(2,1)S(1)} %get-tuple-element.24), channel_id=1, source_target_pairs={{24,0},{25,1},{26,2},{27,3},{7,4},{4,5},{5,6},{6,7},{0,8},{1,9},{2... | collective-permute-start | bytes 196616 | tf_op jit(solution)/shard_map/ppermute | solution.py:59
  20.8 10.4 %collective-permute-start.4 = (bf16[4,208,128]{2,1,0:T(8,128)(2,1)S(1)}, bf16[4,208,128]{2,1,0:T(8,128)(2,1)S(1)}, u32[]{:S(2)}, u32[]{:S(2)}) collective-permute-start(bf16[4,208,128]{2,1,0:T(8,128)(2,1)S(1)} %pad_maximum_fusion.4), channel_id=1, source_target_pairs={{64,0},{65,1},{66,2},{67,3},{20,4},{21,5},{22,6},{23,7},{72,8},{73... | collective-permute-start | bytes 638984 | tf_op jit(solution)/shard_map/ppermute | solution.py:59
  25.5 6.0 %collective-permute-start.34 = (bf16[4,272,128]{2,1,0:T(8,128)(2,1)S(1)}, bf16[4,272,128]{2,1,0:T(8,128)(2,1)S(1)}, u32[]{:S(2)}, u32[]{:S(2)}) collective-permute-start(bf16[4,272,128]{2,1,0:T(8,128)(2,1)S(1)} %pad_maximum_fusion.1), channel_id=1, source_target_pairs={{4,0},{5,1},{6,2},{7,3},{0,4},{1,5},{2,6},{3,7},{12,8},{13,9},{14,... | collective-permute-start | bytes 835592 | tf_op jit(solution)/shard_map/ppermute | solution.py:59
  26.8 13.8 %collective-permute-start.20 = (bf16[4,4,64,128]{3,2,1,0:T(8,128)(2,1)S(1)}, bf16[4,4,64,128]{3,2,1,0:T(8,128)(2,1)S(1)}, u32[]{:S(2)}, u32[]{:S(2)}) collective-permute-start(bf16[4,4,64,128]{3,2,1,0:T(8,128)(2,1)S(1)} %pad_maximum_fusion.3.refs_8_), channel_id=1, source_target_pairs={{32,0},{33,1},{34,2},{35,3},{36,4},{37,5},{38,6},{39,7},{40,8},{41... | collective-permute-start | bytes 786440 | tf_op jit(solution)/shard_map/ppermute | solution.py:59
  29.4 14.2 %collective-permute-start.21 = (bf16[4,4,64,128]{3,2,1,0:T(8,128)(2,1)S(1)}, bf16[4,4,64,128]{3,2,1,0:T(8,128)(2,1)S(1)}, u32[]{:S(2)}, u32[]{:S(2)}) collective-permute-start(bf16[4,4,64,128]{3,2,1,0:T(8,128)(2,1)S(1)} %pad_maximum_fusion.3.refs_8_), channel_id=1, source_target_pairs={{64,0},{65,1},{66,2},{67,3},{68,4},{69,5},{70,6},{71,7},{72,8},{73... | collective-permute-start | bytes 786440 | tf_op jit(solution)/shard_map/ppermute | solution.py:59
  30.1 14.2 %collective-permute-start.22 = (bf16[4,4,64,128]{3,2,1,0:T(8,128)(2,1)S(1)}, bf16[4,4,64,128]{3,2,1,0:T(8,128)(2,1)S(1)}, u32[]{:S(2)}, u32[]{:S(2)}) collective-permute-start(bf16[4,4,64,128]{3,2,1,0:T(8,128)(2,1)S(1)} %pad_maximum_fusion.3.refs_8_), channel_id=1, source_target_pairs={{96,0},{97,1},{98,2},{99,3},{100,4},{101,5},{102,6},{103,7},{104,8... | collective-permute-start | bytes 786440 | tf_op jit(solution)/shard_map/ppermute | solution.py:59
  31.2 15.6 %collective-permute-start.23 = (bf16[4,4,64,128]{3,2,1,0:T(8,128)(2,1)S(1)}, bf16[4,4,64,128]{3,2,1,0:T(8,128)(2,1)S(1)}, u32[]{:S(2)}, u32[]{:S(2)}) collective-permute-start(bf16[4,4,64,128]{3,2,1,0:T(8,128)(2,1)S(1)} %pad_maximum_fusion.3.refs_8_), channel_id=1, source_target_pairs={{4,0},{5,1},{6,2},{7,3},{0,4},{1,5},{2,6},{3,7},{12,8},{13,9},{14,... | collective-permute-start | bytes 786440 | tf_op jit(solution)/shard_map/ppermute | solution.py:59
  31.5 31.7 %collective-permute-start.27 = (bf16[4,4,144,128]{3,2,1,0:T(8,128)(2,1)S(1)}, bf16[4,4,144,128]{3,2,1,0:T(8,128)(2,1)S(1)}, u32[]{:S(2)}, u32[]{:S(2)}) collective-permute-start(bf16[4,4,144,128]{3,2,1,0:T(8,128)(2,1)S(1)} %pad_maximum_fusion.refs_0_), channel_id=1, source_target_pairs={{8,0},{9,1},{10,2},{11,3},{5,4},{6,5},{7,6},{4,7},{16,8},{17,9},{1... | collective-permute-start | bytes 1769480 | tf_op jit(solution)/shard_map/ppermute | solution.py:59
  40.6 22.6 %collective-permute-start.28 = (bf16[4,4,144,128]{3,2,1,0:T(8,128)(2,1)S(1)}, bf16[4,4,144,128]{3,2,1,0:T(8,128)(2,1)S(1)}, u32[]{:S(2)}, u32[]{:S(2)}) collective-permute-start(bf16[4,4,144,128]{3,2,1,0:T(8,128)(2,1)S(1)} %pad_maximum_fusion.refs_0_), channel_id=1, source_target_pairs={{16,0},{17,1},{18,2},{19,3},{6,4},{7,5},{4,6},{5,7},{24,8},{25,9},... | collective-permute-start | bytes 1769480 | tf_op jit(solution)/shard_map/ppermute | solution.py:59
  43.5 20.2 %collective-permute-start.29 = (bf16[4,4,144,128]{3,2,1,0:T(8,128)(2,1)S(1)}, bf16[4,4,144,128]{3,2,1,0:T(8,128)(2,1)S(1)}, u32[]{:S(2)}, u32[]{:S(2)}) collective-permute-start(bf16[4,4,144,128]{3,2,1,0:T(8,128)(2,1)S(1)} %pad_maximum_fusion.refs_0_), channel_id=1, source_target_pairs={{24,0},{25,1},{26,2},{27,3},{7,4},{4,5},{5,6},{6,7},{0,8},{1,9},{2... | collective-permute-start | bytes 1769480 | tf_op jit(solution)/shard_map/ppermute | solution.py:59
  44.3 13.6 %collective-permute-start.6 = (bf16[4,4,64,128]{3,2,1,0:T(8,128)(2,1)S(1)}, bf16[4,4,64,128]{3,2,1,0:T(8,128)(2,1)S(1)}, u32[]{:S(2)}, u32[]{:S(2)}) collective-permute-start(bf16[4,4,64,128]{3,2,1,0:T(8,128)(2,1)S(1)} %pad_maximum_fusion.2.refs_0_), channel_id=1, source_target_pairs={{8,0},{9,1},{10,2},{11,3},{5,4},{6,5},{7,6},{4,7},{16,8},{17,9},{1... | collective-permute-start | bytes 786440 | tf_op jit(solution)/shard_map/ppermute | solution.py:59
  46.8 0.7 collective-permute-start.35
  47.5 15.1 %collective-permute-start.7 = (bf16[4,4,64,128]{3,2,1,0:T(8,128)(2,1)S(1)}, bf16[4,4,64,128]{3,2,1,0:T(8,128)(2,1)S(1)}, u32[]{:S(2)}, u32[]{:S(2)}) collective-permute-start(bf16[4,4,64,128]{3,2,1,0:T(8,128)(2,1)S(1)} %pad_maximum_fusion.2.refs_0_), channel_id=1, source_target_pairs={{16,0},{17,1},{18,2},{19,3},{6,4},{7,5},{4,6},{5,7},{24,8},{25,9},... | collective-permute-start | bytes 786440 | tf_op jit(solution)/shard_map/ppermute | solution.py:59
  57.8 7.6 %collective-permute-start.8 = (bf16[4,4,64,128]{3,2,1,0:T(8,128)(2,1)S(1)}, bf16[4,4,64,128]{3,2,1,0:T(8,128)(2,1)S(1)}, u32[]{:S(2)}, u32[]{:S(2)}) collective-permute-start(bf16[4,4,64,128]{3,2,1,0:T(8,128)(2,1)S(1)} %pad_maximum_fusion.2.refs_0_), channel_id=1, source_target_pairs={{24,0},{25,1},{26,2},{27,3},{7,4},{4,5},{5,6},{6,7},{0,8},{1,9},{2... | collective-permute-start | bytes 786440 | tf_op jit(solution)/shard_map/ppermute | solution.py:59
  62.6 7.1 %collective-permute-start.30 = (bf16[4,4,144,128]{3,2,1,0:T(8,128)(2,1)S(1)}, bf16[4,4,144,128]{3,2,1,0:T(8,128)(2,1)S(1)}, u32[]{:S(2)}, u32[]{:S(2)}) collective-permute-start(bf16[4,4,144,128]{3,2,1,0:T(8,128)(2,1)S(1)} %pad_maximum_fusion.refs_0_), channel_id=1, source_target_pairs={{4,0},{5,1},{6,2},{7,3},{0,4},{1,5},{2,6},{3,7},{12,8},{13,9},{14,... | collective-permute-start | bytes 1769480 | tf_op jit(solution)/shard_map/ppermute | solution.py:59
  63.2 6.6 %collective-permute-start.31 = (bf16[4,4,144,128]{3,2,1,0:T(8,128)(2,1)S(1)}, bf16[4,4,144,128]{3,2,1,0:T(8,128)(2,1)S(1)}, u32[]{:S(2)}, u32[]{:S(2)}) collective-permute-start(bf16[4,4,144,128]{3,2,1,0:T(8,128)(2,1)S(1)} %collective-permute-done.27.refs_1_), channel_id=1, source_target_pairs={{4,0},{5,1},{6,2},{7,3},{0,4},{1,5},{2,6},{3,7},{12,8},{13,9},{14,... | collective-permute-start | bytes 1769480 | tf_op jit(solution)/shard_map/ppermute | solution.py:59
  63.2 7.0 %collective-permute-start.32 = (bf16[4,4,144,128]{3,2,1,0:T(8,128)(2,1)S(1)}, bf16[4,4,144,128]{3,2,1,0:T(8,128)(2,1)S(1)}, u32[]{:S(2)}, u32[]{:S(2)}) collective-permute-start(bf16[4,4,144,128]{3,2,1,0:T(8,128)(2,1)S(1)} %collective-permute-done.28.refs_2_), channel_id=1, source_target_pairs={{4,0},{5,1},{6,2},{7,3},{0,4},{1,5},{2,6},{3,7},{12,8},{13,9},{14,... | collective-permute-start | bytes 1769480 | tf_op jit(solution)/shard_map/ppermute | solution.py:59
  63.7 6.6 %collective-permute-start.33 = (bf16[4,4,144,128]{3,2,1,0:T(8,128)(2,1)S(1)}, bf16[4,4,144,128]{3,2,1,0:T(8,128)(2,1)S(1)}, u32[]{:S(2)}, u32[]{:S(2)}) collective-permute-start(bf16[4,4,144,128]{3,2,1,0:T(8,128)(2,1)S(1)} %collective-permute-done.29.refs_3_), channel_id=1, source_target_pairs={{4,0},{5,1},{6,2},{7,3},{0,4},{1,5},{2,6},{3,7},{12,8},{13,9},{14,... | collective-permute-start | bytes 1769480 | tf_op jit(solution)/shard_map/ppermute | solution.py:59
  65.4 2.3 %collective-permute-start.9 = (bf16[4,4,64,128]{3,2,1,0:T(8,128)(2,1)S(1)}, bf16[4,4,64,128]{3,2,1,0:T(8,128)(2,1)S(1)}, u32[]{:S(2)}, u32[]{:S(2)}) collective-permute-start(bf16[4,4,64,128]{3,2,1,0:T(8,128)(2,1)S(1)} %pad_maximum_fusion.2.refs_0_), channel_id=1, source_target_pairs={{4,0},{5,1},{6,2},{7,3},{0,4},{1,5},{2,6},{3,7},{12,8},{13,9},{14,... | collective-permute-start | bytes 786440 | tf_op jit(solution)/shard_map/ppermute | solution.py:59
  67.8 1.5 %collective-permute-start.24 = (bf16[4,4,64,128]{3,2,1,0:T(8,128)(2,1)S(1)}, bf16[4,4,64,128]{3,2,1,0:T(8,128)(2,1)S(1)}, u32[]{:S(2)}, u32[]{:S(2)}) collective-permute-start(bf16[4,4,64,128]{3,2,1,0:T(8,128)(2,1)S(1)} %collective-permute-done.20.refs_9_), channel_id=1, source_target_pairs={{4,0},{5,1},{6,2},{7,3},{0,4},{1,5},{2,6},{3,7},{12,8},{13,9},{14,... | collective-permute-start | bytes 786440 | tf_op jit(solution)/shard_map/ppermute | solution.py:59
  69.3 7.0 %collective-permute-start.25 = (bf16[4,4,64,128]{3,2,1,0:T(8,128)(2,1)S(1)}, bf16[4,4,64,128]{3,2,1,0:T(8,128)(2,1)S(1)}, u32[]{:S(2)}, u32[]{:S(2)}) collective-permute-start(bf16[4,4,64,128]{3,2,1,0:T(8,128)(2,1)S(1)} %collective-permute-done.21.refs_10_), channel_id=1, source_target_pairs={{4,0},{5,1},{6,2},{7,3},{0,4},{1,5},{2,6},{3,7},{12,8},{13,9},{14,... | collective-permute-start | bytes 786440 | tf_op jit(solution)/shard_map/ppermute | solution.py:59
  69.7 6.6 %collective-permute-start.26 = (bf16[4,4,64,128]{3,2,1,0:T(8,128)(2,1)S(1)}, bf16[4,4,64,128]{3,2,1,0:T(8,128)(2,1)S(1)}, u32[]{:S(2)}, u32[]{:S(2)}) collective-permute-start(bf16[4,4,64,128]{3,2,1,0:T(8,128)(2,1)S(1)} %collective-permute-done.22.refs_11_), channel_id=1, source_target_pairs={{4,0},{5,1},{6,2},{7,3},{0,4},{1,5},{2,6},{3,7},{12,8},{13,9},{14,... | collective-permute-start | bytes 786440 | tf_op jit(solution)/shard_map/ppermute | solution.py:59
  69.8 6.5 %collective-permute-start.10 = (bf16[4,4,64,128]{3,2,1,0:T(8,128)(2,1)S(1)}, bf16[4,4,64,128]{3,2,1,0:T(8,128)(2,1)S(1)}, u32[]{:S(2)}, u32[]{:S(2)}) collective-permute-start(bf16[4,4,64,128]{3,2,1,0:T(8,128)(2,1)S(1)} %collective-permute-done.6.refs_1_), channel_id=1, source_target_pairs={{4,0},{5,1},{6,2},{7,3},{0,4},{1,5},{2,6},{3,7},{12,8},{13,9},{14,... | collective-permute-start | bytes 786440 | tf_op jit(solution)/shard_map/ppermute | solution.py:59
  70.2 6.1 %collective-permute-start.11 = (bf16[4,4,64,128]{3,2,1,0:T(8,128)(2,1)S(1)}, bf16[4,4,64,128]{3,2,1,0:T(8,128)(2,1)S(1)}, u32[]{:S(2)}, u32[]{:S(2)}) collective-permute-start(bf16[4,4,64,128]{3,2,1,0:T(8,128)(2,1)S(1)} %collective-permute-done.7.refs_2_), channel_id=1, source_target_pairs={{4,0},{5,1},{6,2},{7,3},{0,4},{1,5},{2,6},{3,7},{12,8},{13,9},{14,... | collective-permute-start | bytes 786440 | tf_op jit(solution)/shard_map/ppermute | solution.py:59
  70.3 6.0 %collective-permute-start.12 = (bf16[4,4,64,128]{3,2,1,0:T(8,128)(2,1)S(1)}, bf16[4,4,64,128]{3,2,1,0:T(8,128)(2,1)S(1)}, u32[]{:S(2)}, u32[]{:S(2)}) collective-permute-start(bf16[4,4,64,128]{3,2,1,0:T(8,128)(2,1)S(1)} %collective-permute-done.8.refs_3_), channel_id=1, source_target_pairs={{4,0},{5,1},{6,2},{7,3},{0,4},{1,5},{2,6},{3,7},{12,8},{13,9},{14,... | collective-permute-start | bytes 786440 | tf_op jit(solution)/shard_map/ppermute | solution.py:59

commit v4 on v3

v4 whole, which is shorter than its diff:
```python
import functools

import jax
import jax.numpy as jnp
from jax import lax
from jax.experimental import pallas as pl
from jax.experimental.pallas import tpu as pltpu
from jax.sharding import PartitionSpec as P

NZ, NY, NC, NX = 4, 4, 2, 4
AXES = ("sp", "tp")


def flat(z, y, c, x):
    return (((z % NZ) * NY + y % NY) * NC + c) * NX + x % NX


def pairs(source_of):
    return [
        (flat(*source_of(z, y, c, x)), flat(z, y, c, x))
        for z in range(NZ)
        for y in range(NY)
        for c in range(NC)
        for x in range(NX)
    ]


FIRST = ("xzy", "zyx")
LAST = ("xyz", "yxz")


def along(order, step, k):
    def source(z, y, c, x):
        at = dict(z=z, y=y, x=x)
        at[order[c][step]] += k
        return at["z"], at["y"], c, at["x"]

    return pairs(source)


def gather(value, order, step):
    return [send(value, along(order, step, k)) for k in (1, 2, 3)]


def from_core():
    return pairs(lambda z, y, c, x: (z, y, 1 - c, x))


def across_chips():
    count = NZ * NY * NC
    swap = []
    for low in range(1, count - 1, 2):
        for x in range(NX):
            swap += [(low * NX + x, (low + 1) * NX + x), ((low + 1) * NX + x, low * NX + x)]
    return swap


def send(value, perm):
    return lax.ppermute(value, AXES, perm)


def copy_blocks(place, sources, order, copy):
    z, y, _, x = place
    for parts, core in sources:
        first = core == 0
        for k in range(4):
            for m in range(4):
                for j in range(4):
                    north, south = (dict(zip(axes, (j, m, k))) for axes in order)
                    y_at = lax.rem(y + jnp.where(first, north["y"], south["y"]), NY)
                    x_at = lax.rem(x + jnp.where(first, north["x"], south["x"]), NX)
                    z_at = lax.rem(z + jnp.where(first, north["z"], south["z"]), NZ)
                    copy(x_at, z_at * (NY * NC) + y_at * NC + core, parts[k].at[m, j])


def put_layers(layers, w_in, w_out, mix_raw=None):
    def copy(x_at, index, part):
        rows = pl.ds(pl.multiple_of(index * 32, 32), 32)
        for at, l in enumerate(layers):
            w_in[l, x_at, rows, :] = part[64 * at : 64 * at + 32, :]
            w_out[l, x_at, rows, :] = part[64 * at + 32 : 64 * at + 64, :]
        if mix_raw is not None:
            end = 64 * len(layers)
            mix_rows = pl.ds(pl.multiple_of(index * 16, 16), 16)
            mix_raw[x_at, mix_rows, :] = part[end : end + 16, :]

    return copy


def tables(layers, seqs, tok, halo, seq_len, place_ref, *refs):
    z, y, c = (place_ref[k] for k in range(3))
    first = ((z * NY + y) * NC + c) * tok
    for beside, bands, inverse in ((halo, *refs[0:2]), (halo // 2, *refs[2:4])):
        start = first - beside
        span = tok + 2 * beside
        rows = seqs * span
        r = lax.broadcasted_iota(jnp.int32, (rows, rows), 0)
        q = lax.broadcasted_iota(jnp.int32, (rows, rows), 1)
        same = (r >= span) == (q >= span)
        pos_r = start + jnp.where(r >= span, r - span, r)
        pos_q = start + jnp.where(q >= span, q - span, q)
        r1 = lax.broadcasted_iota(jnp.int32, (rows, 128), 0)
        pos_1 = start + jnp.where(r1 >= span, r1 - span, r1)
        for g in range(4):
            half = 2**g
            low = jnp.clip(pos_r - half, 0, seq_len)
            high = jnp.clip(pos_r + half, 0, seq_len)
            inside = same & (pos_q >= low) & (pos_q < high)
            bands[g] = jnp.where(inside, 1.0, 0.0).astype(jnp.bfloat16)
            count = jnp.clip(pos_1 + half, 0, seq_len) - jnp.clip(pos_1 - half, 0, seq_len)
            inverse[g] = 1.0 / jnp.maximum(count, 1).astype(jnp.float32)
    picks = refs[4]
    pick_r = lax.broadcasted_iota(jnp.int32, (128, 512), 0)
    pick_q = lax.broadcasted_iota(jnp.int32, (128, 512), 1)
    base = ((pick_r >> 2) << 4) + (pick_r & 3)
    for l in range(layers):
        picks[l] = jnp.where(pick_q == base + 4 * l, 1.0, 0.0).astype(jnp.bfloat16)


def mix_layer(state, gain, w_in, scales, mixing, bands, inverse):
    mean = jnp.mean(state * state, axis=-1, keepdims=True)
    normed = (state * lax.rsqrt(mean + 1e-06) * gain).astype(jnp.bfloat16)
    weights = jnp.concatenate([w_in[g] for g in range(4)], axis=1)
    pooled = jnp.dot(normed, weights, preferred_element_type=jnp.float32).astype(jnp.bfloat16)
    mixed = []
    for g in range(4):
        part = pooled[:, 128 * g : 128 * (g + 1)]
        sums = jnp.dot(bands[g], part, preferred_element_type=jnp.float32)
        centred = (sums * inverse[g] - part.astype(jnp.float32)).astype(jnp.bfloat16)
        product = jnp.dot(
            centred, mixing[:, 128 * g : 128 * (g + 1)], preferred_element_type=jnp.float32
        )
        mixed.append((product * scales[g]).astype(jnp.bfloat16))
    return jnp.concatenate(mixed, axis=1)


def project_out(mixed, w_out):
    weights = jnp.concatenate([w_out(g) for g in range(4)], axis=1)
    out = lax.dot_general(
        mixed, weights, (((1,), (1,)), ((), ())), preferred_element_type=jnp.float32
    )
    return out.astype(jnp.bfloat16)


def inner(rows, seqs, cut):
    span = rows.shape[0] // seqs
    return jnp.concatenate([rows[s * span + cut : (s + 1) * span - cut] for s in range(seqs)])


def all_layers(dims, place_ref, *refs):
    layers, seqs, tok, halo, _ = dims
    acts, beside, gain = refs[16:19]
    wide, narrow, picks, out = refs[19:21], refs[21:23], refs[23], refs[24]
    w_in, w_out, mix_raw, state_parts, scales = refs[25:]
    place = tuple(place_ref[k] for k in range(4))
    _, _, c, x = place
    span = tok + 2 * halo
    for k in range(4):
        x_at = lax.rem(x + k, NX)
        for h in range(2):
            lanes = slice(128 * h, 128 * (h + 1))
            for s in range(seqs):
                for core in range(NC):
                    low = 16 + ((core * 2 + h) * seqs + s) * tok
                    at = pl.ds(pl.multiple_of(s * span + (1 + core - c) * tok, tok), tok)
                    state_parts[x_at, at, lanes] = acts[k, low : low + tok, :]
                low = (h * seqs + s) * tok
                at = pl.ds(pl.multiple_of(s * span + 2 * c * tok, tok), tok)
                state_parts[x_at, at, lanes] = beside[k, low : low + tok, :]
        parts = acts[k, 0:16, :].astype(jnp.float32)
        scales[x_at] = parts[0:layers] + parts[layers : 2 * layers] + parts[2 * layers : 3 * layers]
    put = put_layers(range(layers - 1), w_in, w_out, mix_raw)
    copy_blocks(place, ((refs[0:4], c), (refs[4:8], 1 - c)), FIRST, put)
    put = put_layers((layers - 1,), w_in, w_out)
    copy_blocks(place, ((refs[8:12], c), (refs[12:16], 1 - c)), LAST, put)

    raw = jnp.concatenate([mix_raw[g] for g in range(4)], axis=1)
    state = jnp.concatenate([state_parts[k] for k in range(4)], axis=1)
    for l in range(layers):
        mixing = jnp.dot(picks[l], raw, preferred_element_type=jnp.float32).astype(jnp.bfloat16)
        bands, inverse = wide if l < layers // 2 else narrow
        mixed = mix_layer(
            state.astype(jnp.float32),
            gain[l : l + 1, :],
            [w_in[l, g] for g in range(4)],
            [scales[g, l : l + 1, :] for g in range(4)],
            mixing,
            bands,
            inverse,
        )
        if l == layers // 2 - 1:
            mixed = inner(mixed, seqs, halo // 2)
        if l < layers - 1:
            state = project_out(mixed, lambda g: w_out[l, g])
        else:
            width = out.shape[-1]
            columns = pl.ds(pl.multiple_of(x * width, width), width)
            mixed = inner(mixed, seqs, halo // 2)
            out[...] = project_out(mixed, lambda g: w_out[l, g, columns, :])


def pack(
    layers, place_ref, in_ref, out_ref, mix_ref, scale_ref, act_ref, gain_ref, first, last, gain
):
    for l in range(layers - 1):
        first[64 * l : 64 * l + 32, :] = in_ref[l]
        first[64 * l + 32 : 64 * l + 64, :] = out_ref[l]
    mix = jnp.concatenate([mix_ref[k].astype(jnp.float32) for k in range(layers)])
    first[64 * layers - 64 : 64 * layers - 48, :] = mix.astype(jnp.bfloat16)
    last[0:32, :] = in_ref[layers - 1]
    last[32:64, :] = out_ref[layers - 1]
    scale = scale_ref[...]
    high = scale.astype(jnp.bfloat16).astype(jnp.float32)
    middle = (scale - high).astype(jnp.bfloat16).astype(jnp.float32)
    terms = jnp.concatenate([high, middle, scale - high - middle, jnp.zeros_like(scale)])
    last[64:80, :] = terms.astype(jnp.bfloat16)
    seqs, tok, _ = act_ref.shape
    own = 80 + place_ref[2] * (seqs * tok * 2)
    for h in range(2):
        for s in range(seqs):
            at = pl.ds(pl.multiple_of(own + (h * seqs + s) * tok, 16), tok)
            last[at, :] = act_ref[s, :, 128 * h : 128 * (h + 1)]
    gain[...] = gain_ref[...]


def body(activations, norm_gain, in_weight, out_weight, mixing, pool_scale):
    layers = in_weight.shape[0]
    seqs, tok, width = activations.shape
    i, x = lax.axis_index("sp"), lax.axis_index("tp")
    z, y, c = i // (NY * NC), (i // NC) % NY, i % NC
    seq_len = tok * NZ * NY * NC
    chip_mate = send(activations, from_core())
    place = jnp.stack([z, y, c, x]).astype(jnp.int32)
    vmem = pl.BlockSpec(memory_space=pltpu.VMEM)
    smem = pl.BlockSpec(memory_space=pltpu.SMEM)
    first, last, gain = pl.pallas_call(
        functools.partial(pack, layers),
        out_shape=(
            jax.ShapeDtypeStruct((64 * layers - 48, 128), jnp.bfloat16),
            jax.ShapeDtypeStruct((80 + 4 * seqs * tok, 128), jnp.bfloat16),
            jax.ShapeDtypeStruct(norm_gain.shape, jnp.float32),
        ),
        in_specs=[smem] + [vmem] * 6,
        out_specs=(vmem, vmem, vmem),
        compiler_params=pltpu.CompilerParams(vmem_limit_bytes=2**21),
        cost_estimate=pl.CostEstimate(flops=10**6, bytes_accessed=3 * 10**5, transcendentals=0),
        name="pack",
    )(
        place,
        in_weight,
        jnp.swapaxes(out_weight, 1, 2),
        mixing.reshape(layers, 4, 128),
        pool_scale,
        activations,
        norm_gain,
    )
    mate_rows = jnp.concatenate(
        [chip_mate.reshape(seqs * tok, width)[:, 128 * h : 128 * (h + 1)] for h in range(2)]
    )
    count = 2 * seqs * tok
    last = lax.dynamic_update_slice(last, mate_rows, (80 + (1 - c) * count, 0))

    got = [first] + gather(first, FIRST, 0)
    got_last = [last] + gather(last, LAST, 0)
    p = jnp.stack(got)
    p = [p] + gather(p, FIRST, 1)
    q = jnp.stack([part[:64] for part in got_last])
    tokens = jnp.stack([part[64:] for part in got_last])
    tokens_2 = send(tokens, from_core())
    q = [q] + gather(q, LAST, 1)

    p = jnp.stack(p)
    p = [p] + gather(p, FIRST, 2)
    tokens = jnp.where(c == 0, tokens, tokens_2)
    mine = jnp.where(c == 0, tokens[:, 16 : 16 + count], tokens[:, 16 + count :])
    beside = send(mine, across_chips())
    q = jnp.stack(q)
    q = [q] + gather(q, LAST, 2)
    p_2 = [send(p[0], from_core())]
    q_2 = [send(q[0], from_core())]
    p_2 += [send(part, from_core()) for part in p[1:]]
    q_2 += [send(part, from_core()) for part in q[1:]]

    rows = seqs * 3 * tok
    dims = (layers, seqs, tok, tok, seq_len)
    inner_rows = seqs * 2 * tok
    made = pl.pallas_call(
        functools.partial(tables, *dims),
        out_shape=(
            jax.ShapeDtypeStruct((4, rows, rows), jnp.bfloat16),
            jax.ShapeDtypeStruct((4, rows, 128), jnp.float32),
            jax.ShapeDtypeStruct((4, inner_rows, inner_rows), jnp.bfloat16),
            jax.ShapeDtypeStruct((4, inner_rows, 128), jnp.float32),
            jax.ShapeDtypeStruct((layers, 128, 512), jnp.bfloat16),
        ),
        in_specs=[smem],
        out_specs=(vmem,) * 5,
        compiler_params=pltpu.CompilerParams(vmem_limit_bytes=2**22),
        cost_estimate=pl.CostEstimate(flops=10**7, bytes_accessed=10**6, transcendentals=0),
        name="tables",
    )(place)
    weights = pltpu.VMEM((layers, 4, 1024, 128), jnp.bfloat16)
    result = pl.pallas_call(
        functools.partial(all_layers, dims),
        out_shape=jax.ShapeDtypeStruct((seqs * tok, width), jnp.bfloat16),
        in_specs=[smem] + [vmem] * 24,
        out_specs=vmem,
        scratch_shapes=[
            weights,
            weights,
            pltpu.VMEM((4, 512, 128), jnp.bfloat16),
            pltpu.VMEM((4, rows, width), jnp.bfloat16),
            pltpu.VMEM((4, layers, 128), jnp.float32),
        ],
        compiler_params=pltpu.CompilerParams(vmem_limit_bytes=18 * 2**20),
        cost_estimate=pl.CostEstimate(
            flops=2 * 10**9, bytes_accessed=18 * 10**6, transcendentals=1000
        ),
        name="all_layers",
    )(place, *p, *p_2, *q, *q_2, tokens, beside, gain, *made)
    return result.reshape(seqs, tok, width)


def solution(mesh):
    return jax.shard_map(
        body,
        mesh=mesh,
        in_specs=(
            P(None, "sp", "tp"),
            P(),
            P(None, "sp", "tp"),
            P(None, "tp", "sp"),
            P(None, "tp", "sp", None),
            P(None, "tp"),
        ),
        out_specs=P(None, "sp", "tp"),
        check_vma=False,
    )
```

time: 82.5 us -> 66.7 us (0.81)
  the two profiles are of different devices: /device:TPU:0 before, /device:TPU:1 now
where the time goes in v4:
time: 66.7 us; the launch traced here: 66.4 us
  starting transfers between devices  34.6 us (52%)
  waiting for transfers between devices  18 us (27%)
  Pallas kernels  9.57 us (14%)
  local copies, waits for them, and re-layouts  2.66 us (4%)
  other arithmetic  1.39 us (2%)
    ppermute x29, starting transfers between devices, send(): return lax.ppermute(value, AXES, perm)  34.6 us
    ppermute x29, waiting for transfers between devices, send(): return lax.ppermute(value, AXES, perm)  18 us
    pallas_call x1, Pallas kernels, body(): pl.pallas_call(functools.partial(all_layers, dims), out_shape=jax.ShapeDt...  7.9 us
    unnamed x16, local copies, waits for them, and re-layouts  2.62 us
  transfers between devices with their start and end apart: 29, of which 7 were waited for; matrix products, arithmetic and copies ran while one was open for 2% of the time, Pallas kernels for 3%

profile of v4, /device:TPU:1, one launch (start us, length us, event | category | flops | bytes accessed | tf_op | source)
XLA Modules:
  0.0 66.4 jit_solution(5597789678040194928)
XLA Ops:
  0.0 1.4 %collective-permute-start.13 = (bf16[2,32,256]{2,1,0:T(8,128)(2,1)}, bf16[2,32,256]{2,1,0:T(8,128)(2,1)S(1)}, u32[]{:S(2)}, u32[]{:S(2)}) collective-permute-start(bf16[2,32,256]{2,1,0:T(8,128)(2,1)} %act_ref.1), channel_id=1, source_target_pairs={{4,0},{5,1},{6,2},{7,3},{0,4},{1,5},{2,6},{3,7},{12,8},{13,9},{14,... | collective-permute-start | bytes 98312 | tf_op jit(solution)/shard_map/ppermute | solution.py:59
  1.4 0.1 pad_add_fusion.place_ref
  1.5 0.6 copy-done.5
  2.1 0.0 copy-done.4
  2.1 0.1 copy-done.2
  2.2 0.0 copy-done.1
  2.2 0.0 copy-done
  2.2 0.7 %copy-done.3 = f32[4,1024]{1,0:T(4,128)S(1)} copy-done((f32[4,1024]{1,0:T(4,128)S(1)}, f32[4,1024]{1,0:T(4,128)}, u32[]{:S(2)}) %copy-start.3) | copy-done | bytes 16408
  2.9 0.6 pack.1
  3.5 1.8 %collective-permute-start.2 = (bf16[208,128]{1,0:T(8,128)(2,1)S(1)}, bf16[208,128]{1,0:T(8,128)(2,1)S(1)}, u32[]{:S(2)}, u32[]{:S(2)}) collective-permute-start(bf16[208,128]{1,0:T(8,128)(2,1)S(1)} %get-tuple-element.13), channel_id=1, source_target_pairs={{3,0},{0,1},{1,2},{2,3},{100,4},{101,5},{102,6},{103,7},{11,8},{8,... | collective-permute-start | bytes 159752 | tf_op jit(solution)/shard_map/ppermute | solution.py:59
  5.3 3.3 %collective-permute-start.1 = (bf16[208,128]{1,0:T(8,128)(2,1)S(1)}, bf16[208,128]{1,0:T(8,128)(2,1)S(1)}, u32[]{:S(2)}, u32[]{:S(2)}) collective-permute-start(bf16[208,128]{1,0:T(8,128)(2,1)S(1)} %get-tuple-element.13), channel_id=1, source_target_pairs={{2,0},{3,1},{0,2},{1,3},{68,4},{69,5},{70,6},{71,7},{10,8},{11,9},... | collective-permute-start | bytes 159752 | tf_op jit(solution)/shard_map/ppermute | solution.py:59
  8.6 0.7 %collective-permute-start = (bf16[208,128]{1,0:T(8,128)(2,1)S(1)}, bf16[208,128]{1,0:T(8,128)(2,1)S(1)}, u32[]{:S(2)}, u32[]{:S(2)}) collective-permute-start(bf16[208,128]{1,0:T(8,128)(2,1)S(1)} %get-tuple-element.13), channel_id=1, source_target_pairs={{1,0},{2,1},{3,2},{0,3},{36,4},{37,5},{38,6},{39,7},{9,8},{10,9},{... | collective-permute-start | bytes 159752 | tf_op jit(solution)/shard_map/ppermute | solution.py:59
  9.4 1.4 %collective-permute-start.16 = (bf16[336,128]{1,0:T(8,128)(2,1)S(1)}, bf16[336,128]{1,0:T(8,128)(2,1)S(1)}, u32[]{:S(2)}, u32[]{:S(2)}) collective-permute-start(bf16[336,128]{1,0:T(8,128)(2,1)S(1)} %maximum_dynamic-update-slice_fusion), channel_id=1, source_target_pairs={{3,0},{0,1},{1,2},{2,3},{28,4},{29,5},{30,6},{31,7},{11,8},{8,9},{... | collective-permute-start | bytes 258056 | tf_op jit(solution)/shard_map/ppermute | solution.py:59
  10.7 2.6 %collective-permute-start.15 = (bf16[336,128]{1,0:T(8,128)(2,1)S(1)}, bf16[336,128]{1,0:T(8,128)(2,1)S(1)}, u32[]{:S(2)}, u32[]{:S(2)}) collective-permute-start(bf16[336,128]{1,0:T(8,128)(2,1)S(1)} %maximum_dynamic-update-slice_fusion), channel_id=1, source_target_pairs={{2,0},{3,1},{0,2},{1,3},{20,4},{21,5},{22,6},{23,7},{10,8},{11,9},... | collective-permute-start | bytes 258056 | tf_op jit(solution)/shard_map/ppermute | solution.py:59
  13.4 1.1 %collective-permute-start.14 = (bf16[336,128]{1,0:T(8,128)(2,1)S(1)}, bf16[336,128]{1,0:T(8,128)(2,1)S(1)}, u32[]{:S(2)}, u32[]{:S(2)}) collective-permute-start(bf16[336,128]{1,0:T(8,128)(2,1)S(1)} %maximum_dynamic-update-slice_fusion), channel_id=1, source_target_pairs={{1,0},{2,1},{3,2},{0,3},{12,4},{13,5},{14,6},{15,7},{9,8},{10,9},{... | collective-permute-start | bytes 258056 | tf_op jit(solution)/shard_map/ppermute | solution.py:59
  14.5 0.3 collective-permute-start.4
  14.8 2.6 %collective-permute-start.3 = (bf16[4,208,128]{2,1,0:T(8,128)(2,1)S(1)}, bf16[4,208,128]{2,1,0:T(8,128)(2,1)S(1)}, u32[]{:S(2)}, u32[]{:S(2)}) collective-permute-start(bf16[4,208,128]{2,1,0:T(8,128)(2,1)S(1)} %get-tuple-element.22), channel_id=1, source_target_pairs={{32,0},{33,1},{34,2},{35,3},{12,4},{13,5},{14,6},{15,7},{40,8},{41... | collective-permute-start | bytes 638984 | tf_op jit(solution)/shard_map/ppermute | solution.py:59
  17.4 2.8 %collective-permute-start.18 = (bf16[4,64,128]{2,1,0:T(8,128)(2,1)S(1)}, bf16[4,64,128]{2,1,0:T(8,128)(2,1)S(1)}, u32[]{:S(2)}, u32[]{:S(2)}) collective-permute-start(bf16[4,64,128]{2,1,0:T(8,128)(2,1)S(1)} %get-tuple-element.24), channel_id=1, source_target_pairs={{16,0},{17,1},{18,2},{19,3},{6,4},{7,5},{4,6},{5,7},{24,8},{25,9},... | collective-permute-start | bytes 196616 | tf_op jit(solution)/shard_map/ppermute | solution.py:59
  20.3 0.9 %collective-permute-start.17 = (bf16[4,64,128]{2,1,0:T(8,128)(2,1)S(1)}, bf16[4,64,128]{2,1,0:T(8,128)(2,1)S(1)}, u32[]{:S(2)}, u32[]{:S(2)}) collective-permute-start(bf16[4,64,128]{2,1,0:T(8,128)(2,1)S(1)} %get-tuple-element.24), channel_id=1, source_target_pairs={{8,0},{9,1},{10,2},{11,3},{5,4},{6,5},{7,6},{4,7},{16,8},{17,9},{1... | collective-permute-start | bytes 196616 | tf_op jit(solution)/shard_map/ppermute | solution.py:59
  21.2 0.6 copy-done.6
  21.8 0.6 copy-done.7
  22.4 0.6 collective-permute-start.19
  23.0 2.5 %collective-permute-start.27 = (bf16[4,272,128]{2,1,0:T(8,128)(2,1)S(1)}, bf16[4,272,128]{2,1,0:T(8,128)(2,1)}, u32[]{:S(2)}, u32[]{:S(2)}) collective-permute-start(bf16[4,272,128]{2,1,0:T(8,128)(2,1)S(1)} %pad_maximum_fusion.1), channel_id=1, source_target_pairs={{4,0},{5,1},{6,2},{7,3},{0,4},{1,5},{2,6},{3,7},{12,8},{13,9},{14,... | collective-permute-start | bytes 835592 | tf_op jit(solution)/shard_map/ppermute | solution.py:59
  25.5 0.1 pad_maximum_fusion.refs_0_
  25.6 0.5 collective-permute-start.8
  26.1 2.3 %collective-permute-start.7 = (bf16[4,4,208,128]{3,2,1,0:T(8,128)(2,1)S(1)}, bf16[4,4,208,128]{3,2,1,0:T(8,128)(2,1)S(1)}, u32[]{:S(2)}, u32[]{:S(2)}) collective-permute-start(bf16[4,4,208,128]{3,2,1,0:T(8,128)(2,1)S(1)} %pad_maximum_fusion.refs_0_), channel_id=1, source_target_pairs={{16,0},{17,1},{18,2},{19,3},{6,4},{7,5},{4,6},{5,7},{24,8},{25,9},... | collective-permute-start | bytes 2555912 | tf_op jit(solution)/shard_map/ppermute | solution.py:59
  28.4 1.8 %collective-permute-start.6 = (bf16[4,4,208,128]{3,2,1,0:T(8,128)(2,1)S(1)}, bf16[4,4,208,128]{3,2,1,0:T(8,128)(2,1)}, u32[]{:S(2)}, u32[]{:S(2)}) collective-permute-start(bf16[4,4,208,128]{3,2,1,0:T(8,128)(2,1)S(1)} %pad_maximum_fusion.refs_0_), channel_id=1, source_target_pairs={{8,0},{9,1},{10,2},{11,3},{5,4},{6,5},{7,6},{4,7},{16,8},{17,9},{1... | collective-permute-start | bytes 2555912 | tf_op jit(solution)/shard_map/ppermute | solution.py:59
  30.3 0.4 collective-permute-start.23
  30.7 0.5 collective-permute-start.22
  31.2 0.7 %collective-permute-done.23.refs_12_ = bf16[4,4,64,128]{3,2,1,0:T(8,128)(2,1)S(1)} collective-permute-done((bf16[4,4,64,128]{3,2,1,0:T(8,128)(2,1)S(1)}, bf16[4,4,64,128]{3,2,1,0:T(8,128)(2,1)S(1)}, u32[]{:S(2)}, u32[]{:S(2)}) %collective-permute-start.23) | collective-permute-done | bytes 262176 | tf_op jit(solution)/shard_map/ppermute | solution.py:59
  31.9 1.7 %collective-permute-start.21 = (bf16[4,4,64,128]{3,2,1,0:T(8,128)(2,1)S(1)}, bf16[4,4,64,128]{3,2,1,0:T(8,128)(2,1)S(1)}, u32[]{:S(2)}, u32[]{:S(2)}) collective-permute-start(bf16[4,4,64,128]{3,2,1,0:T(8,128)(2,1)S(1)} %pad_maximum_fusion.2.refs_8_), channel_id=1, source_target_pairs={{64,0},{65,1},{66,2},{67,3},{68,4},{69,5},{70,6},{71,7},{72,8},{73... | collective-permute-start | bytes 786440 | tf_op jit(solution)/shard_map/ppermute | solution.py:59
  33.7 1.0 %broadcast_select_fusion.refs_16_ = bf16[4,272,128]{2,1,0:T(8,128)(2,1)S(1)} fusion(bf16[4,272,128]{2,1,0:T(8,128)(2,1)} %collective-permute-done.27, pred[]{:T(512)S(6)} %eq.7, bf16[1,272,128]{2,1,0:T(8,128)(2,1)S(1)} %slice_bitcast_fusion, bf16[1,272,128]{2,1,0:T(8,128)(2,1)} %copy-done.6, bf16[1,272,128]{2,1,0:T(8,128)(2,1)} %copy-done.7, ...), kind=kLoop, calls=%fused_computation.2 | loop fusion | flops 557056 | bytes 835585 | tf_op jit(solution)/shard_map/jit(_where)/select_n | solution.py:274
  34.7 4.9 %collective-permute-done.22.refs_11_ = bf16[4,4,64,128]{3,2,1,0:T(8,128)(2,1)S(1)} collective-permute-done((bf16[4,4,64,128]{3,2,1,0:T(8,128)(2,1)S(1)}, bf16[4,4,64,128]{3,2,1,0:T(8,128)(2,1)S(1)}, u32[]{:S(2)}, u32[]{:S(2)}) %collective-permute-start.22) | collective-permute-done | bytes 262176 | tf_op jit(solution)/shard_map/ppermute | solution.py:59
  39.6 0.6 collective-permute-start.20
  40.3 5.3 %collective-permute-done.21.refs_10_ = bf16[4,4,64,128]{3,2,1,0:T(8,128)(2,1)S(1)} collective-permute-done((bf16[4,4,64,128]{3,2,1,0:T(8,128)(2,1)S(1)}, bf16[4,4,64,128]{3,2,1,0:T(8,128)(2,1)S(1)}, u32[]{:S(2)}, u32[]{:S(2)}) %collective-permute-start.21) | collective-permute-done | bytes 262176 | tf_op jit(solution)/shard_map/ppermute | solution.py:59
  45.6 3.3 %collective-permute-start.28 = (bf16[4,128,128]{2,1,0:T(8,128)(2,1)S(1)}, bf16[4,128,128]{2,1,0:T(8,128)(2,1)S(1)}, u32[]{:S(2)}, u32[]{:S(2)}) collective-permute-start(bf16[4,128,128]{2,1,0:T(8,128)(2,1)S(1)} %slice_select_fusion), channel_id=1, source_target_pairs={{4,8},{8,4},{5,9},{9,5},{6,10},{10,6},{7,11},{11,7},{12,16},{16,12... | collective-permute-start | bytes 393224 | tf_op jit(solution)/shard_map/ppermute | solution.py:59
  48.9 0.1 collective-permute-start.9
  49.0 0.5 collective-permute-start.12
  49.5 0.1 collective-permute-start.11
  49.6 0.4 collective-permute-start.10
  50.1 1.8 %collective-permute-done.28.refs_17_ = bf16[4,128,128]{2,1,0:T(8,128)(2,1)S(1)} collective-permute-done((bf16[4,128,128]{2,1,0:T(8,128)(2,1)S(1)}, bf16[4,128,128]{2,1,0:T(8,128)(2,1)S(1)}, u32[]{:S(2)}, u32[]{:S(2)}) %collective-permute-start.28) | collective-permute-done | bytes 131104 | tf_op jit(solution)/shard_map/ppermute | solution.py:59
  51.9 3.6 %collective-permute-done.26.refs_15_ = bf16[4,4,64,128]{3,2,1,0:T(8,128)(2,1)S(1)} collective-permute-done((bf16[4,4,64,128]{3,2,1,0:T(8,128)(2,1)S(1)}, bf16[4,4,64,128]{3,2,1,0:T(8,128)(2,1)S(1)}, u32[]{:S(2)}, u32[]{:S(2)}) %collective-permute-start.26) | collective-permute-done | bytes 262176 | tf_op jit(solution)/shard_map/ppermute | solution.py:59
  55.4 0.1 collective-permute-start.25
  55.6 1.4 %collective-permute-done.25.refs_14_ = bf16[4,4,64,128]{3,2,1,0:T(8,128)(2,1)S(1)} collective-permute-done((bf16[4,4,64,128]{3,2,1,0:T(8,128)(2,1)S(1)}, bf16[4,4,64,128]{3,2,1,0:T(8,128)(2,1)S(1)}, u32[]{:S(2)}, u32[]{:S(2)}) %collective-permute-start.25) | collective-permute-done | bytes 262176 | tf_op jit(solution)/shard_map/ppermute | solution.py:59
  57.0 0.1 collective-permute-start.24
  57.1 1.1 %tables.1 = (bf16[4,192,192]{2,1,0:T(8,128)(2,1)S(1)}, f32[4,192,128]{2,1,0:T(8,128)S(1)}, bf16[4,128,128]{2,1,0:T(8,128)(2,1)S(1)}, f32[4,128,128]{2,1,0:T(8,128)S(1)}, bf16[4,128,512]{2,1,0:T(8,128)(2,1)S(1)}) custom-call(s32[4]{0:T(128)S(1)} %pad_add_fusion.place_ref), custom_call_target="tpu_custom_call" | custom-call | flops 10000000 | bytes 1000000 | tf_op jit(solution)/shard_map/tables/pallas_call | solution.py:287
  58.2 0.3 collective-permute-done.24.refs_13_
  58.5 7.9 %all_layers.1 = bf16[64,256]{1,0:T(8,128)(2,1)} custom-call(s32[4]{0:T(128)S(1)} %pad_add_fusion.place_ref, bf16[4,4,208,128]{3,2,1,0:T(8,128)(2,1)S(1)} %pad_maximum_fusion.refs_0_, bf16[4,4,208,128]{3,2,1,0:T(8,128)(2,1)} %collective-permute-done.6.refs_1_, bf16[4,4,208,128]{3,2,1,0:T(8,128)(2,1)S(1)} %collective-permute-done.7.refs_2_, ...), custom_call_target="tpu_custom_call" | custom-call | flops 2000000000 | bytes 18000000 | tf_op jit(solution)/shard_map/all_layers/pallas_call | solution.py:303
  (47 shorter events, 0.3 us)
Async XLA Ops:
  0.0 9.3 %collective-permute-start.13 = (bf16[2,32,256]{2,1,0:T(8,128)(2,1)}, bf16[2,32,256]{2,1,0:T(8,128)(2,1)S(1)}, u32[]{:S(2)}, u32[]{:S(2)}) collective-permute-start(bf16[2,32,256]{2,1,0:T(8,128)(2,1)} %act_ref.1), channel_id=1, source_target_pairs={{4,0},{5,1},{6,2},{7,3},{0,4},{1,5},{2,6},{3,7},{12,8},{13,9},{14,... | collective-permute-start | bytes 98312 | tf_op jit(solution)/shard_map/ppermute | solution.py:59
  1.4 0.7 %copy-start.5 = (f32[4,128]{1,0:T(4,128)S(1)}, f32[4,128]{1,0:T(4,128)}, u32[]{:S(2)}) copy-start(f32[4,128]{1,0:T(4,128)} %scale_ref.1) | copy-start | bytes 6148
  1.4 0.7 %copy-start.4 = (bf16[4,1,4,128]{3,2,1,0:T(4,128)(2,1)S(1)}, bf16[4,1,4,128]{3,2,1,0:T(4,128)(2,1)}, u32[]{:S(2)}) copy-start(bf16[4,1,4,128]{3,2,1,0:T(4,128)(2,1)} %param.10) | copy-start | bytes 12292
  1.4 0.8 %copy-start.2 = (bf16[2,32,256]{2,1,0:T(8,128)(2,1)S(1)}, bf16[2,32,256]{2,1,0:T(8,128)(2,1)}, u32[]{:S(2)}) copy-start(bf16[2,32,256]{2,1,0:T(8,128)(2,1)} %act_ref.1) | copy-start | bytes 98308
  1.4 0.8 %copy-start.1 = (bf16[4,128,32]{1,2,0:T(8,128)(2,1)S(1)}, bf16[4,128,32]{1,2,0:T(8,128)(2,1)}, u32[]{:S(2)}) copy-start(bf16[4,128,32]{1,2,0:T(8,128)(2,1)} %param.9) | copy-start | bytes 98308
  1.4 0.8 %copy-start = (bf16[4,32,128]{2,1,0:T(8,128)(2,1)S(1)}, bf16[4,32,128]{2,1,0:T(8,128)(2,1)}, u32[]{:S(2)}) copy-start(bf16[4,32,128]{2,1,0:T(8,128)(2,1)} %in_ref.1) | copy-start | bytes 98308
  2.2 0.7 %copy-start.3 = (f32[4,1024]{1,0:T(4,128)S(1)}, f32[4,1024]{1,0:T(4,128)}, u32[]{:S(2)}) copy-start(f32[4,1024]{1,0:T(4,128)} %gain_ref.1) | copy-start | bytes 49156
  3.5 9.9 %collective-permute-start.2 = (bf16[208,128]{1,0:T(8,128)(2,1)S(1)}, bf16[208,128]{1,0:T(8,128)(2,1)S(1)}, u32[]{:S(2)}, u32[]{:S(2)}) collective-permute-start(bf16[208,128]{1,0:T(8,128)(2,1)S(1)} %get-tuple-element.13), channel_id=1, source_target_pairs={{3,0},{0,1},{1,2},{2,3},{100,4},{101,5},{102,6},{103,7},{11,8},{8,... | collective-permute-start | bytes 159752 | tf_op jit(solution)/shard_map/ppermute | solution.py:59
  5.3 9.1 %collective-permute-start.1 = (bf16[208,128]{1,0:T(8,128)(2,1)S(1)}, bf16[208,128]{1,0:T(8,128)(2,1)S(1)}, u32[]{:S(2)}, u32[]{:S(2)}) collective-permute-start(bf16[208,128]{1,0:T(8,128)(2,1)S(1)} %get-tuple-element.13), channel_id=1, source_target_pairs={{2,0},{3,1},{0,2},{1,3},{68,4},{69,5},{70,6},{71,7},{10,8},{11,9},... | collective-permute-start | bytes 159752 | tf_op jit(solution)/shard_map/ppermute | solution.py:59
  8.6 5.8 %collective-permute-start = (bf16[208,128]{1,0:T(8,128)(2,1)S(1)}, bf16[208,128]{1,0:T(8,128)(2,1)S(1)}, u32[]{:S(2)}, u32[]{:S(2)}) collective-permute-start(bf16[208,128]{1,0:T(8,128)(2,1)S(1)} %get-tuple-element.13), channel_id=1, source_target_pairs={{1,0},{2,1},{3,2},{0,3},{36,4},{37,5},{38,6},{39,7},{9,8},{10,9},{... | collective-permute-start | bytes 159752 | tf_op jit(solution)/shard_map/ppermute | solution.py:59
  9.4 8.0 %collective-permute-start.16 = (bf16[336,128]{1,0:T(8,128)(2,1)S(1)}, bf16[336,128]{1,0:T(8,128)(2,1)S(1)}, u32[]{:S(2)}, u32[]{:S(2)}) collective-permute-start(bf16[336,128]{1,0:T(8,128)(2,1)S(1)} %maximum_dynamic-update-slice_fusion), channel_id=1, source_target_pairs={{3,0},{0,1},{1,2},{2,3},{28,4},{29,5},{30,6},{31,7},{11,8},{8,9},{... | collective-permute-start | bytes 258056 | tf_op jit(solution)/shard_map/ppermute | solution.py:59
  10.7 6.6 %collective-permute-start.15 = (bf16[336,128]{1,0:T(8,128)(2,1)S(1)}, bf16[336,128]{1,0:T(8,128)(2,1)S(1)}, u32[]{:S(2)}, u32[]{:S(2)}) collective-permute-start(bf16[336,128]{1,0:T(8,128)(2,1)S(1)} %maximum_dynamic-update-slice_fusion), channel_id=1, source_target_pairs={{2,0},{3,1},{0,2},{1,3},{20,4},{21,5},{22,6},{23,7},{10,8},{11,9},... | collective-permute-start | bytes 258056 | tf_op jit(solution)/shard_map/ppermute | solution.py:59
  13.4 4.0 %collective-permute-start.14 = (bf16[336,128]{1,0:T(8,128)(2,1)S(1)}, bf16[336,128]{1,0:T(8,128)(2,1)S(1)}, u32[]{:S(2)}, u32[]{:S(2)}) collective-permute-start(bf16[336,128]{1,0:T(8,128)(2,1)S(1)} %maximum_dynamic-update-slice_fusion), channel_id=1, source_target_pairs={{1,0},{2,1},{3,2},{0,3},{12,4},{13,5},{14,6},{15,7},{9,8},{10,9},{... | collective-permute-start | bytes 258056 | tf_op jit(solution)/shard_map/ppermute | solution.py:59
  14.5 7.9 %collective-permute-start.4 = (bf16[4,208,128]{2,1,0:T(8,128)(2,1)S(1)}, bf16[4,208,128]{2,1,0:T(8,128)(2,1)S(1)}, u32[]{:S(2)}, u32[]{:S(2)}) collective-permute-start(bf16[4,208,128]{2,1,0:T(8,128)(2,1)S(1)} %get-tuple-element.22), channel_id=1, source_target_pairs={{64,0},{65,1},{66,2},{67,3},{20,4},{21,5},{22,6},{23,7},{72,8},{73... | collective-permute-start | bytes 638984 | tf_op jit(solution)/shard_map/ppermute | solution.py:59
  14.8 8.2 %collective-permute-start.3 = (bf16[4,208,128]{2,1,0:T(8,128)(2,1)S(1)}, bf16[4,208,128]{2,1,0:T(8,128)(2,1)S(1)}, u32[]{:S(2)}, u32[]{:S(2)}) collective-permute-start(bf16[4,208,128]{2,1,0:T(8,128)(2,1)S(1)} %get-tuple-element.22), channel_id=1, source_target_pairs={{32,0},{33,1},{34,2},{35,3},{12,4},{13,5},{14,6},{15,7},{40,8},{41... | collective-permute-start | bytes 638984 | tf_op jit(solution)/shard_map/ppermute | solution.py:59
  17.4 8.1 %collective-permute-start.5 = (bf16[4,208,128]{2,1,0:T(8,128)(2,1)S(1)}, bf16[4,208,128]{2,1,0:T(8,128)(2,1)S(1)}, u32[]{:S(2)}, u32[]{:S(2)}) collective-permute-start(bf16[4,208,128]{2,1,0:T(8,128)(2,1)S(1)} %get-tuple-element.22), channel_id=1, source_target_pairs={{96,0},{97,1},{98,2},{99,3},{28,4},{29,5},{30,6},{31,7},{104,8},{1... | collective-permute-start | bytes 638984 | tf_op jit(solution)/shard_map/ppermute | solution.py:59
  17.4 8.7 %collective-permute-start.18 = (bf16[4,64,128]{2,1,0:T(8,128)(2,1)S(1)}, bf16[4,64,128]{2,1,0:T(8,128)(2,1)S(1)}, u32[]{:S(2)}, u32[]{:S(2)}) collective-permute-start(bf16[4,64,128]{2,1,0:T(8,128)(2,1)S(1)} %get-tuple-element.24), channel_id=1, source_target_pairs={{16,0},{17,1},{18,2},{19,3},{6,4},{7,5},{4,6},{5,7},{24,8},{25,9},... | collective-permute-start | bytes 196616 | tf_op jit(solution)/shard_map/ppermute | solution.py:59
  20.3 8.2 %collective-permute-start.17 = (bf16[4,64,128]{2,1,0:T(8,128)(2,1)S(1)}, bf16[4,64,128]{2,1,0:T(8,128)(2,1)S(1)}, u32[]{:S(2)}, u32[]{:S(2)}) collective-permute-start(bf16[4,64,128]{2,1,0:T(8,128)(2,1)S(1)} %get-tuple-element.24), channel_id=1, source_target_pairs={{8,0},{9,1},{10,2},{11,3},{5,4},{6,5},{7,6},{4,7},{16,8},{17,9},{1... | collective-permute-start | bytes 196616 | tf_op jit(solution)/shard_map/ppermute | solution.py:59
  21.1 0.6 copy-start.6
  21.8 0.6 copy-start.7
  22.4 7.9 %collective-permute-start.19 = (bf16[4,64,128]{2,1,0:T(8,128)(2,1)S(1)}, bf16[4,64,128]{2,1,0:T(8,128)(2,1)S(1)}, u32[]{:S(2)}, u32[]{:S(2)}) collective-permute-start(bf16[4,64,128]{2,1,0:T(8,128)(2,1)S(1)} %get-tuple-element.24), channel_id=1, source_target_pairs={{24,0},{25,1},{26,2},{27,3},{7,4},{4,5},{5,6},{6,7},{0,8},{1,9},{2... | collective-permute-start | bytes 196616 | tf_op jit(solution)/shard_map/ppermute | solution.py:59
  23.0 7.7 %collective-permute-start.27 = (bf16[4,272,128]{2,1,0:T(8,128)(2,1)S(1)}, bf16[4,272,128]{2,1,0:T(8,128)(2,1)}, u32[]{:S(2)}, u32[]{:S(2)}) collective-permute-start(bf16[4,272,128]{2,1,0:T(8,128)(2,1)S(1)} %pad_maximum_fusion.1), channel_id=1, source_target_pairs={{4,0},{5,1},{6,2},{7,3},{0,4},{1,5},{2,6},{3,7},{12,8},{13,9},{14,... | collective-permute-start | bytes 835592 | tf_op jit(solution)/shard_map/ppermute | solution.py:59
  25.6 23.4 %collective-permute-start.8 = (bf16[4,4,208,128]{3,2,1,0:T(8,128)(2,1)S(1)}, bf16[4,4,208,128]{3,2,1,0:T(8,128)(2,1)S(1)}, u32[]{:S(2)}, u32[]{:S(2)}) collective-permute-start(bf16[4,4,208,128]{3,2,1,0:T(8,128)(2,1)S(1)} %pad_maximum_fusion.refs_0_), channel_id=1, source_target_pairs={{24,0},{25,1},{26,2},{27,3},{7,4},{4,5},{5,6},{6,7},{0,8},{1,9},{2... | collective-permute-start | bytes 2555912 | tf_op jit(solution)/shard_map/ppermute | solution.py:59
  26.1 23.4 %collective-permute-start.7 = (bf16[4,4,208,128]{3,2,1,0:T(8,128)(2,1)S(1)}, bf16[4,4,208,128]{3,2,1,0:T(8,128)(2,1)S(1)}, u32[]{:S(2)}, u32[]{:S(2)}) collective-permute-start(bf16[4,4,208,128]{3,2,1,0:T(8,128)(2,1)S(1)} %pad_maximum_fusion.refs_0_), channel_id=1, source_target_pairs={{16,0},{17,1},{18,2},{19,3},{6,4},{7,5},{4,6},{5,7},{24,8},{25,9},... | collective-permute-start | bytes 2555912 | tf_op jit(solution)/shard_map/ppermute | solution.py:59
  28.4 21.2 %collective-permute-start.6 = (bf16[4,4,208,128]{3,2,1,0:T(8,128)(2,1)S(1)}, bf16[4,4,208,128]{3,2,1,0:T(8,128)(2,1)}, u32[]{:S(2)}, u32[]{:S(2)}) collective-permute-start(bf16[4,4,208,128]{3,2,1,0:T(8,128)(2,1)S(1)} %pad_maximum_fusion.refs_0_), channel_id=1, source_target_pairs={{8,0},{9,1},{10,2},{11,3},{5,4},{6,5},{7,6},{4,7},{16,8},{17,9},{1... | collective-permute-start | bytes 2555912 | tf_op jit(solution)/shard_map/ppermute | solution.py:59
  30.3 1.6 %collective-permute-start.23 = (bf16[4,4,64,128]{3,2,1,0:T(8,128)(2,1)S(1)}, bf16[4,4,64,128]{3,2,1,0:T(8,128)(2,1)S(1)}, u32[]{:S(2)}, u32[]{:S(2)}) collective-permute-start(bf16[4,4,64,128]{3,2,1,0:T(8,128)(2,1)S(1)} %pad_maximum_fusion.2.refs_8_), channel_id=1, source_target_pairs={{4,0},{5,1},{6,2},{7,3},{0,4},{1,5},{2,6},{3,7},{12,8},{13,9},{14,... | collective-permute-start | bytes 786440 | tf_op jit(solution)/shard_map/ppermute | solution.py:59
  30.7 8.9 %collective-permute-start.22 = (bf16[4,4,64,128]{3,2,1,0:T(8,128)(2,1)S(1)}, bf16[4,4,64,128]{3,2,1,0:T(8,128)(2,1)S(1)}, u32[]{:S(2)}, u32[]{:S(2)}) collective-permute-start(bf16[4,4,64,128]{3,2,1,0:T(8,128)(2,1)S(1)} %pad_maximum_fusion.2.refs_8_), channel_id=1, source_target_pairs={{96,0},{97,1},{98,2},{99,3},{100,4},{101,5},{102,6},{103,7},{104,8... | collective-permute-start | bytes 786440 | tf_op jit(solution)/shard_map/ppermute | solution.py:59
  31.9 13.7 %collective-permute-start.21 = (bf16[4,4,64,128]{3,2,1,0:T(8,128)(2,1)S(1)}, bf16[4,4,64,128]{3,2,1,0:T(8,128)(2,1)S(1)}, u32[]{:S(2)}, u32[]{:S(2)}) collective-permute-start(bf16[4,4,64,128]{3,2,1,0:T(8,128)(2,1)S(1)} %pad_maximum_fusion.2.refs_8_), channel_id=1, source_target_pairs={{64,0},{65,1},{66,2},{67,3},{68,4},{69,5},{70,6},{71,7},{72,8},{73... | collective-permute-start | bytes 786440 | tf_op jit(solution)/shard_map/ppermute | solution.py:59
  39.6 9.3 %collective-permute-start.20 = (bf16[4,4,64,128]{3,2,1,0:T(8,128)(2,1)S(1)}, bf16[4,4,64,128]{3,2,1,0:T(8,128)(2,1)S(1)}, u32[]{:S(2)}, u32[]{:S(2)}) collective-permute-start(bf16[4,4,64,128]{3,2,1,0:T(8,128)(2,1)S(1)} %pad_maximum_fusion.2.refs_8_), channel_id=1, source_target_pairs={{32,0},{33,1},{34,2},{35,3},{36,4},{37,5},{38,6},{39,7},{40,8},{41... | collective-permute-start | bytes 786440 | tf_op jit(solution)/shard_map/ppermute | solution.py:59
  45.6 6.3 %collective-permute-start.28 = (bf16[4,128,128]{2,1,0:T(8,128)(2,1)S(1)}, bf16[4,128,128]{2,1,0:T(8,128)(2,1)S(1)}, u32[]{:S(2)}, u32[]{:S(2)}) collective-permute-start(bf16[4,128,128]{2,1,0:T(8,128)(2,1)S(1)} %slice_select_fusion), channel_id=1, source_target_pairs={{4,8},{8,4},{5,9},{9,5},{6,10},{10,6},{7,11},{11,7},{12,16},{16,12... | collective-permute-start | bytes 393224 | tf_op jit(solution)/shard_map/ppermute | solution.py:59
  48.9 9.6 %collective-permute-start.9 = (bf16[4,4,208,128]{3,2,1,0:T(8,128)(2,1)S(1)}, bf16[4,4,208,128]{3,2,1,0:T(8,128)(2,1)S(1)}, u32[]{:S(2)}, u32[]{:S(2)}) collective-permute-start(bf16[4,4,208,128]{3,2,1,0:T(8,128)(2,1)S(1)} %pad_maximum_fusion.refs_0_), channel_id=1, source_target_pairs={{4,0},{5,1},{6,2},{7,3},{0,4},{1,5},{2,6},{3,7},{12,8},{13,9},{14,... | collective-permute-start | bytes 2555912 | tf_op jit(solution)/shard_map/ppermute | solution.py:59
  49.0 9.5 %collective-permute-start.12 = (bf16[4,4,208,128]{3,2,1,0:T(8,128)(2,1)S(1)}, bf16[4,4,208,128]{3,2,1,0:T(8,128)(2,1)S(1)}, u32[]{:S(2)}, u32[]{:S(2)}) collective-permute-start(bf16[4,4,208,128]{3,2,1,0:T(8,128)(2,1)S(1)} %collective-permute-done.8.refs_3_), channel_id=1, source_target_pairs={{4,0},{5,1},{6,2},{7,3},{0,4},{1,5},{2,6},{3,7},{12,8},{13,9},{14,... | collective-permute-start | bytes 2555912 | tf_op jit(solution)/shard_map/ppermute | solution.py:59
  49.5 9.0 %collective-permute-start.11 = (bf16[4,4,208,128]{3,2,1,0:T(8,128)(2,1)S(1)}, bf16[4,4,208,128]{3,2,1,0:T(8,128)(2,1)S(1)}, u32[]{:S(2)}, u32[]{:S(2)}) collective-permute-start(bf16[4,4,208,128]{3,2,1,0:T(8,128)(2,1)S(1)} %collective-permute-done.7.refs_2_), channel_id=1, source_target_pairs={{4,0},{5,1},{6,2},{7,3},{0,4},{1,5},{2,6},{3,7},{12,8},{13,9},{14,... | collective-permute-start | bytes 2555912 | tf_op jit(solution)/shard_map/ppermute | solution.py:59
  49.6 8.9 %collective-permute-start.10 = (bf16[4,4,208,128]{3,2,1,0:T(8,128)(2,1)}, bf16[4,4,208,128]{3,2,1,0:T(8,128)(2,1)S(1)}, u32[]{:S(2)}, u32[]{:S(2)}) collective-permute-start(bf16[4,4,208,128]{3,2,1,0:T(8,128)(2,1)} %collective-permute-done.6.refs_1_), channel_id=1, source_target_pairs={{4,0},{5,1},{6,2},{7,3},{0,4},{1,5},{2,6},{3,7},{12,8},{13,9},{14,... | collective-permute-start | bytes 2555912 | tf_op jit(solution)/shard_map/ppermute | solution.py:59
  51.9 3.6 %collective-permute-start.26 = (bf16[4,4,64,128]{3,2,1,0:T(8,128)(2,1)S(1)}, bf16[4,4,64,128]{3,2,1,0:T(8,128)(2,1)S(1)}, u32[]{:S(2)}, u32[]{:S(2)}) collective-permute-start(bf16[4,4,64,128]{3,2,1,0:T(8,128)(2,1)S(1)} %collective-permute-done.22.refs_11_), channel_id=1, source_target_pairs={{4,0},{5,1},{6,2},{7,3},{0,4},{1,5},{2,6},{3,7},{12,8},{13,9},{14,... | collective-permute-start | bytes 786440 | tf_op jit(solution)/shard_map/ppermute | solution.py:59
  55.4 1.5 %collective-permute-start.25 = (bf16[4,4,64,128]{3,2,1,0:T(8,128)(2,1)S(1)}, bf16[4,4,64,128]{3,2,1,0:T(8,128)(2,1)S(1)}, u32[]{:S(2)}, u32[]{:S(2)}) collective-permute-start(bf16[4,4,64,128]{3,2,1,0:T(8,128)(2,1)S(1)} %collective-permute-done.21.refs_10_), channel_id=1, source_target_pairs={{4,0},{5,1},{6,2},{7,3},{0,4},{1,5},{2,6},{3,7},{12,8},{13,9},{14,... | collective-permute-start | bytes 786440 | tf_op jit(solution)/shard_map/ppermute | solution.py:59
  57.0 1.5 %collective-permute-start.24 = (bf16[4,4,64,128]{3,2,1,0:T(8,128)(2,1)S(1)}, bf16[4,4,64,128]{3,2,1,0:T(8,128)(2,1)S(1)}, u32[]{:S(2)}, u32[]{:S(2)}) collective-permute-start(bf16[4,4,64,128]{3,2,1,0:T(8,128)(2,1)S(1)} %collective-permute-done.20.refs_9_), channel_id=1, source_target_pairs={{4,0},{5,1},{6,2},{7,3},{0,4},{1,5},{2,6},{3,7},{12,8},{13,9},{14,... | collective-permute-start | bytes 786440 | tf_op jit(solution)/shard_map/ppermute | solution.py:59

commit v5 on v4

--- a/solution.py
+++ b/solution.py
@@ -87,7 +87,7 @@
     return copy
 
 
-def tables(layers, seqs, tok, halo, seq_len, place_ref, *refs):
+def tables(layers, seqs, tok, halo, seq_len, place_ref, gain_ref, *refs):
     z, y, c = (place_ref[k] for k in range(3))
     first = ((z * NY + y) * NC + c) * tok
     for beside, bands, inverse in ((halo, *refs[0:2]), (halo // 2, *refs[2:4])):
@@ -109,7 +109,8 @@
             bands[g] = jnp.where(inside, 1.0, 0.0).astype(jnp.bfloat16)
             count = jnp.clip(pos_1 + half, 0, seq_len) - jnp.clip(pos_1 - half, 0, seq_len)
             inverse[g] = 1.0 / jnp.maximum(count, 1).astype(jnp.float32)
-    picks = refs[4]
+    picks, gain = refs[4:6]
+    gain[...] = gain_ref[...]
     pick_r = lax.broadcasted_iota(jnp.int32, (128, 512), 0)
     pick_q = lax.broadcasted_iota(jnp.int32, (128, 512), 1)
     base = ((pick_r >> 2) << 4) + (pick_r & 3)
@@ -149,26 +150,33 @@
 
 def all_layers(dims, place_ref, *refs):
     layers, seqs, tok, halo, _ = dims
-    acts, beside, gain = refs[16:19]
-    wide, narrow, picks, out = refs[19:21], refs[21:23], refs[23], refs[24]
-    w_in, w_out, mix_raw, state_parts, scales = refs[25:]
+    tokens, beside = refs[16:18], refs[18]
+    wide, narrow, picks, gain, out = refs[19:21], refs[21:23], refs[23], refs[24], refs[25]
+    w_in, w_out, mix_raw, state_parts, scales = refs[26:]
     place = tuple(place_ref[k] for k in range(4))
     _, _, c, x = place
     span = tok + 2 * halo
-    for k in range(4):
-        x_at = lax.rem(x + k, NX)
-        for h in range(2):
-            lanes = slice(128 * h, 128 * (h + 1))
-            for s in range(seqs):
-                for core in range(NC):
-                    low = 16 + ((core * 2 + h) * seqs + s) * tok
-                    at = pl.ds(pl.multiple_of(s * span + (1 + core - c) * tok, tok), tok)
-                    state_parts[x_at, at, lanes] = acts[k, low : low + tok, :]
-                low = (h * seqs + s) * tok
-                at = pl.ds(pl.multiple_of(s * span + 2 * c * tok, tok), tok)
-                state_parts[x_at, at, lanes] = beside[k, low : low + tok, :]
-        parts = acts[k, 0:16, :].astype(jnp.float32)
-        scales[x_at] = parts[0:layers] + parts[layers : 2 * layers] + parts[2 * layers : 3 * layers]
+
+    def place_tokens(acts):
+        for k in range(4):
+            x_at = lax.rem(x + k, NX)
+            for h in range(2):
+                lanes = slice(128 * h, 128 * (h + 1))
+                for s in range(seqs):
+                    for core in range(NC):
+                        low = 80 + ((core * 2 + h) * seqs + s) * tok
+                        at = pl.ds(pl.multiple_of(s * span + (1 + core - c) * tok, tok), tok)
+                        state_parts[x_at, at, lanes] = acts[k, low : low + tok, :]
+                    low = (h * seqs + s) * tok
+                    at = pl.ds(pl.multiple_of(s * span + 2 * c * tok, tok), tok)
+                    state_parts[x_at, at, lanes] = beside[k, low : low + tok, :]
+            terms = acts[k, 64:80, :].astype(jnp.float32)
+            scales[x_at] = (
+                terms[0:layers] + terms[layers : 2 * layers] + terms[2 * layers : 3 * layers]
+            )
+
+    for core in range(NC):
+        pl.when(c == core)(functools.partial(place_tokens, tokens[core]))
     put = put_layers(range(layers - 1), w_in, w_out, mix_raw)
     copy_blocks(place, ((refs[0:4], c), (refs[4:8], 1 - c)), FIRST, put)
     put = put_layers((layers - 1,), w_in, w_out)
@@ -200,7 +208,7 @@
 
 
 def pack(
-    layers, place_ref, in_ref, out_ref, mix_ref, scale_ref, act_ref, gain_ref, first, last, gain
+    layers, place_ref, in_ref, out_ref, mix_ref, scale_ref, act_ref, first, last
 ):
     for l in range(layers - 1):
         first[64 * l : 64 * l + 32, :] = in_ref[l]
@@ -220,7 +228,6 @@
         for s in range(seqs):
             at = pl.ds(pl.multiple_of(own + (h * seqs + s) * tok, 16), tok)
             last[at, :] = act_ref[s, :, 128 * h : 128 * (h + 1)]
-    gain[...] = gain_ref[...]
 
 
 def body(activations, norm_gain, in_weight, out_weight, mixing, pool_scale):
@@ -233,15 +240,14 @@
     place = jnp.stack([z, y, c, x]).astype(jnp.int32)
     vmem = pl.BlockSpec(memory_space=pltpu.VMEM)
     smem = pl.BlockSpec(memory_space=pltpu.SMEM)
-    first, last, gain = pl.pallas_call(
+    first, last = pl.pallas_call(
         functools.partial(pack, layers),
         out_shape=(
             jax.ShapeDtypeStruct((64 * layers - 48, 128), jnp.bfloat16),
             jax.ShapeDtypeStruct((80 + 4 * seqs * tok, 128), jnp.bfloat16),
-            jax.ShapeDtypeStruct(norm_gain.shape, jnp.float32),
         ),
-        in_specs=[smem] + [vmem] * 6,
-        out_specs=(vmem, vmem, vmem),
+        in_specs=[smem] + [vmem] * 5,
+        out_specs=(vmem, vmem),
         compiler_params=pltpu.CompilerParams(vmem_limit_bytes=2**21),
         cost_estimate=pl.CostEstimate(flops=10**6, bytes_accessed=3 * 10**5, transcendentals=0),
         name="pack",
@@ -252,7 +258,6 @@
         mixing.reshape(layers, 4, 128),
         pool_scale,
         activations,
-        norm_gain,
     )
     mate_rows = jnp.concatenate(
         [chip_mate.reshape(seqs * tok, width)[:, 128 * h : 128 * (h + 1)] for h in range(2)]
@@ -265,17 +270,16 @@
     p = jnp.stack(got)
     p = [p] + gather(p, FIRST, 1)
     q = jnp.stack([part[:64] for part in got_last])
-    tokens = jnp.stack([part[64:] for part in got_last])
-    tokens_2 = send(tokens, from_core())
     q = [q] + gather(q, LAST, 1)
 
     p = jnp.stack(p)
     p = [p] + gather(p, FIRST, 2)
-    tokens = jnp.where(c == 0, tokens, tokens_2)
-    mine = jnp.where(c == 0, tokens[:, 16 : 16 + count], tokens[:, 16 + count :])
-    beside = send(mine, across_chips())
     q = jnp.stack(q)
     q = [q] + gather(q, LAST, 2)
+    tokens = jnp.stack(got_last)
+    tokens_2 = send(tokens, from_core())
+    mine = jnp.where(c == 0, tokens[:, 80 : 80 + count], tokens_2[:, 80 + count :])
+    beside = send(mine, across_chips())
     p_2 = [send(p[0], from_core())]
     q_2 = [send(q[0], from_core())]
     p_2 += [send(part, from_core()) for part in p[1:]]
@@ -292,18 +296,19 @@
             jax.ShapeDtypeStruct((4, inner_rows, inner_rows), jnp.bfloat16),
             jax.ShapeDtypeStruct((4, inner_rows, 128), jnp.float32),
             jax.ShapeDtypeStruct((layers, 128, 512), jnp.bfloat16),
+            jax.ShapeDtypeStruct(norm_gain.shape, jnp.float32),
         ),
-        in_specs=[smem],
-        out_specs=(vmem,) * 5,
+        in_specs=[smem, vmem],
+        out_specs=(vmem,) * 6,
         compiler_params=pltpu.CompilerParams(vmem_limit_bytes=2**22),
         cost_estimate=pl.CostEstimate(flops=10**7, bytes_accessed=10**6, transcendentals=0),
         name="tables",
-    )(place)
+    )(place, norm_gain)
     weights = pltpu.VMEM((layers, 4, 1024, 128), jnp.bfloat16)
     result = pl.pallas_call(
         functools.partial(all_layers, dims),
         out_shape=jax.ShapeDtypeStruct((seqs * tok, width), jnp.bfloat16),
-        in_specs=[smem] + [vmem] * 24,
+        in_specs=[smem] + [vmem] * 25,
         out_specs=vmem,
         scratch_shapes=[
             weights,
@@ -317,7 +322,7 @@
             flops=2 * 10**9, bytes_accessed=18 * 10**6, transcendentals=1000
         ),
         name="all_layers",
-    )(place, *p, *p_2, *q, *q_2, tokens, beside, gain, *made)
+    )(place, *p, *p_2, *q, *q_2, tokens, tokens_2, beside, *made)
     return result.reshape(seqs, tok, width)
 
 

time: 66.7 us -> 81.7 us (1.22)
  the two profiles are of different devices: /device:TPU:1 before, /device:TPU:0 now
where the time goes in v5:
time: 81.7 us; the launch traced here: 80.4 us
  waiting for transfers between devices  37.5 us (46%)
  starting transfers between devices  29.4 us (36%)
  Pallas kernels  9.82 us (12%)
  local copies, waits for them, and re-layouts  3.08 us (4%)
    ppermute x29, waiting for transfers between devices, send(): return lax.ppermute(value, AXES, perm)  37.5 us
    ppermute x29, starting transfers between devices, send(): return lax.ppermute(value, AXES, perm)  29.4 us
    pallas_call x1, Pallas kernels, body(): pl.pallas_call(functools.partial(all_layers, dims), out_shape=jax.ShapeDt...  8.15 us
    unnamed x20, local copies, waits for them, and re-layouts  3.06 us
  transfers between devices with their start and end apart: 29, of which 11 were waited for; matrix products, arithmetic and copies ran while one was open for 0% of the time, Pallas kernels for 2%

profile of v5, /device:TPU:0, one launch (start us, length us, event | category | flops | bytes accessed | tf_op | source)
XLA Modules:
  0.0 80.4 jit_solution(3284815497790068148)
XLA Ops:
  0.1 0.1 pad_add_fusion.place_ref
  0.1 0.5 copy-done.8
  0.7 0.0 copy-done.7
  0.7 0.1 copy-done.6
  0.8 0.6 pack.1
  1.4 1.7 %collective-permute-start.2 = (bf16[208,128]{1,0:T(8,128)(2,1)S(1)}, bf16[208,128]{1,0:T(8,128)(2,1)S(1)}, u32[]{:S(2)}, u32[]{:S(2)}) collective-permute-start(bf16[208,128]{1,0:T(8,128)(2,1)S(1)} %get-tuple-element.13), channel_id=1, source_target_pairs={{3,0},{0,1},{1,2},{2,3},{100,4},{101,5},{102,6},{103,7},{11,8},{8,... | collective-permute-start | bytes 159752 | tf_op jit(solution)/shard_map/ppermute | solution.py:59
  3.1 2.7 %collective-permute-start.1 = (bf16[208,128]{1,0:T(8,128)(2,1)S(1)}, bf16[208,128]{1,0:T(8,128)(2,1)S(1)}, u32[]{:S(2)}, u32[]{:S(2)}) collective-permute-start(bf16[208,128]{1,0:T(8,128)(2,1)S(1)} %get-tuple-element.13), channel_id=1, source_target_pairs={{2,0},{3,1},{0,2},{1,3},{68,4},{69,5},{70,6},{71,7},{10,8},{11,9},... | collective-permute-start | bytes 159752 | tf_op jit(solution)/shard_map/ppermute | solution.py:59
  5.8 1.4 %collective-permute-start = (bf16[208,128]{1,0:T(8,128)(2,1)S(1)}, bf16[208,128]{1,0:T(8,128)(2,1)S(1)}, u32[]{:S(2)}, u32[]{:S(2)}) collective-permute-start(bf16[208,128]{1,0:T(8,128)(2,1)S(1)} %get-tuple-element.13), channel_id=1, source_target_pairs={{1,0},{2,1},{3,2},{0,3},{36,4},{37,5},{38,6},{39,7},{9,8},{10,9},{... | collective-permute-start | bytes 159752 | tf_op jit(solution)/shard_map/ppermute | solution.py:59
  7.2 0.7 collective-permute-start.16
  7.9 0.9 %collective-permute-start.15 = (bf16[336,128]{1,0:T(8,128)(2,1)S(1)}, bf16[336,128]{1,0:T(8,128)(2,1)S(1)}, u32[]{:S(2)}, u32[]{:S(2)}) collective-permute-start(bf16[336,128]{1,0:T(8,128)(2,1)S(1)} %maximum_dynamic-update-slice_fusion), channel_id=1, source_target_pairs={{2,0},{3,1},{0,2},{1,3},{20,4},{21,5},{22,6},{23,7},{10,8},{11,9},... | collective-permute-start | bytes 258056 | tf_op jit(solution)/shard_map/ppermute | solution.py:59
  8.8 4.2 %collective-permute-done.16 = bf16[336,128]{1,0:T(8,128)(2,1)S(1)} collective-permute-done((bf16[336,128]{1,0:T(8,128)(2,1)S(1)}, bf16[336,128]{1,0:T(8,128)(2,1)S(1)}, u32[]{:S(2)}, u32[]{:S(2)}) %collective-permute-start.16) | collective-permute-done | bytes 86048 | tf_op jit(solution)/shard_map/ppermute | solution.py:59
  13.0 0.9 %collective-permute-done.15 = bf16[336,128]{1,0:T(8,128)(2,1)S(1)} collective-permute-done((bf16[336,128]{1,0:T(8,128)(2,1)S(1)}, bf16[336,128]{1,0:T(8,128)(2,1)S(1)}, u32[]{:S(2)}, u32[]{:S(2)}) %collective-permute-start.15) | collective-permute-done | bytes 86048 | tf_op jit(solution)/shard_map/ppermute | solution.py:59
  13.9 3.6 %collective-permute-done.14 = bf16[336,128]{1,0:T(8,128)(2,1)S(1)} collective-permute-done((bf16[336,128]{1,0:T(8,128)(2,1)S(1)}, bf16[336,128]{1,0:T(8,128)(2,1)S(1)}, u32[]{:S(2)}, u32[]{:S(2)}) %collective-permute-start.14) | collective-permute-done | bytes 86048 | tf_op jit(solution)/shard_map/ppermute | solution.py:59
  17.5 3.3 %collective-permute-start.18 = (bf16[4,64,128]{2,1,0:T(8,128)(2,1)S(1)}, bf16[4,64,128]{2,1,0:T(8,128)(2,1)S(1)}, u32[]{:S(2)}, u32[]{:S(2)}) collective-permute-start(bf16[4,64,128]{2,1,0:T(8,128)(2,1)S(1)} %get-tuple-element.24), channel_id=1, source_target_pairs={{16,0},{17,1},{18,2},{19,3},{6,4},{7,5},{4,6},{5,7},{24,8},{25,9},... | collective-permute-start | bytes 196616 | tf_op jit(solution)/shard_map/ppermute | solution.py:59
  20.9 4.1 %collective-permute-start.4 = (bf16[4,208,128]{2,1,0:T(8,128)(2,1)S(1)}, bf16[4,208,128]{2,1,0:T(8,128)(2,1)S(1)}, u32[]{:S(2)}, u32[]{:S(2)}) collective-permute-start(bf16[4,208,128]{2,1,0:T(8,128)(2,1)S(1)} %get-tuple-element.22), channel_id=1, source_target_pairs={{64,0},{65,1},{66,2},{67,3},{20,4},{21,5},{22,6},{23,7},{72,8},{73... | collective-permute-start | bytes 638984 | tf_op jit(solution)/shard_map/ppermute | solution.py:59
  25.0 0.6 collective-permute-start.3
  25.5 1.5 %collective-permute-start.5 = (bf16[4,208,128]{2,1,0:T(8,128)(2,1)S(1)}, bf16[4,208,128]{2,1,0:T(8,128)(2,1)S(1)}, u32[]{:S(2)}, u32[]{:S(2)}) collective-permute-start(bf16[4,208,128]{2,1,0:T(8,128)(2,1)S(1)} %get-tuple-element.22), channel_id=1, source_target_pairs={{96,0},{97,1},{98,2},{99,3},{28,4},{29,5},{30,6},{31,7},{104,8},{1... | collective-permute-start | bytes 638984 | tf_op jit(solution)/shard_map/ppermute | solution.py:59
  27.0 1.1 %collective-permute-start.17 = (bf16[4,64,128]{2,1,0:T(8,128)(2,1)S(1)}, bf16[4,64,128]{2,1,0:T(8,128)(2,1)S(1)}, u32[]{:S(2)}, u32[]{:S(2)}) collective-permute-start(bf16[4,64,128]{2,1,0:T(8,128)(2,1)S(1)} %get-tuple-element.24), channel_id=1, source_target_pairs={{8,0},{9,1},{10,2},{11,3},{5,4},{6,5},{7,6},{4,7},{16,8},{17,9},{1... | collective-permute-start | bytes 196616 | tf_op jit(solution)/shard_map/ppermute | solution.py:59
  28.1 0.9 %collective-permute-start.19 = (bf16[4,64,128]{2,1,0:T(8,128)(2,1)S(1)}, bf16[4,64,128]{2,1,0:T(8,128)(2,1)S(1)}, u32[]{:S(2)}, u32[]{:S(2)}) collective-permute-start(bf16[4,64,128]{2,1,0:T(8,128)(2,1)S(1)} %get-tuple-element.24), channel_id=1, source_target_pairs={{24,0},{25,1},{26,2},{27,3},{7,4},{4,5},{5,6},{6,7},{0,8},{1,9},{2... | collective-permute-start | bytes 196616 | tf_op jit(solution)/shard_map/ppermute | solution.py:59
  29.0 2.2 %collective-permute-done.17 = bf16[4,64,128]{2,1,0:T(8,128)(2,1)S(1)} collective-permute-done((bf16[4,64,128]{2,1,0:T(8,128)(2,1)S(1)}, bf16[4,64,128]{2,1,0:T(8,128)(2,1)S(1)}, u32[]{:S(2)}, u32[]{:S(2)}) %collective-permute-start.17) | collective-permute-done | bytes 65568 | tf_op jit(solution)/shard_map/ppermute | solution.py:59
  31.3 2.4 %collective-permute-done.19 = bf16[4,64,128]{2,1,0:T(8,128)(2,1)S(1)} collective-permute-done((bf16[4,64,128]{2,1,0:T(8,128)(2,1)S(1)}, bf16[4,64,128]{2,1,0:T(8,128)(2,1)S(1)}, u32[]{:S(2)}, u32[]{:S(2)}) %collective-permute-start.19) | collective-permute-done | bytes 65568 | tf_op jit(solution)/shard_map/ppermute | solution.py:59
  33.7 0.1 collective-permute-start.23
  33.8 0.1 pad_maximum_fusion.refs_0_
  33.9 0.1 collective-permute-start.8
  34.0 1.4 %collective-permute-start.7 = (bf16[4,4,208,128]{3,2,1,0:T(8,128)(2,1)S(1)}, bf16[4,4,208,128]{3,2,1,0:T(8,128)(2,1)S(1)}, u32[]{:S(2)}, u32[]{:S(2)}) collective-permute-start(bf16[4,4,208,128]{3,2,1,0:T(8,128)(2,1)S(1)} %pad_maximum_fusion.refs_0_), channel_id=1, source_target_pairs={{16,0},{17,1},{18,2},{19,3},{6,4},{7,5},{4,6},{5,7},{24,8},{25,9},... | collective-permute-start | bytes 2555912 | tf_op jit(solution)/shard_map/ppermute | solution.py:59
  35.4 1.8 %collective-permute-start.6 = (bf16[4,4,208,128]{3,2,1,0:T(8,128)(2,1)S(1)}, bf16[4,4,208,128]{3,2,1,0:T(8,128)(2,1)}, u32[]{:S(2)}, u32[]{:S(2)}) collective-permute-start(bf16[4,4,208,128]{3,2,1,0:T(8,128)(2,1)S(1)} %pad_maximum_fusion.refs_0_), channel_id=1, source_target_pairs={{8,0},{9,1},{10,2},{11,3},{5,4},{6,5},{7,6},{4,7},{16,8},{17,9},{1... | collective-permute-start | bytes 2555912 | tf_op jit(solution)/shard_map/ppermute | solution.py:59
  37.3 0.1 collective-permute-start.27
  37.4 0.7 copy-done
  38.1 1.3 %collective-permute-start.22 = (bf16[4,4,64,128]{3,2,1,0:T(8,128)(2,1)S(1)}, bf16[4,4,64,128]{3,2,1,0:T(8,128)(2,1)S(1)}, u32[]{:S(2)}, u32[]{:S(2)}) collective-permute-start(bf16[4,4,64,128]{3,2,1,0:T(8,128)(2,1)S(1)} %pad_maximum_fusion.2.refs_8_), channel_id=1, source_target_pairs={{96,0},{97,1},{98,2},{99,3},{100,4},{101,5},{102,6},{103,7},{104,8... | collective-permute-start | bytes 786440 | tf_op jit(solution)/shard_map/ppermute | solution.py:59
  39.4 8.6 %collective-permute-done.22.refs_11_ = bf16[4,4,64,128]{3,2,1,0:T(8,128)(2,1)S(1)} collective-permute-done((bf16[4,4,64,128]{3,2,1,0:T(8,128)(2,1)S(1)}, bf16[4,4,64,128]{3,2,1,0:T(8,128)(2,1)S(1)}, u32[]{:S(2)}, u32[]{:S(2)}) %collective-permute-start.22) | collective-permute-done | bytes 262176 | tf_op jit(solution)/shard_map/ppermute | solution.py:59
  48.0 0.7 copy-done.2
  48.7 0.4 collective-permute-start.21
  49.2 2.3 %collective-permute-start.20 = (bf16[4,4,64,128]{3,2,1,0:T(8,128)(2,1)S(1)}, bf16[4,4,64,128]{3,2,1,0:T(8,128)(2,1)S(1)}, u32[]{:S(2)}, u32[]{:S(2)}) collective-permute-start(bf16[4,4,64,128]{3,2,1,0:T(8,128)(2,1)S(1)} %pad_maximum_fusion.2.refs_8_), channel_id=1, source_target_pairs={{32,0},{33,1},{34,2},{35,3},{36,4},{37,5},{38,6},{39,7},{40,8},{41... | collective-permute-start | bytes 786440 | tf_op jit(solution)/shard_map/ppermute | solution.py:59
  51.5 6.7 %collective-permute-done.21.refs_10_ = bf16[4,4,64,128]{3,2,1,0:T(8,128)(2,1)} collective-permute-done((bf16[4,4,64,128]{3,2,1,0:T(8,128)(2,1)S(1)}, bf16[4,4,64,128]{3,2,1,0:T(8,128)(2,1)}, u32[]{:S(2)}, u32[]{:S(2)}) %collective-permute-start.21) | collective-permute-done | bytes 262176 | tf_op jit(solution)/shard_map/ppermute | solution.py:59
  58.2 0.7 collective-permute-start.28
  58.8 2.8 %collective-permute-done.20.refs_9_ = bf16[4,4,64,128]{3,2,1,0:T(8,128)(2,1)S(1)} collective-permute-done((bf16[4,4,64,128]{3,2,1,0:T(8,128)(2,1)S(1)}, bf16[4,4,64,128]{3,2,1,0:T(8,128)(2,1)S(1)}, u32[]{:S(2)}, u32[]{:S(2)}) %collective-permute-start.20) | collective-permute-done | bytes 262176 | tf_op jit(solution)/shard_map/ppermute | solution.py:59
  61.6 0.5 collective-permute-start.12
  62.1 0.1 collective-permute-start.11
  62.2 0.4 collective-permute-start.10
  62.6 1.1 %collective-permute-start.26 = (bf16[4,4,64,128]{3,2,1,0:T(8,128)(2,1)}, bf16[4,4,64,128]{3,2,1,0:T(8,128)(2,1)S(1)}, u32[]{:S(2)}, u32[]{:S(2)}) collective-permute-start(bf16[4,4,64,128]{3,2,1,0:T(8,128)(2,1)} %copy-done.2), channel_id=1, source_target_pairs={{4,0},{5,1},{6,2},{7,3},{0,4},{1,5},{2,6},{3,7},{12,8},{13,9},{14,... | collective-permute-start | bytes 786440 | tf_op jit(solution)/shard_map/ppermute | solution.py:59
  63.7 4.3 %collective-permute-done.26.refs_15_ = bf16[4,4,64,128]{3,2,1,0:T(8,128)(2,1)S(1)} collective-permute-done((bf16[4,4,64,128]{3,2,1,0:T(8,128)(2,1)}, bf16[4,4,64,128]{3,2,1,0:T(8,128)(2,1)S(1)}, u32[]{:S(2)}, u32[]{:S(2)}) %collective-permute-start.26) | collective-permute-done | bytes 262176 | tf_op jit(solution)/shard_map/ppermute | solution.py:59
  68.0 0.1 collective-permute-start.25
  68.1 1.6 %collective-permute-done.25.refs_14_ = bf16[4,4,64,128]{3,2,1,0:T(8,128)(2,1)S(1)} collective-permute-done((bf16[4,4,64,128]{3,2,1,0:T(8,128)(2,1)}, bf16[4,4,64,128]{3,2,1,0:T(8,128)(2,1)S(1)}, u32[]{:S(2)}, u32[]{:S(2)}) %collective-permute-start.25) | collective-permute-done | bytes 262176 | tf_op jit(solution)/shard_map/ppermute | solution.py:59
  69.7 0.1 collective-permute-start.24
  69.9 1.1 %tables.1 = (bf16[4,192,192]{2,1,0:T(8,128)(2,1)S(1)}, f32[4,192,128]{2,1,0:T(8,128)S(1)}, bf16[4,128,128]{2,1,0:T(8,128)(2,1)S(1)}, f32[4,128,128]{2,1,0:T(8,12...) custom-call(s32[4]{0:T(128)S(1)} %pad_add_fusion.place_ref, f32[4,1024]{1,0:T(4,128)S(1)} %copy-done.9), custom_call_target="tpu_custom_call" | custom-call | flops 10000000 | bytes 1000000 | tf_op jit(solution)/shard_map/tables/pallas_call | solution.py:291
  71.0 0.3 collective-permute-done.24.refs_13_
  71.3 0.9 %copy-done.3 = bf16[4,4,64,128]{3,2,1,0:T(8,128)(2,1)S(1)} copy-done((bf16[4,4,64,128]{3,2,1,0:T(8,128)(2,1)S(1)}, bf16[4,4,64,128]{3,2,1,0:T(8,128)(2,1)}, u32[]{:S(2)}) %copy-start.3) | copy-done | bytes 262168
  72.3 8.1 %all_layers.1 = bf16[64,256]{1,0:T(8,128)(2,1)} custom-call(s32[4]{0:T(128)S(1)} %pad_add_fusion.place_ref, bf16[4,4,208,128]{3,2,1,0:T(8,128)(2,1)S(1)} %pad_maximum_fusion.refs_0_, bf16[4,4,208,128]{3,2,1,0:T(8,128)(2,1)} %collective-permute-done.6.refs_1_, bf16[4,4,208,128]{3,2,1,0:T(8,128)(2,1)S(1)} %collective-permute-done.7.refs_2_, ...), custom_call_target="tpu_custom_call" | custom-call | flops 2000000000 | bytes 18000000 | tf_op jit(solution)/shard_map/all_layers/pallas_call | solution.py:308
  (46 shorter events, 0.3 us)
Async XLA Ops:
  0.0 7.2 %collective-permute-start.13 = (bf16[2,32,256]{2,1,0:T(8,128)(2,1)}, bf16[2,32,256]{2,1,0:T(8,128)(2,1)S(1)}, u32[]{:S(2)}, u32[]{:S(2)}) collective-permute-start(bf16[2,32,256]{2,1,0:T(8,128)(2,1)} %act_ref.1), channel_id=1, source_target_pairs={{4,0},{5,1},{6,2},{7,3},{0,4},{1,5},{2,6},{3,7},{12,8},{13,9},{14,... | collective-permute-start | bytes 98312 | tf_op jit(solution)/shard_map/ppermute | solution.py:59
  0.0 0.7 copy-start.8
  0.0 0.7 copy-start.7
  0.0 0.8 copy-start.6
  0.0 0.8 copy-start.5
  0.0 0.8 copy-start.4
  1.4 19.4 %collective-permute-start.2 = (bf16[208,128]{1,0:T(8,128)(2,1)S(1)}, bf16[208,128]{1,0:T(8,128)(2,1)S(1)}, u32[]{:S(2)}, u32[]{:S(2)}) collective-permute-start(bf16[208,128]{1,0:T(8,128)(2,1)S(1)} %get-tuple-element.13), channel_id=1, source_target_pairs={{3,0},{0,1},{1,2},{2,3},{100,4},{101,5},{102,6},{103,7},{11,8},{8,... | collective-permute-start | bytes 159752 | tf_op jit(solution)/shard_map/ppermute | solution.py:59
  3.1 17.7 %collective-permute-start.1 = (bf16[208,128]{1,0:T(8,128)(2,1)S(1)}, bf16[208,128]{1,0:T(8,128)(2,1)S(1)}, u32[]{:S(2)}, u32[]{:S(2)}) collective-permute-start(bf16[208,128]{1,0:T(8,128)(2,1)S(1)} %get-tuple-element.13), channel_id=1, source_target_pairs={{2,0},{3,1},{0,2},{1,3},{68,4},{69,5},{70,6},{71,7},{10,8},{11,9},... | collective-permute-start | bytes 159752 | tf_op jit(solution)/shard_map/ppermute | solution.py:59
  5.8 15.0 %collective-permute-start = (bf16[208,128]{1,0:T(8,128)(2,1)S(1)}, bf16[208,128]{1,0:T(8,128)(2,1)S(1)}, u32[]{:S(2)}, u32[]{:S(2)}) collective-permute-start(bf16[208,128]{1,0:T(8,128)(2,1)S(1)} %get-tuple-element.13), channel_id=1, source_target_pairs={{1,0},{2,1},{3,2},{0,3},{36,4},{37,5},{38,6},{39,7},{9,8},{10,9},{... | collective-permute-start | bytes 159752 | tf_op jit(solution)/shard_map/ppermute | solution.py:59
  7.2 5.8 %collective-permute-start.16 = (bf16[336,128]{1,0:T(8,128)(2,1)S(1)}, bf16[336,128]{1,0:T(8,128)(2,1)S(1)}, u32[]{:S(2)}, u32[]{:S(2)}) collective-permute-start(bf16[336,128]{1,0:T(8,128)(2,1)S(1)} %maximum_dynamic-update-slice_fusion), channel_id=1, source_target_pairs={{3,0},{0,1},{1,2},{2,3},{28,4},{29,5},{30,6},{31,7},{11,8},{8,9},{... | collective-permute-start | bytes 258056 | tf_op jit(solution)/shard_map/ppermute | solution.py:59
  7.9 6.0 %collective-permute-start.15 = (bf16[336,128]{1,0:T(8,128)(2,1)S(1)}, bf16[336,128]{1,0:T(8,128)(2,1)S(1)}, u32[]{:S(2)}, u32[]{:S(2)}) collective-permute-start(bf16[336,128]{1,0:T(8,128)(2,1)S(1)} %maximum_dynamic-update-slice_fusion), channel_id=1, source_target_pairs={{2,0},{3,1},{0,2},{1,3},{20,4},{21,5},{22,6},{23,7},{10,8},{11,9},... | collective-permute-start | bytes 258056 | tf_op jit(solution)/shard_map/ppermute | solution.py:59
  13.0 4.5 %collective-permute-start.14 = (bf16[336,128]{1,0:T(8,128)(2,1)S(1)}, bf16[336,128]{1,0:T(8,128)(2,1)S(1)}, u32[]{:S(2)}, u32[]{:S(2)}) collective-permute-start(bf16[336,128]{1,0:T(8,128)(2,1)S(1)} %maximum_dynamic-update-slice_fusion), channel_id=1, source_target_pairs={{1,0},{2,1},{3,2},{0,3},{12,4},{13,5},{14,6},{15,7},{9,8},{10,9},{... | collective-permute-start | bytes 258056 | tf_op jit(solution)/shard_map/ppermute | solution.py:59
  17.5 10.6 %collective-permute-start.18 = (bf16[4,64,128]{2,1,0:T(8,128)(2,1)S(1)}, bf16[4,64,128]{2,1,0:T(8,128)(2,1)S(1)}, u32[]{:S(2)}, u32[]{:S(2)}) collective-permute-start(bf16[4,64,128]{2,1,0:T(8,128)(2,1)S(1)} %get-tuple-element.24), channel_id=1, source_target_pairs={{16,0},{17,1},{18,2},{19,3},{6,4},{7,5},{4,6},{5,7},{24,8},{25,9},... | collective-permute-start | bytes 196616 | tf_op jit(solution)/shard_map/ppermute | solution.py:59
  20.9 12.9 %collective-permute-start.4 = (bf16[4,208,128]{2,1,0:T(8,128)(2,1)S(1)}, bf16[4,208,128]{2,1,0:T(8,128)(2,1)S(1)}, u32[]{:S(2)}, u32[]{:S(2)}) collective-permute-start(bf16[4,208,128]{2,1,0:T(8,128)(2,1)S(1)} %get-tuple-element.22), channel_id=1, source_target_pairs={{64,0},{65,1},{66,2},{67,3},{20,4},{21,5},{22,6},{23,7},{72,8},{73... | collective-permute-start | bytes 638984 | tf_op jit(solution)/shard_map/ppermute | solution.py:59
  25.0 8.8 %collective-permute-start.3 = (bf16[4,208,128]{2,1,0:T(8,128)(2,1)S(1)}, bf16[4,208,128]{2,1,0:T(8,128)(2,1)S(1)}, u32[]{:S(2)}, u32[]{:S(2)}) collective-permute-start(bf16[4,208,128]{2,1,0:T(8,128)(2,1)S(1)} %get-tuple-element.22), channel_id=1, source_target_pairs={{32,0},{33,1},{34,2},{35,3},{12,4},{13,5},{14,6},{15,7},{40,8},{41... | collective-permute-start | bytes 638984 | tf_op jit(solution)/shard_map/ppermute | solution.py:59
  25.5 8.3 %collective-permute-start.5 = (bf16[4,208,128]{2,1,0:T(8,128)(2,1)S(1)}, bf16[4,208,128]{2,1,0:T(8,128)(2,1)S(1)}, u32[]{:S(2)}, u32[]{:S(2)}) collective-permute-start(bf16[4,208,128]{2,1,0:T(8,128)(2,1)S(1)} %get-tuple-element.22), channel_id=1, source_target_pairs={{96,0},{97,1},{98,2},{99,3},{28,4},{29,5},{30,6},{31,7},{104,8},{1... | collective-permute-start | bytes 638984 | tf_op jit(solution)/shard_map/ppermute | solution.py:59
  27.0 4.3 %collective-permute-start.17 = (bf16[4,64,128]{2,1,0:T(8,128)(2,1)S(1)}, bf16[4,64,128]{2,1,0:T(8,128)(2,1)S(1)}, u32[]{:S(2)}, u32[]{:S(2)}) collective-permute-start(bf16[4,64,128]{2,1,0:T(8,128)(2,1)S(1)} %get-tuple-element.24), channel_id=1, source_target_pairs={{8,0},{9,1},{10,2},{11,3},{5,4},{6,5},{7,6},{4,7},{16,8},{17,9},{1... | collective-permute-start | bytes 196616 | tf_op jit(solution)/shard_map/ppermute | solution.py:59
  28.1 5.5 %collective-permute-start.19 = (bf16[4,64,128]{2,1,0:T(8,128)(2,1)S(1)}, bf16[4,64,128]{2,1,0:T(8,128)(2,1)S(1)}, u32[]{:S(2)}, u32[]{:S(2)}) collective-permute-start(bf16[4,64,128]{2,1,0:T(8,128)(2,1)S(1)} %get-tuple-element.24), channel_id=1, source_target_pairs={{24,0},{25,1},{26,2},{27,3},{7,4},{4,5},{5,6},{6,7},{0,8},{1,9},{2... | collective-permute-start | bytes 196616 | tf_op jit(solution)/shard_map/ppermute | solution.py:59
  33.7 3.7 %collective-permute-start.23 = (bf16[4,4,64,128]{3,2,1,0:T(8,128)(2,1)S(1)}, bf16[4,4,64,128]{3,2,1,0:T(8,128)(2,1)S(1)}, u32[]{:S(2)}, u32[]{:S(2)}) collective-permute-start(bf16[4,4,64,128]{3,2,1,0:T(8,128)(2,1)S(1)} %pad_maximum_fusion.2.refs_8_), channel_id=1, source_target_pairs={{4,0},{5,1},{6,2},{7,3},{0,4},{1,5},{2,6},{3,7},{12,8},{13,9},{14,... | collective-permute-start | bytes 786440 | tf_op jit(solution)/shard_map/ppermute | solution.py:59
  33.9 27.7 %collective-permute-start.8 = (bf16[4,4,208,128]{3,2,1,0:T(8,128)(2,1)S(1)}, bf16[4,4,208,128]{3,2,1,0:T(8,128)(2,1)S(1)}, u32[]{:S(2)}, u32[]{:S(2)}) collective-permute-start(bf16[4,4,208,128]{3,2,1,0:T(8,128)(2,1)S(1)} %pad_maximum_fusion.refs_0_), channel_id=1, source_target_pairs={{24,0},{25,1},{26,2},{27,3},{7,4},{4,5},{5,6},{6,7},{0,8},{1,9},{2... | collective-permute-start | bytes 2555912 | tf_op jit(solution)/shard_map/ppermute | solution.py:59
  34.0 28.1 %collective-permute-start.7 = (bf16[4,4,208,128]{3,2,1,0:T(8,128)(2,1)S(1)}, bf16[4,4,208,128]{3,2,1,0:T(8,128)(2,1)S(1)}, u32[]{:S(2)}, u32[]{:S(2)}) collective-permute-start(bf16[4,4,208,128]{3,2,1,0:T(8,128)(2,1)S(1)} %pad_maximum_fusion.refs_0_), channel_id=1, source_target_pairs={{16,0},{17,1},{18,2},{19,3},{6,4},{7,5},{4,6},{5,7},{24,8},{25,9},... | collective-permute-start | bytes 2555912 | tf_op jit(solution)/shard_map/ppermute | solution.py:59
  35.4 26.8 %collective-permute-start.6 = (bf16[4,4,208,128]{3,2,1,0:T(8,128)(2,1)S(1)}, bf16[4,4,208,128]{3,2,1,0:T(8,128)(2,1)}, u32[]{:S(2)}, u32[]{:S(2)}) collective-permute-start(bf16[4,4,208,128]{3,2,1,0:T(8,128)(2,1)S(1)} %pad_maximum_fusion.refs_0_), channel_id=1, source_target_pairs={{8,0},{9,1},{10,2},{11,3},{5,4},{6,5},{7,6},{4,7},{16,8},{17,9},{1... | collective-permute-start | bytes 2555912 | tf_op jit(solution)/shard_map/ppermute | solution.py:59
  37.3 11.9 %collective-permute-start.27 = (bf16[4,336,128]{2,1,0:T(8,128)(2,1)S(1)}, bf16[4,336,128]{2,1,0:T(8,128)(2,1)S(1)}, u32[]{:S(2)}, u32[]{:S(2)}) collective-permute-start(bf16[4,336,128]{2,1,0:T(8,128)(2,1)S(1)} %pad_maximum_fusion.1.refs_16_), channel_id=1, source_target_pairs={{4,0},{5,1},{6,2},{7,3},{0,4},{1,5},{2,6},{3,7},{12,8},{13,9},{14,... | collective-permute-start | bytes 1032200 | tf_op jit(solution)/shard_map/ppermute | solution.py:59
  37.4 0.7 copy-start
  38.1 9.9 %collective-permute-start.22 = (bf16[4,4,64,128]{3,2,1,0:T(8,128)(2,1)S(1)}, bf16[4,4,64,128]{3,2,1,0:T(8,128)(2,1)S(1)}, u32[]{:S(2)}, u32[]{:S(2)}) collective-permute-start(bf16[4,4,64,128]{3,2,1,0:T(8,128)(2,1)S(1)} %pad_maximum_fusion.2.refs_8_), channel_id=1, source_target_pairs={{96,0},{97,1},{98,2},{99,3},{100,4},{101,5},{102,6},{103,7},{104,8... | collective-permute-start | bytes 786440 | tf_op jit(solution)/shard_map/ppermute | solution.py:59
  48.0 0.7 copy-start.2
  48.7 9.5 %collective-permute-start.21 = (bf16[4,4,64,128]{3,2,1,0:T(8,128)(2,1)S(1)}, bf16[4,4,64,128]{3,2,1,0:T(8,128)(2,1)}, u32[]{:S(2)}, u32[]{:S(2)}) collective-permute-start(bf16[4,4,64,128]{3,2,1,0:T(8,128)(2,1)S(1)} %pad_maximum_fusion.2.refs_8_), channel_id=1, source_target_pairs={{64,0},{65,1},{66,2},{67,3},{68,4},{69,5},{70,6},{71,7},{72,8},{73... | collective-permute-start | bytes 786440 | tf_op jit(solution)/shard_map/ppermute | solution.py:59
  49.1 20.7 %copy-start.9 = (f32[4,1024]{1,0:T(4,128)S(1)}, f32[4,1024]{1,0:T(4,128)}, u32[]{:S(2)}) copy-start(f32[4,1024]{1,0:T(4,128)} %gain_ref.1) | copy-start | bytes 49156
  49.1 22.2 %copy-start.1 = (bf16[4,4,64,128]{3,2,1,0:T(8,128)(2,1)S(1)}, bf16[4,4,64,128]{3,2,1,0:T(8,128)(2,1)}, u32[]{:S(2)}) copy-start(bf16[4,4,64,128]{3,2,1,0:T(8,128)(2,1)} %copy-done) | copy-start | bytes 786436
  49.2 12.4 %collective-permute-start.20 = (bf16[4,4,64,128]{3,2,1,0:T(8,128)(2,1)S(1)}, bf16[4,4,64,128]{3,2,1,0:T(8,128)(2,1)S(1)}, u32[]{:S(2)}, u32[]{:S(2)}) collective-permute-start(bf16[4,4,64,128]{3,2,1,0:T(8,128)(2,1)S(1)} %pad_maximum_fusion.2.refs_8_), channel_id=1, source_target_pairs={{32,0},{33,1},{34,2},{35,3},{36,4},{37,5},{38,6},{39,7},{40,8},{41... | collective-permute-start | bytes 786440 | tf_op jit(solution)/shard_map/ppermute | solution.py:59
  58.2 4.5 %collective-permute-start.28 = (bf16[4,128,128]{2,1,0:T(8,128)(2,1)S(1)}, bf16[4,128,128]{2,1,0:T(8,128)(2,1)S(1)}, u32[]{:S(2)}, u32[]{:S(2)}) collective-permute-start(bf16[4,128,128]{2,1,0:T(8,128)(2,1)S(1)} %slice_select_fusion), channel_id=1, source_target_pairs={{4,8},{8,4},{5,9},{9,5},{6,10},{10,6},{7,11},{11,7},{12,16},{16,12... | collective-permute-start | bytes 393224 | tf_op jit(solution)/shard_map/ppermute | solution.py:59
  61.6 9.7 %collective-permute-start.9 = (bf16[4,4,208,128]{3,2,1,0:T(8,128)(2,1)S(1)}, bf16[4,4,208,128]{3,2,1,0:T(8,128)(2,1)S(1)}, u32[]{:S(2)}, u32[]{:S(2)}) collective-permute-start(bf16[4,4,208,128]{3,2,1,0:T(8,128)(2,1)S(1)} %pad_maximum_fusion.refs_0_), channel_id=1, source_target_pairs={{4,0},{5,1},{6,2},{7,3},{0,4},{1,5},{2,6},{3,7},{12,8},{13,9},{14,... | collective-permute-start | bytes 2555912 | tf_op jit(solution)/shard_map/ppermute | solution.py:59
  61.6 9.7 %collective-permute-start.12 = (bf16[4,4,208,128]{3,2,1,0:T(8,128)(2,1)S(1)}, bf16[4,4,208,128]{3,2,1,0:T(8,128)(2,1)S(1)}, u32[]{:S(2)}, u32[]{:S(2)}) collective-permute-start(bf16[4,4,208,128]{3,2,1,0:T(8,128)(2,1)S(1)} %collective-permute-done.8.refs_3_), channel_id=1, source_target_pairs={{4,0},{5,1},{6,2},{7,3},{0,4},{1,5},{2,6},{3,7},{12,8},{13,9},{14,... | collective-permute-start | bytes 2555912 | tf_op jit(solution)/shard_map/ppermute | solution.py:59
  62.1 9.2 %collective-permute-start.11 = (bf16[4,4,208,128]{3,2,1,0:T(8,128)(2,1)S(1)}, bf16[4,4,208,128]{3,2,1,0:T(8,128)(2,1)S(1)}, u32[]{:S(2)}, u32[]{:S(2)}) collective-permute-start(bf16[4,4,208,128]{3,2,1,0:T(8,128)(2,1)S(1)} %collective-permute-done.7.refs_2_), channel_id=1, source_target_pairs={{4,0},{5,1},{6,2},{7,3},{0,4},{1,5},{2,6},{3,7},{12,8},{13,9},{14,... | collective-permute-start | bytes 2555912 | tf_op jit(solution)/shard_map/ppermute | solution.py:59
  62.2 9.1 %collective-permute-start.10 = (bf16[4,4,208,128]{3,2,1,0:T(8,128)(2,1)}, bf16[4,4,208,128]{3,2,1,0:T(8,128)(2,1)S(1)}, u32[]{:S(2)}, u32[]{:S(2)}) collective-permute-start(bf16[4,4,208,128]{3,2,1,0:T(8,128)(2,1)} %collective-permute-done.6.refs_1_), channel_id=1, source_target_pairs={{4,0},{5,1},{6,2},{7,3},{0,4},{1,5},{2,6},{3,7},{12,8},{13,9},{14,... | collective-permute-start | bytes 2555912 | tf_op jit(solution)/shard_map/ppermute | solution.py:59
  62.6 5.4 %collective-permute-start.26 = (bf16[4,4,64,128]{3,2,1,0:T(8,128)(2,1)}, bf16[4,4,64,128]{3,2,1,0:T(8,128)(2,1)S(1)}, u32[]{:S(2)}, u32[]{:S(2)}) collective-permute-start(bf16[4,4,64,128]{3,2,1,0:T(8,128)(2,1)} %copy-done.2), channel_id=1, source_target_pairs={{4,0},{5,1},{6,2},{7,3},{0,4},{1,5},{2,6},{3,7},{12,8},{13,9},{14,... | collective-permute-start | bytes 786440 | tf_op jit(solution)/shard_map/ppermute | solution.py:59
  68.0 1.7 %collective-permute-start.25 = (bf16[4,4,64,128]{3,2,1,0:T(8,128)(2,1)}, bf16[4,4,64,128]{3,2,1,0:T(8,128)(2,1)S(1)}, u32[]{:S(2)}, u32[]{:S(2)}) collective-permute-start(bf16[4,4,64,128]{3,2,1,0:T(8,128)(2,1)} %collective-permute-done.21.refs_10_), channel_id=1, source_target_pairs={{4,0},{5,1},{6,2},{7,3},{0,4},{1,5},{2,6},{3,7},{12,8},{13,9},{14,... | collective-permute-start | bytes 786440 | tf_op jit(solution)/shard_map/ppermute | solution.py:59
  69.7 1.5 %collective-permute-start.24 = (bf16[4,4,64,128]{3,2,1,0:T(8,128)(2,1)S(1)}, bf16[4,4,64,128]{3,2,1,0:T(8,128)(2,1)S(1)}, u32[]{:S(2)}, u32[]{:S(2)}) collective-permute-start(bf16[4,4,64,128]{3,2,1,0:T(8,128)(2,1)S(1)} %collective-permute-done.20.refs_9_), channel_id=1, source_target_pairs={{4,0},{5,1},{6,2},{7,3},{0,4},{1,5},{2,6},{3,7},{12,8},{13,9},{14,... | collective-permute-start | bytes 786440 | tf_op jit(solution)/shard_map/ppermute | solution.py:59
  71.3 1.0 %copy-start.3 = (bf16[4,4,64,128]{3,2,1,0:T(8,128)(2,1)S(1)}, bf16[4,4,64,128]{3,2,1,0:T(8,128)(2,1)}, u32[]{:S(2)}) copy-start(bf16[4,4,64,128]{3,2,1,0:T(8,128)(2,1)} %copy-done.2) | copy-start | bytes 786436
